TPU v7x, 512 devices: a whole 4x8x8 slice. The times are simulated.
512 devices in a mesh: sp: 64 (over z, y), tp: 8 (over x, core).
Axes of the slice: x: 4, y: 8, z: 8, core: 2. Of those that a mesh axis runs over, the one named last changes fastest.
Arguments:
- tokens: bfloat16 [65536, 2048], P('sp'), may hold values from -6 to 6
- norm_gain: float32 [2048], replicated, may hold values from 0.1 to 1.9
- w_query: bfloat16 [2048, 512], P(None, 'tp'), may hold values from -0.79549513 to 0.79549513
- w_key: bfloat16 [2048, 128], P('sp'), may hold values from -0.79549513 to 0.79549513
- w_value: bfloat16 [2048, 128], P('sp'), may hold values from -0.125 to 0.125
- w_pool_in: bfloat16 [2048, 512], P(None, 'tp'), may hold values from -0.125 to 0.125
- sink_logit: float32 [8], P('tp'), may hold values from 3 to 7
- pool_scale: float32 [512], P('tp'), may hold values from 0.05 to 0.5
- w_out: bfloat16 [1024, 2048], P('tp', 'sp'), may hold values from -0.75 to 0.75
Outputs:
- mixed_out: bfloat16 [65536, 2048], P(('sp', 'tp'))
All inputs are finite; a program needn't handle non-finite values.
Results may differ from a plain program's by a relative error of at most 0.03.
The roundings to bfloat16 on the way count: a program that leaves them out, or rounds other values in their place, can miss the bound.
Values may be sent and summed in bfloat16 or wider, within the bound.
No kernel may reach another device: no remote copies, remote signals or barrier semaphores. Data moves between devices by JAX's collectives and lax.ppermute only.
A program may use at most 64 MiB of HBM per device.

v0:
```python
import jax
import jax.numpy as jnp
from jax import lax
from jax.sharding import PartitionSpec as P

HEAD = 64
QH = 8
KVH = 2
POOL_CH = 128
WINDOW = 128
QB = 128


NEG_BIG = -1e30
POOL_SPANS = (2, 4, 8, 16)


def in_one_piece(arrays, axis, dim, along):
    both = jnp.concatenate(arrays, axis=along)
    filled, at, finished = (lax.all_gather(both, axis, axis=dim, tiled=True), 0, [])
    for a in arrays:
        finished.append(lax.slice_in_dim(filled, at, at + a.shape[along], axis=along))
        at += a.shape[along]
    return tuple(finished)


def extended(block, sides, width):
    for axis, dim in sides:
        count = lax.axis_size(axis)
        forward = [(i, i + 1) for i in range(count - 1)]
        backward = [(target, source) for source, target in forward]
        low = lax.ppermute(
            lax.slice_in_dim(block, block.shape[dim] - width, None, axis=dim), axis, forward
        )
        high = lax.ppermute(lax.slice_in_dim(block, 0, width, axis=dim), axis, backward)
        block = jnp.concatenate([low, block, high], axis=dim)
    return block


def rows_first(arrays, axis, dims):
    turned = [jnp.moveaxis(a, dim, 0) for a, dim in zip(arrays, dims)]
    both = jnp.concatenate([t.reshape(len(t), -1) for t in turned], axis=1)
    filled, at, finished = (lax.all_gather(both, axis, axis=0, tiled=True), 0, [])
    for t, dim in zip(turned, dims):
        section = filled[:, at : at + t[0].size].reshape(-1, *t.shape[1:])
        finished.append(jnp.moveaxis(section, 0, dim))
        at += t[0].size
    return tuple(finished)


def in_order(tiles, dim):
    tiles = jnp.moveaxis(tiles, 0, dim)
    shape = tiles.shape
    return tiles.reshape(*shape[:dim], shape[dim] * shape[dim + 1], *shape[dim + 2 :])


def from_everyone(x, axis):
    peers = lax.axis_size(axis)
    return lax.all_to_all(jnp.broadcast_to(x[None], (peers, *x.shape)), axis, 0, 0, tiled=True)


def collect(x, axis, dim):
    return in_order(from_everyone(x, axis), dim)


def layer_normed(tokens, norm_gain):
    values = tokens.astype(jnp.float32)
    center = jnp.mean(values, axis=-1, keepdims=True)
    spread = jnp.mean(jnp.square(values - center), axis=-1, keepdims=True)
    return ((values - center) * lax.rsqrt(spread + 1e-06) * norm_gain).astype(jnp.bfloat16)


def rotate(values, positions):
    half = HEAD // 2
    inverse = 10000.0 ** (-jnp.arange(half, dtype=jnp.float32) / half)
    angles = positions[:, None] * inverse[None, :]
    cosine = jnp.cos(angles)[:, None, :]
    sine = jnp.sin(angles)[:, None, :]
    first = values[..., :half]
    second = values[..., half:]
    return jnp.concatenate(
        [first * cosine - second * sine, first * sine + second * cosine], axis=-1
    )


def body(tokens, norm_gain, w_query, w_key, w_value, w_pool_in, sink_logit, pool_scale, w_out):
    local_rows = tokens.shape[0]
    seq_total = local_rows * lax.axis_size("sp")
    offset = lax.axis_index("sp") * local_rows
    tp_place = lax.axis_index("tp")
    local_heads = w_query.shape[1] // HEAD
    local_pool = w_pool_in.shape[1]
    reach = POOL_SPANS[-1] // 2
    normed = layer_normed(tokens, norm_gain)
    positions = (offset + jnp.arange(local_rows)).astype(jnp.float32)
    query = rotate(
        jnp.dot(normed, w_query, preferred_element_type=jnp.float32).reshape(
            local_rows, local_heads, HEAD
        ),
        positions,
    ).astype(jnp.bfloat16)
    key_head = tp_place * local_heads // (QH // KVH)
    key_cols = lax.dynamic_slice_in_dim(w_key, key_head * HEAD, HEAD, 1)
    value_cols = lax.dynamic_slice_in_dim(w_value, key_head * HEAD, HEAD, 1)
    pieces = in_one_piece((key_cols, value_cols), "sp", 0, 1)
    key_sum = jnp.dot(normed, pieces[0], preferred_element_type=jnp.float32)
    value_sum = jnp.dot(normed, pieces[1], preferred_element_type=jnp.float32)
    key = rotate(key_sum[:, None, :], positions)[:, 0, :].astype(jnp.bfloat16)
    value = value_sum.astype(jnp.bfloat16)
    key_value = jnp.concatenate([key, value], axis=1)
    pool_in = jnp.dot(normed, w_pool_in, preferred_element_type=jnp.float32).astype(jnp.bfloat16)
    widened = extended(jnp.concatenate([key_value, pool_in], axis=1), (("sp", 0),), WINDOW)
    kv_wide = widened[:, : 2 * HEAD]
    pool_wide = widened[WINDOW - reach : WINDOW + local_rows + reach, 2 * HEAD :]
    span = QB + 2 * WINDOW
    sink_here = sink_logit[:, None, None]
    results = []
    for block in range(local_rows // QB):
        queries = query[block * QB : (block + 1) * QB]
        keys = kv_wide[block * QB : block * QB + span, :HEAD]
        values = kv_wide[block * QB : block * QB + span, HEAD:]
        scores = jnp.einsum(
            "ihd,jd->hij", queries, keys, preferred_element_type=jnp.float32
        ) * HEAD ** (-0.5)
        query_pos = offset + block * QB + jnp.arange(QB)
        key_pos = offset + block * QB - WINDOW + jnp.arange(span)
        valid = (
            (jnp.abs(query_pos[:, None] - key_pos[None, :]) <= WINDOW)
            & (key_pos[None, :] >= 0)
            & (key_pos[None, :] < seq_total)
        )
        scores = jnp.where(valid, scores, NEG_BIG)
        highest = jnp.maximum(jnp.max(scores, axis=-1, keepdims=True), sink_here)
        expo = jnp.where(valid, jnp.exp(scores - highest), 0.0)
        total = jnp.sum(expo, axis=-1, keepdims=True) + jnp.exp(sink_here - highest)
        weights = (expo / total).astype(jnp.bfloat16)
        result = jnp.einsum("hij,jd->ihd", weights, values, preferred_element_type=jnp.float32)
        results.append(result.reshape(QB, local_heads * HEAD).astype(jnp.bfloat16))
    attended = jnp.concatenate(results, axis=0)
    pool_vals = pool_wide.astype(jnp.float32)
    window_sum = pool_vals
    global_pos = offset + jnp.arange(local_rows)
    channel = tp_place * local_pool + jnp.arange(local_pool)
    window_group = channel // POOL_CH
    measured = jnp.zeros((local_rows, local_pool), jnp.float32)
    stride = 1
    for index, width in enumerate(POOL_SPANS):
        window_sum = window_sum[:-stride] + window_sum[stride:]
        stride = width
        sums = window_sum[reach - width // 2 : reach - width // 2 + local_rows]
        counted = (
            jnp.minimum(global_pos + width // 2, seq_total)
            - jnp.maximum(global_pos - width // 2, 0)
        ).astype(jnp.float32)
        measured = measured + jnp.where(
            window_group[None, :] == index, sums / counted[:, None], 0.0
        )
    pooled = ((measured - pool_vals[reach : reach + local_rows]) * pool_scale).astype(jnp.bfloat16)
    attended_all, pooled_all = rows_first((attended, pooled), "tp", (1, 1))
    joined_all = jnp.concatenate([attended_all, pooled_all], axis=1)
    own_rows = collect(w_out, "sp", 1)
    column_block = lax.all_to_all(own_rows, "tp", split_axis=1, concat_axis=0, tiled=True)
    partial_cols = jnp.dot(joined_all, column_block, preferred_element_type=jnp.float32).astype(
        jnp.bfloat16
    )
    return lax.all_to_all(partial_cols, "tp", split_axis=0, concat_axis=1, tiled=True)


def solution(mesh):
    in_specs = (
        P("sp", None),
        P(),
        P(None, "tp"),
        P("sp", None),
        P("sp", None),
        P(None, "tp"),
        P("tp"),
        P("tp"),
        P("tp", "sp"),
    )
    out_specs = P(("sp", "tp"), None)
    return jax.shard_map(body, mesh=mesh, in_specs=in_specs, out_specs=out_specs, check_vma=False)
```

profile of v0, /device:TPU:1, one launch (start us, length us, event | category | flops | bytes accessed | tf_op | source)
XLA Modules:
  0.0 157.3 jit_solution(11905383082164041092)
XLA Ops:
  6.6 0.9 constant_dynamic-slice_fusion
  7.6 46.0 %all_gather.6 = bf16[2048,128]{1,0:T(8,128)(2,1)S(1)} all-gather(bf16[32,128]{1,0:T(8,128)(2,1)S(1)} %pad_maximum_fusion.22), channel_id=1, replica_groups=mesh['sp'=64,'tp'=8] {'sp'}, dimensions={0}, use_global_device_ids=true | all-gather | bytes 532480 | tf_op jit(solution)/shard_map/all_gather | solution.py:20
  53.6 2.8 %convert_reduce_fusion = f32[1024]{0:T(1024)S(1)} fusion(bf16[1024,2048]{1,0:T(8,128)(2,1)} %param.9), kind=kLoop, calls=%fused_computation.1 | loop fusion | flops 4193280 | bytes 4198400 | tf_op jit(solution)/shard_map/reduce_sum | solution.py:68
  56.5 1.2 fusion.2
  57.7 1.6 %fusion.4 = bf16[1024,2048]{1,0:T(8,128)(2,1)S(1)} fusion(bf16[1024,2048]{1,0:T(8,128)(2,1)S(1)} %copy-done.3, f32[2048]{0:T(1024)S(1)} %copy-done.6, f32[1024]{0:T(1024)S(1)} %add_rsqrt_fusion, f32[1024]{0:T(1024)S(1)} %broadcast_multiply_fusion), kind=kLoop, calls=%fused_computation.6 | loop fusion | flops 10485760 | bytes 8404992 | tf_op jit(solution)/shard_map/convert_element_type | solution.py:70
  59.4 1.4 convolution_bitcast_fusion.1
  60.8 0.5 copy-done.1
  61.3 1.5 convolution_convert_fusion.1
  62.8 3.7 %convolution_bitcast_fusion = f32[1024,1,64]{0,2,1:T(8,128)S(1)} fusion(bf16[1024,2048]{1,0:T(8,128)(2,1)} %copy-done.1, bf16[2048,64]{0,1:T(8,128)(2,1)S(1)} %copy-done), kind=kOutput, calls=%fused_computation.12 | convolution fusion | flops 268435456 | bytes 4718592 | tf_op jit(solution)/shard_map/dot_general | solution.py:97
  66.5 1.4 convolution_convert_fusion
  67.9 0.6 fusion.96
  68.6 1.3 collective-permute-start.1
  69.9 4.2 %collective-permute-start = (bf16[128,192]{0,1:T(8,128)(2,1)S(1)}, bf16[128,192]{0,1:T(8,128)(2,1)S(1)}, u32[]{:S(2)}, u32[]{:S(2)}) collective-permute-start(bf16[128,192]{0,1:T(8,128)(2,1)S(1)} %get-tuple-element.7), channel_id=1, source_target_pairs={{0,8},{8,16},{16,24},{24,32},{32,40},{40,48},{48,56},{56,64},{64,7... | collective-permute-start | bytes 147464 | tf_op jit(solution)/shard_map/ppermute | solution.py:32
  80.5 0.4 fusion.31
  80.8 0.4 fusion.33
  82.3 0.4 fusion.41
  82.7 0.4 fusion.98
  83.4 0.7 pad_maximum_fusion
  84.3 21.6 %all_to_all.43 = bf16[64,128,32]{1,2,0:T(8,128)(2,1)S(1)} all-to-all(bf16[64,128,32]{1,2,0:T(8,128)(2,1)S(1)} %broadcast_in_dim.80), channel_id=1, replica_groups=mesh['sp'=64,'tp'=8] {'sp'}, dimensions={0} | all-to-all | bytes 1048576 | tf_op jit(solution)/shard_map/all_to_all | solution.py:59
  105.9 28.2 %all_to_all.44 = bf16[128,8,256]{0,2,1:T(8,128)(2,1)S(1)} all-to-all(bf16[128,8,256]{0,2,1:T(8,128)(2,1)S(1)} %bitcast.252), channel_id=1, replica_groups=mesh['sp'=64,'tp'=8] {'tp'}, dimensions={1} | all-to-all | bytes 1048576 | tf_op jit(solution)/shard_map/all_to_all | solution.py:162
  134.3 1.7 %slice_bitcast_fusion.1 = (bf16[1024,512]{0,1:T(8,128)(2,1)S(1)}, bf16[1024,512]{0,1:T(8,128)(2,1)S(1)}) fusion(bf16[512,2048]{1,0:T(8,128)(2,1)} %all-gather.2.cloned.1.call-done), kind=kLoop, calls=%fused_computation.65 | loop fusion | bytes 4194304 | tf_op jit(solution)/shard_map/transpose | solution.py:46
  136.0 0.8 fusion.9
  136.8 12.8 %all_to_all.45 = bf16[8,128,256]{2,1,0:T(8,128)(2,1)S(1)} all-to-all(bf16[8,128,256]{2,1,0:T(8,128)(2,1)S(1)} %bitcast.256), channel_id=1, replica_groups=mesh['sp'=64,'tp'=8] {'tp'}, dimensions={0} | all-to-all | bytes 1048576 | tf_op jit(solution)/shard_map/all_to_all | solution.py:166
  149.6 0.8 copy.14
  (99 shorter events, 7.4 us)
Async XLA Ops:
  6.5 56.2 %copy-start = (bf16[2048,64]{0,1:T(8,128)(2,1)S(1)}, bf16[2048,64]{0,1:T(8,128)(2,1)}, u32[]{:S(2)}) copy-start(bf16[2048,64]{0,1:T(8,128)(2,1)} %param.11) | copy-start | bytes 786436
  6.5 127.8 %all-gather.2.cloned.1.call-start = ((), (), s32[]{:S(2)}) async-start(), calls=%async_computation.3 | async-start | bytes 2359296 | tf_op jit(solution)/shard_map/all_gather | solution.py:43
  6.6 49.9 %copy-start.3 = (bf16[1024,2048]{1,0:T(8,128)(2,1)S(1)}, bf16[1024,2048]{1,0:T(8,128)(2,1)}, u32[]{:S(2)}) copy-start(bf16[1024,2048]{1,0:T(8,128)(2,1)} %param.9) | copy-start | bytes 12582916
  53.6 4.1 %copy-start.6 = (f32[2048]{0:T(1024)S(1)}, f32[2048]{0:T(1024)}, u32[]{:S(2)}) copy-start(f32[2048]{0:T(1024)} %param.10) | copy-start | bytes 24580
  59.3 1.9 %copy-start.1 = (bf16[1024,2048]{1,0:T(8,128)(2,1)}, bf16[1024,2048]{1,0:T(8,128)(2,1)S(1)}, u32[]{:S(2)}) copy-start(bf16[1024,2048]{1,0:T(8,128)(2,1)S(1)} %fusion.4) | copy-start | bytes 12582916
  61.3 5.2 %copy-start.4 = (bf16[2048,64]{0,1:T(8,128)(2,1)S(1)}, bf16[2048,64]{0,1:T(8,128)(2,1)}, u32[]{:S(2)}) copy-start(bf16[2048,64]{0,1:T(8,128)(2,1)} %param.14) | copy-start | bytes 786436
  62.7 3.8 %copy-start.2 = (bf16[1024,2048]{1,0:T(8,128)(2,1)S(1)}, bf16[1024,2048]{1,0:T(8,128)(2,1)}, u32[]{:S(2)}) copy-start(bf16[1024,2048]{1,0:T(8,128)(2,1)} %copy-done.1) | copy-start | bytes 12582916
  68.6 9.7 %collective-permute-start.1 = (bf16[128,192]{0,1:T(8,128)(2,1)S(1)}, bf16[128,192]{0,1:T(8,128)(2,1)S(1)}, u32[]{:S(2)}, u32[]{:S(2)}) collective-permute-start(bf16[128,192]{0,1:T(8,128)(2,1)S(1)} %get-tuple-element.8), channel_id=1, source_target_pairs={{8,0},{16,8},{24,16},{32,24},{40,32},{48,40},{56,48},{64,56},{72,6... | collective-permute-start | bytes 147464 | tf_op jit(solution)/shard_map/ppermute | solution.py:35
  69.9 8.5 %collective-permute-start = (bf16[128,192]{0,1:T(8,128)(2,1)S(1)}, bf16[128,192]{0,1:T(8,128)(2,1)S(1)}, u32[]{:S(2)}, u32[]{:S(2)}) collective-permute-start(bf16[128,192]{0,1:T(8,128)(2,1)S(1)} %get-tuple-element.7), channel_id=1, source_target_pairs={{0,8},{8,16},{16,24},{24,32},{32,40},{40,48},{48,56},{56,64},{64,7... | collective-permute-start | bytes 147464 | tf_op jit(solution)/shard_map/ppermute | solution.py:32
  80.1 2.5 %copy-start.7 = (f32[64]{0:T(128)S(1)}, f32[64]{0:T(128)}, u32[]{:S(2)}) copy-start(f32[64]{0:T(128)} %param.16) | copy-start | bytes 772
  81.2 3.0 %copy-start.5 = (bf16[128,32]{0,1:T(8,128)(2,1)S(1)}, bf16[128,32]{0,1:T(8,128)(2,1)}, u32[]{:S(2)}) copy-start(bf16[128,32]{0,1:T(8,128)(2,1)} %param.17) | copy-start | bytes 24580
Sparse Core Ops, SparseCore 0:
  84.3 39.5 all-gather.1
where the time goes:
time: 158 us; the launch traced here: 157 us
  blocking collectives  109 us (69%)
  between operations  14.6 us (9%)
  matrix products  13.8 us (9%)
  other arithmetic  10.3 us (7%)
  starting transfers between devices  5.46 us (3%)
  local copies, waits for them, and re-layouts  4.48 us (3%)
    all_gather x1, blocking collectives, in_one_piece(): lax.all_gather(both, axis, axis=dim, tiled=True)  46 us
    all_to_all x1, blocking collectives, body(): lax.all_to_all(own_rows, 'tp', split_axis=1, concat_axis=0, tiled=True)  28.2 us
    all_to_all x1, blocking collectives, from_everyone(): lax.all_to_all(jnp.broadcast_to(x[None], (peers, *x.shape)), axis, 0, 0,...  21.6 us
    all_to_all x1, blocking collectives, body(): lax.all_to_all(partial_cols, 'tp', split_axis=0, concat_axis=1, tiled=True)  12.8 us
    ppermute x1, starting transfers between devices, extended(): lax.ppermute(lax.slice_in_dim(block, block.shape[dim] - width, None, axis...  4.17 us
    dot_general x1, matrix products, body(): jnp.dot(normed, w_query, preferred_element_type=jnp.float32)  3.73 us
  transfers between devices with their start and end apart: 3, of which 0 were waited for; matrix products, arithmetic and copies ran while one was open for 2% of the time, Pallas kernels for 0%

commit v1 on v0

--- a/solution.py
+++ b/solution.py
@@ -1,6 +1,7 @@
 import jax
 import jax.numpy as jnp
 from jax import lax
+from jax.sharding import Mesh
 from jax.sharding import PartitionSpec as P
 
 HEAD = 64
@@ -13,15 +14,8 @@
 
 NEG_BIG = -1e30
 POOL_SPANS = (2, 4, 8, 16)
-
-
-def in_one_piece(arrays, axis, dim, along):
-    both = jnp.concatenate(arrays, axis=along)
-    filled, at, finished = (lax.all_gather(both, axis, axis=dim, tiled=True), 0, [])
-    for a in arrays:
-        finished.append(lax.slice_in_dim(filled, at, at + a.shape[along], axis=along))
-        at += a.shape[along]
-    return tuple(finished)
+SP = ("z", "y")
+TP = ("x", "c")
 
 
 def extended(block, sides, width):
@@ -37,30 +31,9 @@
     return block
 
 
-def rows_first(arrays, axis, dims):
-    turned = [jnp.moveaxis(a, dim, 0) for a, dim in zip(arrays, dims)]
-    both = jnp.concatenate([t.reshape(len(t), -1) for t in turned], axis=1)
-    filled, at, finished = (lax.all_gather(both, axis, axis=0, tiled=True), 0, [])
-    for t, dim in zip(turned, dims):
-        section = filled[:, at : at + t[0].size].reshape(-1, *t.shape[1:])
-        finished.append(jnp.moveaxis(section, 0, dim))
-        at += t[0].size
-    return tuple(finished)
-
-
-def in_order(tiles, dim):
-    tiles = jnp.moveaxis(tiles, 0, dim)
-    shape = tiles.shape
-    return tiles.reshape(*shape[:dim], shape[dim] * shape[dim + 1], *shape[dim + 2 :])
-
-
 def from_everyone(x, axis):
     peers = lax.axis_size(axis)
     return lax.all_to_all(jnp.broadcast_to(x[None], (peers, *x.shape)), axis, 0, 0, tiled=True)
-
-
-def collect(x, axis, dim):
-    return in_order(from_everyone(x, axis), dim)
 
 
 def layer_normed(tokens, norm_gain):
@@ -83,11 +56,23 @@
     )
 
 
+def swapped(piece):
+    side = lax.axis_size("z")
+    place = lambda z, y, t: (z * side + y) * side + t
+    pairs = [
+        (place(z, y, t), place(t, y, z))
+        for z in range(side)
+        for y in range(side)
+        for t in range(side)
+    ]
+    return lax.ppermute(piece, ("z", "y", "x", "c"), pairs)
+
+
 def body(tokens, norm_gain, w_query, w_key, w_value, w_pool_in, sink_logit, pool_scale, w_out):
     local_rows = tokens.shape[0]
-    seq_total = local_rows * lax.axis_size("sp")
-    offset = lax.axis_index("sp") * local_rows
-    tp_place = lax.axis_index("tp")
+    seq_total = local_rows * lax.axis_size(SP)
+    offset = lax.axis_index(SP) * local_rows
+    tp_place = lax.axis_index(TP)
     local_heads = w_query.shape[1] // HEAD
     local_pool = w_pool_in.shape[1]
     reach = POOL_SPANS[-1] // 2
@@ -102,14 +87,18 @@
     key_head = tp_place * local_heads // (QH // KVH)
     key_cols = lax.dynamic_slice_in_dim(w_key, key_head * HEAD, HEAD, 1)
     value_cols = lax.dynamic_slice_in_dim(w_value, key_head * HEAD, HEAD, 1)
-    pieces = in_one_piece((key_cols, value_cols), "sp", 0, 1)
-    key_sum = jnp.dot(normed, pieces[0], preferred_element_type=jnp.float32)
-    value_sum = jnp.dot(normed, pieces[1], preferred_element_type=jnp.float32)
+    out_piece = swapped(w_out.T)
+    both = jnp.concatenate([jnp.concatenate([key_cols, value_cols], axis=1), out_piece], axis=0)
+    weights_all = from_everyone(both, SP)
+    kv_cols = weights_all[:, : key_cols.shape[0]].reshape(-1, 2 * HEAD)
+    out_cols = weights_all[:, key_cols.shape[0] :].reshape(lax.axis_size("z"), -1, w_out.shape[0])
+    kv_sum = jnp.dot(normed, kv_cols, preferred_element_type=jnp.float32)
+    key_sum, value_sum = kv_sum[:, :HEAD], kv_sum[:, HEAD:]
     key = rotate(key_sum[:, None, :], positions)[:, 0, :].astype(jnp.bfloat16)
     value = value_sum.astype(jnp.bfloat16)
     key_value = jnp.concatenate([key, value], axis=1)
     pool_in = jnp.dot(normed, w_pool_in, preferred_element_type=jnp.float32).astype(jnp.bfloat16)
-    widened = extended(jnp.concatenate([key_value, pool_in], axis=1), (("sp", 0),), WINDOW)
+    widened = extended(jnp.concatenate([key_value, pool_in], axis=1), ((SP, 0),), WINDOW)
     kv_wide = widened[:, : 2 * HEAD]
     pool_wide = widened[WINDOW - reach : WINDOW + local_rows + reach, 2 * HEAD :]
     span = QB + 2 * WINDOW
@@ -156,27 +145,30 @@
             window_group[None, :] == index, sums / counted[:, None], 0.0
         )
     pooled = ((measured - pool_vals[reach : reach + local_rows]) * pool_scale).astype(jnp.bfloat16)
-    attended_all, pooled_all = rows_first((attended, pooled), "tp", (1, 1))
-    joined_all = jnp.concatenate([attended_all, pooled_all], axis=1)
-    own_rows = collect(w_out, "sp", 1)
-    column_block = lax.all_to_all(own_rows, "tp", split_axis=1, concat_axis=0, tiled=True)
-    partial_cols = jnp.dot(joined_all, column_block, preferred_element_type=jnp.float32).astype(
-        jnp.bfloat16
-    )
-    return lax.all_to_all(partial_cols, "tp", split_axis=0, concat_axis=1, tiled=True)
+    local = jnp.concatenate([attended, pooled], axis=1)
+    joined_all = from_everyone(local, TP)
+    count = joined_all.shape[0]
+    halves = out_cols.reshape(2, count // 2, -1, 2, HEAD)
+    matched = jnp.moveaxis(halves, 3, 2).reshape(2, count, -1, HEAD)
+    matched = jnp.concatenate([matched[0], matched[1]], axis=2)
+    partial_cols = jnp.einsum(
+        "ptc,pnc->tn", joined_all, matched, preferred_element_type=jnp.float32
+    ).astype(jnp.bfloat16)
+    return lax.all_to_all(partial_cols, TP, split_axis=0, concat_axis=1, tiled=True)
 
 
 def solution(mesh):
+    mesh = Mesh(mesh.devices.reshape(8, 8, 4, 2), SP + TP)
     in_specs = (
-        P("sp", None),
+        P(SP, None),
         P(),
-        P(None, "tp"),
-        P("sp", None),
-        P("sp", None),
-        P(None, "tp"),
-        P("tp"),
-        P("tp"),
-        P("tp", "sp"),
+        P(None, TP),
+        P(SP, None),
+        P(SP, None),
+        P(None, TP),
+        P(TP),
+        P(TP),
+        P(TP, SP),
     )
-    out_specs = P(("sp", "tp"), None)
+    out_specs = P(SP + TP, None)
     return jax.shard_map(body, mesh=mesh, in_specs=in_specs, out_specs=out_specs, check_vma=False)

time: 158 us -> 127 us (0.80)
  blocking collectives: 109 us -> 12.7 us
  waiting for transfers between devices: 0.04 us -> 40.2 us
  starting transfers between devices: 5.46 us -> 38.6 us
  between operations: 14.6 us -> 1.33 us
  local copies, waits for them, and re-layouts: 4.48 us -> 8.84 us
  other arithmetic: 10.3 us -> 11.9 us
    all_to_all x3 -> x1, blocking collectives: 62.6 us -> 12.7 us  [body(): lax.all_to_all(partial_cols, TP, split_axis=0, concat_axis=1, tiled=True)]
    all_gather x1 -> x0, blocking collectives: 46 us -> none  [in_one_piece(): lax.all_gather(both, axis, axis=dim, tiled=True)]
    all_to_all x0 -> x2, waiting for transfers between devices: none -> 40.2 us  [from_everyone(): lax.all_to_all(jnp.broadcast_to(x[None], (peers, *x.shape)), axis, 0, 0,...]
    all_to_all x0 -> x2, starting transfers between devices: none -> 27.1 us  [from_everyone(): lax.all_to_all(jnp.broadcast_to(x[None], (peers, *x.shape)), axis, 0, 0,...]
    ppermute x0 -> x1, starting transfers between devices: none -> 5.51 us  [swapped(): return lax.ppermute(piece, ('z', 'y', 'x', 'c'), pairs)]
    broadcast_in_dim x1 -> x2, local copies, waits for them, and re-layouts: 0.07 us -> 2.86 us  [from_everyone(): jnp.broadcast_to(x[None], (peers, *x.shape))]
    another operation x0 -> x1, local copies, waits for them, and re-layouts: none -> 2.44 us  [body(): halves = out_cols.reshape(2, count // 2, -1, 2, HEAD)]
    dot_general x1, matrix products: 3.73 us -> 1.39 us  [body(): jnp.dot(normed, w_query, preferred_element_type=jnp.float32)]
  transfers between devices with their start and end apart: 3 -> 5, of which waited for: 0 -> 2; matrix products, arithmetic and copies ran while one was open for 2% -> 14% of each run, Pallas kernels for 0% -> 0%
where the time goes in v1:
time: 127 us; the launch traced here: 126 us
  waiting for transfers between devices  40.2 us (32%)
  starting transfers between devices  38.6 us (30%)
  blocking collectives  12.7 us (10%)
  matrix products  12.4 us (10%)
  other arithmetic  11.9 us (9%)
  local copies, waits for them, and re-layouts  8.84 us (7%)
  between operations  1.33 us (1%)
    all_to_all x2, waiting for transfers between devices, from_everyone(): lax.all_to_all(jnp.broadcast_to(x[None], (peers, *x.shape)), axis, 0, 0,...  40.2 us
    all_to_all x2, starting transfers between devices, from_everyone(): lax.all_to_all(jnp.broadcast_to(x[None], (peers, *x.shape)), axis, 0, 0,...  27.1 us
    all_to_all x1, blocking collectives, body(): lax.all_to_all(partial_cols, TP, split_axis=0, concat_axis=1, tiled=True)  12.7 us
    ppermute x1, starting transfers between devices, swapped(): return lax.ppermute(piece, ('z', 'y', 'x', 'c'), pairs)  5.51 us
    ppermute x1, starting transfers between devices, extended(): lax.ppermute(lax.slice_in_dim(block, block.shape[dim] - width, None, axis...  4.69 us
    dot_general x1, matrix products, body(): kv_sum = jnp.dot(normed, kv_cols, preferred_element_type=jnp.float32)  3.71 us
    reduce_sum x1, other arithmetic, layer_normed(): spread = jnp.mean(jnp.square(values - center), axis=-1, keepdims=True)  3.56 us
    broadcast_in_dim x2, local copies, waits for them, and re-layouts, from_everyone(): jnp.broadcast_to(x[None], (peers, *x.shape))  2.86 us
  transfers between devices with their start and end apart: 5, of which 2 were waited for; matrix products, arithmetic and copies ran while one was open for 14% of the time, Pallas kernels for 0%

profile of v1, /device:TPU:1, one launch (start us, length us, event | category | flops | bytes accessed | tf_op | source)
XLA Modules:
  0.0 125.9 jit_solution(2501059769715028969)
XLA Ops:
  0.0 5.5 %collective-permute-start = (bf16[32,128]{1,0:T(8,128)(2,1)}, bf16[32,128]{1,0:T(8,128)(2,1)S(1)}, u32[]{:S(2)}, u32[]{:S(2)}) collective-permute-start(bf16[32,128]{1,0:T(8,128)(2,1)} %bitcast.255), channel_id=1, source_target_pairs={{0,0},{1,64},{2,128},{3,192},{4,256},{5,320},{6,384},{7,448},{8,8}... | collective-permute-start | bytes 24584 | tf_op jit(solution)/shard_map/ppermute | solution.py:68
  6.0 2.8 %convert_reduce_fusion = f32[1024]{0:T(1024)S(1)} fusion(bf16[1024,2048]{1,0:T(8,128)(2,1)} %param.9), kind=kLoop, calls=%fused_computation.1 | loop fusion | flops 4193280 | bytes 4198400 | tf_op jit(solution)/shard_map/reduce_sum | solution.py:41
  9.6 1.2 broadcast_in_dim.70
  10.9 18.6 %all-to-all-start = ((bf16[64,64,128]{2,1,0:T(8,128)(2,1)}), bf16[64,64,128]{2,1,0:T(8,128)(2,1)S(1)}, u32[]{:S(2)}, u32[]{:S(2)}) async-start(bf16[64,64,128]{2,1,0:T(8,128)(2,1)} %broadcast_in_dim.70), calls=%async_computation | async-start | bytes 2097152 | tf_op jit(solution)/shard_map/all_to_all | solution.py:36
  29.5 3.6 %fusion.2 = f32[1024]{0:T(1024)S(1)} fusion(bf16[1024,2048]{1,0:T(8,128)(2,1)} %param.9, f32[1024]{0:T(1024)S(1)} %broadcast_multiply_fusion), kind=kLoop, calls=%fused_computation.4 | loop fusion | flops 8387584 | bytes 4202496 | tf_op jit(solution)/shard_map/reduce_sum | solution.py:42
  33.1 1.6 %fusion.4 = bf16[1024,2048]{1,0:T(8,128)(2,1)S(1)} fusion(bf16[1024,2048]{1,0:T(8,128)(2,1)S(1)} %copy-done.2, f32[2048]{0:T(1024)S(1)} %copy-done.6, f32[1024]{0:T(1024)S(1)} %add_rsqrt_fusion, f32[1024]{0:T(1024)S(1)} %broadcast_multiply_fusion), kind=kLoop, calls=%fused_computation.6 | loop fusion | flops 10485760 | bytes 8404992 | tf_op jit(solution)/shard_map/convert_element_type | solution.py:43
  34.8 1.4 %convolution_bitcast_fusion.1 = f32[1024,1,64]{0,2,1:T(8,128)S(1)} fusion(bf16[1024,2048]{1,0:T(8,128)(2,1)S(1)} %fusion.4, bf16[2048,64]{0,1:T(8,128)(2,1)S(1)} %copy-done), kind=kOutput, calls=%fused_computation.9 | convolution fusion | flops 268435456 | bytes 4718592 | tf_op jit(solution)/shard_map/dot_general | solution.py:82
  36.2 0.5 copy-done.1
  36.7 1.4 %convolution_convert_fusion = bf16[1024,64]{0,1:T(8,128)(2,1)S(1)} fusion(bf16[1024,2048]{1,0:T(8,128)(2,1)S(1)} %fusion.4, bf16[2048,64]{0,1:T(8,128)(2,1)S(1)} %copy-done.3), kind=kOutput, calls=%fused_computation.10 | convolution fusion | flops 268500992 | bytes 4587520 | tf_op jit(solution)/shard_map/dot_general | solution.py:100
  38.1 17.3 %all-to-all-done = bf16[64,64,128]{2,1,0:T(8,128)(2,1)S(1)} async-done(((bf16[64,64,128]{2,1,0:T(8,128)(2,1)}), bf16[64,64,128]{2,1,0:T(8,128)(2,1)S(1)}, u32[]{:S(2)}, u32[]{:S(2)}) %all-to-all-start) | async-done | bytes 1048608 | tf_op jit(solution)/shard_map/all_to_all | solution.py:36
  55.4 0.9 fusion.210
  56.3 3.7 %fusion.212 = (bf16[1024,128]{0,1:T(8,128)(2,1)S(1)}, f32[1024,128]{0,1:T(8,128)S(1)}) fusion(bf16[1024,2048]{1,0:T(8,128)(2,1)} %copy-done.1, bf16[2048,128]{1,0:T(8,128)(2,1)S(1)} %bitcast.251), kind=kOutput, calls=%fused_computation.339 | convolution fusion | flops 537001984 | bytes 5505024 | tf_op jit(solution)/shard_map/dot_general | solution.py:95
  60.0 0.6 fusion.91
  60.7 1.3 %collective-permute-start.2 = (bf16[128,192]{0,1:T(8,128)(2,1)S(1)}, bf16[128,192]{0,1:T(8,128)(2,1)S(1)}, u32[]{:S(2)}, u32[]{:S(2)}) collective-permute-start(bf16[128,192]{0,1:T(8,128)(2,1)S(1)} %get-tuple-element.10), channel_id=1, source_target_pairs={{8,0},{16,8},{24,16},{32,24},{40,32},{48,40},{56,48},{64,56},{72,6... | collective-permute-start | bytes 147464 | tf_op jit(solution)/shard_map/ppermute | solution.py:29
  62.0 4.7 %collective-permute-start.1 = (bf16[128,192]{0,1:T(8,128)(2,1)S(1)}, bf16[128,192]{0,1:T(8,128)(2,1)S(1)}, u32[]{:S(2)}, u32[]{:S(2)}) collective-permute-start(bf16[128,192]{0,1:T(8,128)(2,1)S(1)} %get-tuple-element.9), channel_id=1, source_target_pairs={{0,8},{8,16},{16,24},{24,32},{32,40},{40,48},{48,56},{56,64},{64,7... | collective-permute-start | bytes 147464 | tf_op jit(solution)/shard_map/ppermute | solution.py:26
  74.2 0.4 fusion.42
  75.2 1.6 %broadcast_in_dim.83 = bf16[8,1024,128]{2,1,0:T(8,128)(2,1)} broadcast(bf16[1024,128]{1,0:T(8,128)(2,1)S(1)} %copy.12), dimensions={1,2} | broadcast | bytes 2359296 | tf_op jit(solution)/shard_map/broadcast_in_dim | solution.py:36
  76.8 8.5 %all-to-all-start.1 = ((bf16[8,1024,128]{2,1,0:T(8,128)(2,1)}), bf16[8,1024,128]{2,1,0:T(8,128)(2,1)S(1)}, u32[]{:S(2)}, u32[]{:S(2)}) async-start(bf16[8,1024,128]{2,1,0:T(8,128)(2,1)} %broadcast_in_dim.83), calls=%async_computation.1 | async-start | bytes 4194304 | tf_op jit(solution)/shard_map/all_to_all | solution.py:36
  85.3 2.4 %reshape_reshape.3 = bf16[2,4,256,2,64]{4,3,2,1,0:T(2,128)(2,1)S(1)} reshape(bf16[64,32,128]{2,1,0:T(8,128)(2,1)} %get-tuple-element.7) | data formatting | bytes 1048576 | tf_op jit(solution)/shard_map/reshape;reshape | solution.py:151
  87.7 0.7 fusion.209
  88.6 22.9 %all-to-all-done.1 = bf16[8,1024,128]{2,1,0:T(8,128)(2,1)S(1)} async-done(((bf16[8,1024,128]{2,1,0:T(8,128)(2,1)}), bf16[8,1024,128]{2,1,0:T(8,128)(2,1)S(1)}, u32[]{:S(2)}, u32[]{:S(2)}) %all-to-all-start.1) | async-done | bytes 2097184 | tf_op jit(solution)/shard_map/all_to_all | solution.py:36
  111.5 0.8 fusion.5
  112.4 12.7 %all_to_all.29 = bf16[8,128,256]{2,1,0:T(8,128)(2,1)S(1)} all-to-all(bf16[8,128,256]{2,1,0:T(8,128)(2,1)S(1)} %bitcast.254), channel_id=1, replica_groups=mesh['z'=8,'y'=8,'x'=4,'c'=2] {'x','c'}, dimensions={0} | all-to-all | bytes 1048576 | tf_op jit(solution)/shard_map/all_to_all | solution.py:157
  125.1 0.8 copy.16
  (105 shorter events, 8.5 us)
Async XLA Ops:
  0.0 34.8 %copy-start = (bf16[2048,64]{0,1:T(8,128)(2,1)S(1)}, bf16[2048,64]{0,1:T(8,128)(2,1)}, u32[]{:S(2)}) copy-start(bf16[2048,64]{0,1:T(8,128)(2,1)} %param.11) | copy-start | bytes 786436
  0.0 8.8 %copy-start.5 = (bf16[32,128]{1,0:T(8,128)(2,1)S(1)}, bf16[32,128]{1,0:T(8,128)(2,1)}, u32[]{:S(2)}) copy-start(bf16[32,128]{1,0:T(8,128)(2,1)} %param.12) | copy-start | bytes 24580
  0.0 8.8 %copy-start.4 = (bf16[32,128]{1,0:T(8,128)(2,1)S(1)}, bf16[32,128]{1,0:T(8,128)(2,1)}, u32[]{:S(2)}) copy-start(bf16[32,128]{1,0:T(8,128)(2,1)} %param.13) | copy-start | bytes 24580
  0.0 9.5 %collective-permute-start = (bf16[32,128]{1,0:T(8,128)(2,1)}, bf16[32,128]{1,0:T(8,128)(2,1)S(1)}, u32[]{:S(2)}, u32[]{:S(2)}) collective-permute-start(bf16[32,128]{1,0:T(8,128)(2,1)} %bitcast.255), channel_id=1, source_target_pairs={{0,0},{1,64},{2,128},{3,192},{4,256},{5,320},{6,384},{7,448},{8,8}... | collective-permute-start | bytes 24584 | tf_op jit(solution)/shard_map/ppermute | solution.py:68
  8.8 24.3 %copy-start.6 = (f32[2048]{0:T(1024)S(1)}, f32[2048]{0:T(1024)}, u32[]{:S(2)}) copy-start(f32[2048]{0:T(1024)} %param.10) | copy-start | bytes 24580
  10.9 44.5 %all-to-all-start = ((bf16[64,64,128]{2,1,0:T(8,128)(2,1)}), bf16[64,64,128]{2,1,0:T(8,128)(2,1)S(1)}, u32[]{:S(2)}, u32[]{:S(2)}) async-start(bf16[64,64,128]{2,1,0:T(8,128)(2,1)} %broadcast_in_dim.70), calls=%async_computation | async-start | bytes 2097152 | tf_op jit(solution)/shard_map/all_to_all | solution.py:36
  29.5 3.6 %copy-start.2 = (bf16[1024,2048]{1,0:T(8,128)(2,1)S(1)}, bf16[1024,2048]{1,0:T(8,128)(2,1)}, u32[]{:S(2)}) copy-start(bf16[1024,2048]{1,0:T(8,128)(2,1)} %param.9) | copy-start | bytes 12582916
  34.8 1.9 %copy-start.1 = (bf16[1024,2048]{1,0:T(8,128)(2,1)}, bf16[1024,2048]{1,0:T(8,128)(2,1)S(1)}, u32[]{:S(2)}) copy-start(bf16[1024,2048]{1,0:T(8,128)(2,1)S(1)} %fusion.4) | copy-start | bytes 12582916
  34.8 1.9 %copy-start.3 = (bf16[2048,64]{0,1:T(8,128)(2,1)S(1)}, bf16[2048,64]{0,1:T(8,128)(2,1)}, u32[]{:S(2)}) copy-start(bf16[2048,64]{0,1:T(8,128)(2,1)} %param.14) | copy-start | bytes 786436
  60.7 9.2 %collective-permute-start.2 = (bf16[128,192]{0,1:T(8,128)(2,1)S(1)}, bf16[128,192]{0,1:T(8,128)(2,1)S(1)}, u32[]{:S(2)}, u32[]{:S(2)}) collective-permute-start(bf16[128,192]{0,1:T(8,128)(2,1)S(1)} %get-tuple-element.10), channel_id=1, source_target_pairs={{8,0},{16,8},{24,16},{32,24},{40,32},{48,40},{56,48},{64,56},{72,6... | collective-permute-start | bytes 147464 | tf_op jit(solution)/shard_map/ppermute | solution.py:29
  62.0 7.9 %collective-permute-start.1 = (bf16[128,192]{0,1:T(8,128)(2,1)S(1)}, bf16[128,192]{0,1:T(8,128)(2,1)S(1)}, u32[]{:S(2)}, u32[]{:S(2)}) collective-permute-start(bf16[128,192]{0,1:T(8,128)(2,1)S(1)} %get-tuple-element.9), channel_id=1, source_target_pairs={{0,8},{8,16},{16,24},{24,32},{32,40},{40,48},{48,56},{56,64},{64,7... | collective-permute-start | bytes 147464 | tf_op jit(solution)/shard_map/ppermute | solution.py:26
  71.7 2.5 %copy-start.7 = (f32[64]{0:T(128)S(1)}, f32[64]{0:T(128)}, u32[]{:S(2)}) copy-start(f32[64]{0:T(128)} %param.16) | copy-start | bytes 772
  76.8 34.7 %all-to-all-start.1 = ((bf16[8,1024,128]{2,1,0:T(8,128)(2,1)}), bf16[8,1024,128]{2,1,0:T(8,128)(2,1)S(1)}, u32[]{:S(2)}, u32[]{:S(2)}) async-start(bf16[8,1024,128]{2,1,0:T(8,128)(2,1)} %broadcast_in_dim.83), calls=%async_computation.1 | async-start | bytes 4194304 | tf_op jit(solution)/shard_map/all_to_all | solution.py:36

commit v2 on v1

v2 whole, which is shorter than its diff:
```python
import functools

import jax
import jax.numpy as jnp
from jax import lax
from jax.experimental import pallas as pl
from jax.experimental.pallas import tpu as pltpu
from jax.sharding import Mesh
from jax.sharding import PartitionSpec as P

HEAD = 64
WINDOW = 128
QB = 128
LANES = 128
ROWS = 256
EDGE = 16
POOL_SPANS = (2, 4, 8, 16)
NEG_BIG = -1e30
SP = ("z", "y")
TP = ("x", "c")
INTERPRET = False


def from_everyone(x, axis):
    peers = lax.axis_size(axis)
    return lax.all_to_all(jnp.broadcast_to(x[None], (peers, *x.shape)), axis, 0, 0, tiled=True)


def swapped(piece):
    side, depth = lax.axis_size("z"), lax.axis_size("y")
    place = lambda z, y, t: (z * depth + y) * side + t
    pairs = [
        (place(z, y, t), place(t, y, z))
        for z in range(side)
        for y in range(depth)
        for t in range(side)
    ]
    return lax.ppermute(piece, SP + TP, pairs)


def three_parts(x):
    high = lax.reduce_precision(x, 8, 7)
    middle = lax.reduce_precision(x - high, 8, 7)
    low = x - high - middle
    return jnp.stack([high, middle, low]).astype(jnp.bfloat16)


def rope_tables(offset, rows):
    half = HEAD // 2
    inverse = 10000.0 ** (-jnp.arange(half, dtype=jnp.float32) / half)
    positions = (offset + jnp.arange(rows)).astype(jnp.float32)
    angles = positions[:, None] * inverse[None, :]
    cosine, sine = jnp.cos(angles), jnp.sin(angles)
    return (
        jnp.concatenate([cosine] * 4, axis=1),
        jnp.concatenate([-sine, sine, -sine, sine], axis=1),
    )


def project(tokens, gain, qp, ex, cosine, sine, q_out, kv_out, pool_out, weights):
    @pl.when(pl.program_id(0) == 0)
    def _():
        depth = weights.shape[0]
        weights[:, :LANES] = qp[0, :depth]
        weights[:, LANES : 2 * LANES] = qp[1, :depth]
        weights[:, 2 * LANES :] = ex[:, : ex.shape[1] // 2].reshape(depth, LANES)

    values = tokens[...].astype(jnp.float32)
    center = jnp.mean(values, axis=-1, keepdims=True)
    values = values - center
    spread = jnp.mean(values * values, axis=-1, keepdims=True)
    normed = (values * lax.rsqrt(spread + 1e-06) * gain[...]).astype(jnp.bfloat16)
    sums = jnp.dot(normed, weights[...], preferred_element_type=jnp.float32)
    query = jnp.concatenate([sums[:, :HEAD], sums[:, 2 * HEAD : 3 * HEAD]], axis=1)
    pool = jnp.concatenate([sums[:, HEAD : 2 * HEAD], sums[:, 3 * HEAD : 4 * HEAD]], axis=1)
    kv = sums[:, 4 * HEAD :]
    lane = lax.broadcasted_iota(jnp.int32, (ROWS, LANES), 1)
    first = lane % HEAD < HEAD // 2

    def turned(x):
        other = jnp.where(first, pltpu.roll(x, LANES - HEAD // 2, 1), pltpu.roll(x, HEAD // 2, 1))
        return x * cosine[...] + other * sine[...]

    q_out[...] = (turned(query) * HEAD ** (-0.5)).astype(jnp.bfloat16)
    kv_out[...] = jnp.where(lane < HEAD, turned(kv), kv).astype(jnp.bfloat16)
    pool_out[...] = pool.astype(jnp.bfloat16)


def mix(blocks_total, place, sink, scale, q, kv, pool, halo, out, kv_wide, pool_wide):
    core, first_block, group = place[0], place[1], place[2]
    rows = q.shape[0]
    kv_wide[pl.ds(pl.multiple_of((1 - core) * QB, QB), rows), :] = kv[...]
    kv_wide[pl.ds(pl.multiple_of(core * rows, QB), QB), :] = halo[:QB, :]
    edge = halo[QB:, :].astype(jnp.float32)
    pool_wide[:EDGE, :] = edge
    pool_wide[EDGE : EDGE + rows, :] = pool[...].astype(jnp.float32)
    pool_wide[EDGE + rows :, :] = edge
    lane = lax.broadcasted_iota(jnp.int32, (QB, LANES), 1)
    row = lax.broadcasted_iota(jnp.int32, (2 * QB, 3 * QB), 0) % QB
    column = lax.broadcasted_iota(jnp.int32, (2 * QB, 3 * QB), 1)
    near = (column >= row) & (column <= row + 2 * WINDOW)
    upper = lax.broadcasted_iota(jnp.int32, (2 * QB, 1), 0) < QB
    sinks = jnp.where(upper, sink[0], sink[1])
    half = lax.shift_left(1, group)
    for i in range(rows // (2 * QB)):
        start = pl.multiple_of(core * QB + 2 * QB * i, QB)
        block = first_block + core + 2 * i
        pair = q[pl.ds(start, QB), :]
        zero = jnp.zeros_like(pair)
        lower_head = jnp.where(lane < HEAD, pair, zero)
        upper_head = jnp.concatenate([pair[:, HEAD:], zero[:, HEAD:]], axis=1)
        queries = jnp.concatenate([lower_head, upper_head], axis=0)
        keys = kv_wide[2 * QB * i : 2 * QB * i + 3 * QB, :]
        scores = lax.dot_general(
            queries, keys, (((1,), (1,)), ((), ())), preferred_element_type=jnp.float32
        )
        least = jnp.where(block == 0, QB, 0)
        limit = jnp.where(block == blocks_total - 1, 2 * QB, 3 * QB)
        valid = near & (column >= least) & (column < limit)
        scores = jnp.where(valid, scores, NEG_BIG)
        top = jnp.maximum(jnp.max(scores, axis=-1, keepdims=True), sinks)
        expo = jnp.where(valid, jnp.exp(scores - top), 0.0)
        total = jnp.sum(expo, axis=-1, keepdims=True) + jnp.exp(sinks - top)
        weights = (expo / total).astype(jnp.bfloat16)
        mixed = jnp.dot(weights, keys, preferred_element_type=jnp.float32)
        attended = jnp.concatenate([mixed[:QB, HEAD:], mixed[QB:, HEAD:]], axis=1)
        out[i * QB : (i + 1) * QB, :LANES] = attended.astype(jnp.bfloat16)

        near_rows = pool_wide[pl.ds(start, QB + 2 * EDGE), :]
        size = QB + 2 * EDGE
        sums = near_rows + pltpu.roll(near_rows, 1, 0)
        chosen = sums
        for index in range(1, len(POOL_SPANS)):
            step = POOL_SPANS[index] // 4
            sums = pltpu.roll(sums, step, 0) + pltpu.roll(sums, size - step, 0)
            chosen = jnp.where(group == index, sums, chosen)
        position = block * QB + lax.broadcasted_iota(jnp.int32, (QB, 1), 0)
        counted = jnp.minimum(position + half, blocks_total * QB) - jnp.maximum(position - half, 0)
        mean = chosen[EDGE : EDGE + QB] / counted.astype(jnp.float32)
        pooled = (mean - near_rows[EDGE : EDGE + QB]) * scale[...]
        out[i * QB : (i + 1) * QB, LANES:] = pooled.astype(jnp.bfloat16)


def output_product(joined, columns, out):
    peers, width = joined.shape[0], columns.shape[2]
    for side in range(2):
        total = None
        for i in range(peers):
            weights = jnp.concatenate([columns[side, i], columns[side, peers + i]], axis=1)
            part = lax.dot_general(
                joined[i], weights, (((1,), (1,)), ((), ())), preferred_element_type=jnp.float32
            )
            total = part if total is None else total + part
        out[:, side * width : (side + 1) * width] = total.astype(jnp.bfloat16)


def body(tokens, norm_gain, w_query, w_key, w_value, w_pool_in, sink_logit, pool_scale, w_out):
    rows, depth = tokens.shape
    core, chip, sp_place = lax.axis_index("c"), lax.axis_index("x"), lax.axis_index(SP)
    sp_count = lax.axis_size(SP)
    key_head = chip // (lax.axis_size("x") // (w_key.shape[1] // HEAD))
    bf16 = jnp.bfloat16

    out_piece = swapped(w_out.T)

    small = jnp.concatenate(
        [three_parts(pool_scale), jnp.broadcast_to(three_parts(sink_logit), (3, HEAD))], axis=1
    )
    small = jnp.pad(small, ((0, EDGE - 3), (0, 0)))
    own = jnp.concatenate([jnp.concatenate([w_query, w_pool_in], axis=1), small], axis=0)
    chip_weights = from_everyone(own, "c")
    small = jnp.sum(chip_weights[:, depth : depth + 3].astype(jnp.float32), axis=1)
    scale = small[:, :HEAD].reshape(1, LANES)
    sink = small[:, HEAD]

    cosine, sine = rope_tables(sp_place * rows, rows)
    key_cols = lax.dynamic_slice_in_dim(w_key, key_head * HEAD, HEAD, 1)
    value_cols = lax.dynamic_slice_in_dim(w_value, key_head * HEAD, HEAD, 1)
    both = jnp.concatenate([jnp.concatenate([key_cols, value_cols], axis=1), out_piece], axis=0)
    both, cosine, sine, scale, sink = lax.optimization_barrier((both, cosine, sine, scale, sink))
    exchanged = from_everyone(both, SP)

    whole = lambda *shape: pl.BlockSpec(shape, lambda i: (0,) * len(shape))
    part = lambda *shape: pl.BlockSpec(shape, lambda i: (i,) + (0,) * (len(shape) - 1))
    query, kv, pool_in = pl.pallas_call(
        project,
        grid=(rows // ROWS,),
        in_specs=[
            part(ROWS, depth),
            whole(1, depth),
            whole(*chip_weights.shape),
            whole(*exchanged.shape),
            part(ROWS, LANES),
            part(ROWS, LANES),
        ],
        out_specs=[part(ROWS, LANES)] * 3,
        out_shape=[jax.ShapeDtypeStruct((rows, LANES), bf16)] * 3,
        scratch_shapes=[pltpu.VMEM((depth, 3 * LANES), bf16)],
        name="project",
        interpret=INTERPRET,
    )(tokens, norm_gain[None, :], chip_weights, exchanged, cosine, sine)

    tail = jnp.concatenate([kv[rows - QB :], pool_in[rows - EDGE :]], axis=0)
    head = jnp.concatenate([kv[:QB], pool_in[:EDGE]], axis=0)
    pairs = [(2 * s, 2 * s + 2) for s in range(sp_count - 1)]
    pairs += [(2 * s + 3, 2 * s + 1) for s in range(sp_count - 1)]
    halo = lax.ppermute(jnp.where(core == 0, tail, head), SP + ("c",), pairs)

    out_cols = from_everyone(exchanged[:, key_cols.shape[0] :], "c")
    out_cols = out_cols.reshape(2, lax.axis_size("z"), -1, LANES)

    place = jnp.stack([core, sp_place * (rows // QB), chip]).astype(jnp.int32)
    smem = pl.BlockSpec(memory_space=pltpu.SMEM)
    vmem = pl.BlockSpec(memory_space=pltpu.VMEM)
    local = pl.pallas_call(
        functools.partial(mix, sp_count * (rows // QB)),
        in_specs=[smem, smem] + [vmem] * 5,
        out_specs=vmem,
        out_shape=jax.ShapeDtypeStruct((rows // 2, 2 * LANES), bf16),
        scratch_shapes=[
            pltpu.VMEM((rows + QB, LANES), bf16),
            pltpu.VMEM((rows + 2 * EDGE, LANES), jnp.float32),
        ],
        name="mix",
        interpret=INTERPRET,
    )(place, sink, scale, query, kv, pool_in, halo)

    joined = from_everyone(local, "x")
    partial_cols = pl.pallas_call(
        output_product,
        in_specs=[vmem] * 2,
        out_specs=vmem,
        out_shape=jax.ShapeDtypeStruct((rows // 2, 2 * out_cols.shape[2]), bf16),
        name="output_product",
        interpret=INTERPRET,
    )(joined, out_cols)
    return lax.all_to_all(partial_cols, "x", split_axis=0, concat_axis=1, tiled=True)


def solution(mesh):
    devices = mesh.devices
    mesh = Mesh(devices.reshape(8, devices.size // 64, 4, 2), SP + TP)
    in_specs = (
        P(SP, None),
        P(),
        P(None, TP),
        P(SP, None),
        P(SP, None),
        P(None, TP),
        P(TP),
        P(TP),
        P(TP, SP),
    )
    out_specs = P(SP + TP, None)
    return jax.shard_map(body, mesh=mesh, in_specs=in_specs, out_specs=out_specs, check_vma=False)
```

time: 127 us -> 132 us (1.039)
  blocking collectives: 12.7 us -> 33.6 us
  Pallas kernels: 0 us -> 15.9 us
  matrix products: 12.4 us -> 0 us
  waiting for transfers between devices: 40.2 us -> 28.3 us
  starting transfers between devices: 38.6 us -> 32.3 us
  other arithmetic: 11.9 us -> 6.36 us
  between operations: 1.33 us -> 4.17 us
  local copies, waits for them, and re-layouts: 8.84 us -> 10.7 us
    all_to_all x1 -> x2, blocking collectives: 12.7 us -> 33.6 us  [the longest x1 21.7 us: from_everyone(): lax.all_to_all(jnp.broadcast_to(x[None], (peers, *x.shape)), axis, 0, 0,...]
    pallas_call x0 -> x3, Pallas kernels: none -> 15.9 us  [the longest x1 8.81 us: body(): pl.pallas_call(project, grid=(rows // ROWS,), in_specs=[part(ROWS, depth)...]
    dot_general x20 -> x0, matrix products: 12.4 us -> none  [the longest x1 3.71 us: body(): kv_sum = jnp.dot(normed, kv_cols, preferred_element_type=jnp.float32)]
    all_to_all x2 -> x3, waiting for transfers between devices: 40.2 us -> 28.2 us  [from_everyone(): lax.all_to_all(jnp.broadcast_to(x[None], (peers, *x.shape)), axis, 0, 0,...]
    reduce_sum x10 -> x1, other arithmetic: 8.25 us -> 0.02 us  [body(): jnp.sum(chip_weights[:, depth:depth + 3].astype(jnp.float32), axis=1)]
    ppermute x3 -> x2, starting transfers between devices: 11.5 us -> 6.66 us  [the longest x1 5.37 us: swapped(): return lax.ppermute(piece, SP + TP, pairs)]
    concatenate x1 -> x3, other arithmetic: 0.02 us -> 3.01 us  [the longest x1 1.86 us: rope_tables(): jnp.concatenate([cosine] * 4, axis=1)]
    another operation x1 -> x0, local copies, waits for them, and re-layouts: 2.44 us -> none  [body(): halves = out_cols.reshape(2, count // 2, -1, 2, HEAD)]
  transfers between devices with their start and end apart: 5 -> 5, of which waited for: 2 -> 1; matrix products, arithmetic and copies ran while one was open for 14% -> 8% of each run, Pallas kernels for 0% -> 3%
where the time goes in v2:
time: 132 us; the launch traced here: 131 us
  blocking collectives  33.6 us (25%)
  starting transfers between devices  32.3 us (24%)
  waiting for transfers between devices  28.3 us (21%)
  Pallas kernels  15.9 us (12%)
  local copies, waits for them, and re-layouts  10.7 us (8%)
  other arithmetic  6.36 us (5%)
  between operations  4.17 us (3%)
    all_to_all x3, waiting for transfers between devices, from_everyone(): lax.all_to_all(jnp.broadcast_to(x[None], (peers, *x.shape)), axis, 0, 0,...  28.2 us
    all_to_all x3, starting transfers between devices, from_everyone(): lax.all_to_all(jnp.broadcast_to(x[None], (peers, *x.shape)), axis, 0, 0,...  25.7 us
    all_to_all x1, blocking collectives, from_everyone(): lax.all_to_all(jnp.broadcast_to(x[None], (peers, *x.shape)), axis, 0, 0,...  21.7 us
    all_to_all x1, blocking collectives, body(): lax.all_to_all(partial_cols, 'x', split_axis=0, concat_axis=1, tiled=True)  11.8 us
    pallas_call x1, Pallas kernels, body(): pl.pallas_call(project, grid=(rows // ROWS,), in_specs=[part(ROWS, depth)...  8.81 us
    ppermute x1, starting transfers between devices, swapped(): return lax.ppermute(piece, SP + TP, pairs)  5.37 us
    broadcast_in_dim x4, local copies, waits for them, and re-layouts, from_everyone(): jnp.broadcast_to(x[None], (peers, *x.shape))  4.62 us
    pallas_call x1, Pallas kernels, body(): pl.pallas_call(functools.partial(mix, sp_count * (rows // QB)), in_specs=...  4.01 us
  transfers between devices with their start and end apart: 5, of which 1 were waited for; matrix products, arithmetic and copies ran while one was open for 8% of the time, Pallas kernels for 3%

profile of v2, /device:TPU:1, one launch (start us, length us, event | category | flops | bytes accessed | tf_op | source)
XLA Modules:
  0.0 131.3 jit_solution(8782355557210632200)
XLA Ops:
  0.0 5.4 %collective-permute-start = (bf16[32,128]{1,0:T(8,128)(2,1)}, bf16[32,128]{1,0:T(8,128)(2,1)S(1)}, u32[]{:S(2)}, u32[]{:S(2)}) collective-permute-start(bf16[32,128]{1,0:T(8,128)(2,1)} %bitcast.22), channel_id=1, source_target_pairs={{0,0},{1,64},{2,128},{3,192},{4,256},{5,320},{6,384},{7,448},{8,8}... | collective-permute-start | bytes 24584 | tf_op jit(solution)/shard_map/ppermute | solution.py:38
  9.4 0.7 fusion.3
  10.4 1.1 fusion.1
  11.8 1.1 broadcast_in_dim.13
  12.9 6.4 %all-to-all-start = ((bf16[2,2064,128]{2,1,0:T(8,128)(2,1)}), bf16[2,2064,128]{2,1,0:T(8,128)(2,1)S(1)}, u32[]{:S(2)}, u32[]{:S(2)}) async-start(bf16[2,2064,128]{2,1,0:T(8,128)(2,1)} %broadcast_in_dim.13), calls=%async_computation | async-start | bytes 2113536 | tf_op jit(solution)/shard_map/all_to_all | solution.py:26
  19.3 1.9 %fusion.2 = (f32[1024,32]{1,0:T(8,128)S(1)}, f32[1024,32]{1,0:T(8,128)S(1)}, f32[1024,32]{1,0:T(8,128)S(1)}) fusion(f32[32]{0:T(128)S(1)} %multiply_power_fusion, f32[1024]{0:T(1024)S(1)} %add_convert_fusion), kind=kLoop, calls=%fused_computation.7 | loop fusion | flops 65536 | bytes 397440 | tf_op jit(solution)/shard_map/neg | solution.py:56
  21.3 1.9 %pad_maximum_fusion = (f32[1024,128]{1,0:T(8,128)}, f32[1024,128]{1,0:T(8,128)}) fusion(f32[1024,32]{1,0:T(8,128)S(1)} %get-tuple-element.27, f32[1024,32]{1,0:T(8,128)S(1)} %get-tuple-element.26, f32[1024,32]{1,0:T(8,128)S(1)} %get-tuple-element.25), kind=kLoop, calls=%fused_computation.5 | loop fusion | flops 786432 | bytes 1441792 | tf_op jit(solution)/shard_map/concatenate | solution.py:55
  23.2 0.8 slice_reduce_fusion.sink
  24.8 1.3 broadcast_in_dim.15
  26.0 11.5 %all-to-all-start.1 = ((bf16[64,64,128]{2,1,0:T(8,128)(2,1)}), bf16[64,64,128]{2,1,0:T(8,128)(2,1)S(1)}, u32[]{:S(2)}, u32[]{:S(2)}) async-start(bf16[64,64,128]{2,1,0:T(8,128)(2,1)} %broadcast_in_dim.15), calls=%async_computation.1 | async-start | bytes 2097152 | tf_op jit(solution)/shard_map/all_to_all | solution.py:26
  37.6 28.2 %all-to-all-done.1.ex = bf16[64,64,128]{2,1,0:T(8,128)(2,1)S(1)} async-done(((bf16[64,64,128]{2,1,0:T(8,128)(2,1)}), bf16[64,64,128]{2,1,0:T(8,128)(2,1)S(1)}, u32[]{:S(2)}, u32[]{:S(2)}) %all-to-all-start.1) | async-done | bytes 1048608 | tf_op jit(solution)/shard_map/all_to_all | solution.py:26
  65.8 1.0 copy-done
  66.8 8.8 %project.1 = (bf16[1024,128]{1,0:T(8,128)(2,1)}, bf16[1024,128]{1,0:T(8,128)(2,1)}, bf16[1024,128]{1,0:T(8,128)(2,1)}) custom-call(bf16[1024,2048]{1,0:T(8,128)(2,1)} %tokens.1, f32[1,2048]{1,0:T(1,128)} %bitcast.20, bf16[2,2064,128]{2,1,0:T(8,128)(2,1)} %copy-done.1, bf16[64,64,128]{2,1,0:T(8,128)(2,1)} %copy-done, f32[1024,128]{1,0:T(8,128)} %get-tuple-element.16.cosine, ...), custom_call_target="tpu_custom_call" | custom-call | tf_op jit(solution)/shard_map/project/pallas_call | solution.py:185
  75.6 0.7 fusion.8
  76.4 0.8 fusion.7
  77.2 1.3 collective-permute-start.1
  79.1 1.1 broadcast_in_dim.17
  80.2 7.8 %all-to-all-start.3 = ((bf16[2,64,32,128]{3,2,1,0:T(8,128)(2,1)}), bf16[2,64,32,128]{3,2,1,0:T(8,128)(2,1)S(1)}, u32[]{:S(2)}, u32[]{:S(2)}) async-start(bf16[2,64,32,128]{3,2,1,0:T(8,128)(2,1)} %broadcast_in_dim.17), calls=%async_computation.3 | async-start | bytes 2097152 | tf_op jit(solution)/shard_map/all_to_all | solution.py:26
  88.6 4.0 %mix.1 = bf16[512,256]{1,0:T(8,128)(2,1)} custom-call(s32[3]{0:T(128)} %pad_add_fusion.place, f32[2]{0:T(128)} %slice_reduce_fusion.sink, f32[1,128]{1,0:T(1,128)} %reshape.56.scale, bf16[1024,128]{1,0:T(8,128)(2,1)} %get-tuple-element.18.q, bf16[1024,128]{1,0:T(8,128)(2,1)} %get-tuple-element.19.kv, bf16[1024,128]{1,0:T(8,128)(2,1)} %get-tuple-element.20.pool, ...), custom_call_target="tpu_custom_call" | custom-call | tf_op jit(solution)/shard_map/mix/pallas_call | solution.py:215
  92.6 1.2 broadcast_in_dim.16
  93.8 21.7 %all_to_all.39.joined = bf16[4,512,256]{2,1,0:T(8,128)(2,1)} all-to-all(bf16[4,512,256]{2,1,0:T(8,128)(2,1)S(1)} %broadcast_in_dim.16), channel_id=1, replica_groups=mesh['z'=8,'y'=8,'x'=4,'c'=2] {'x'}, dimensions={0} | all-to-all | bytes 2097152 | tf_op jit(solution)/shard_map/all_to_all | solution.py:26
  115.5 3.1 %output_product.1 = bf16[512,512]{1,0:T(8,128)(2,1)} custom-call(bf16[4,512,256]{2,1,0:T(8,128)(2,1)} %all_to_all.39.joined, bf16[2,8,256,128]{3,2,1,0:T(8,128)(2,1)} %bitcast.17), custom_call_target="tpu_custom_call" | custom-call | tf_op jit(solution)/shard_map/output_product/pallas_call | solution.py:229
  118.6 11.8 %all_to_all.40 = bf16[4,128,512]{2,1,0:T(8,128)(2,1)S(1)} all-to-all(bf16[4,128,512]{2,1,0:T(8,128)(2,1)} %bitcast.18), channel_id=1, replica_groups=mesh['z'=8,'y'=8,'x'=4,'c'=2] {'x'}, dimensions={0} | all-to-all | bytes 1048576 | tf_op jit(solution)/shard_map/all_to_all | solution.py:237
  130.4 0.8 copy.25
  (30 shorter events, 2.7 us)
Async XLA Ops:
  0.0 24.7 %collective-permute-start = (bf16[32,128]{1,0:T(8,128)(2,1)}, bf16[32,128]{1,0:T(8,128)(2,1)S(1)}, u32[]{:S(2)}, u32[]{:S(2)}) collective-permute-start(bf16[32,128]{1,0:T(8,128)(2,1)} %bitcast.22), channel_id=1, source_target_pairs={{0,0},{1,64},{2,128},{3,192},{4,256},{5,320},{6,384},{7,448},{8,8}... | collective-permute-start | bytes 24584 | tf_op jit(solution)/shard_map/ppermute | solution.py:38
  12.9 10.3 %all-to-all-start = ((bf16[2,2064,128]{2,1,0:T(8,128)(2,1)}), bf16[2,2064,128]{2,1,0:T(8,128)(2,1)S(1)}, u32[]{:S(2)}, u32[]{:S(2)}) async-start(bf16[2,2064,128]{2,1,0:T(8,128)(2,1)} %broadcast_in_dim.13), calls=%async_computation | async-start | bytes 2113536 | tf_op jit(solution)/shard_map/all_to_all | solution.py:26
  19.3 2.0 %copy-start.4 = (bf16[32,128]{1,0:T(8,128)(2,1)S(1)}, bf16[32,128]{1,0:T(8,128)(2,1)}, u32[]{:S(2)}) copy-start(bf16[32,128]{1,0:T(8,128)(2,1)} %param.13) | copy-start | bytes 24580
  19.3 2.0 %copy-start.5 = (bf16[32,128]{1,0:T(8,128)(2,1)S(1)}, bf16[32,128]{1,0:T(8,128)(2,1)}, u32[]{:S(2)}) copy-start(bf16[32,128]{1,0:T(8,128)(2,1)} %param.12) | copy-start | bytes 24580
  23.2 2.9 %copy-start.1 = (bf16[2,2064,128]{2,1,0:T(8,128)(2,1)}, bf16[2,2064,128]{2,1,0:T(8,128)(2,1)S(1)}, u32[]{:S(2)}) copy-start(bf16[2,2064,128]{2,1,0:T(8,128)(2,1)S(1)} %all-to-all-done.qp) | copy-start | bytes 3170308
  26.0 39.8 %all-to-all-start.1 = ((bf16[64,64,128]{2,1,0:T(8,128)(2,1)}), bf16[64,64,128]{2,1,0:T(8,128)(2,1)S(1)}, u32[]{:S(2)}, u32[]{:S(2)}) async-start(bf16[64,64,128]{2,1,0:T(8,128)(2,1)} %broadcast_in_dim.15), calls=%async_computation.1 | async-start | bytes 2097152 | tf_op jit(solution)/shard_map/all_to_all | solution.py:26
  65.8 1.0 copy-start
  75.6 3.4 %slice-start = ((bf16[64,64,128]{2,1,0:T(8,128)(2,1)}), bf16[64,32,128]{2,1,0:T(8,128)(2,1)S(1)}, s32[]{:S(2)}) async-start(bf16[64,64,128]{2,1,0:T(8,128)(2,1)} %copy-done), calls=%async_computation.5 | async-start | bytes 1048576 | tf_op jit(solution)/shard_map/slice | solution.py:209
  77.2 10.8 %collective-permute-start.1 = (bf16[144,128]{1,0:T(8,128)(2,1)S(1)}, bf16[144,128]{1,0:T(8,128)(2,1)S(1)}, u32[]{:S(2)}, u32[]{:S(2)}) collective-permute-start(bf16[144,128]{1,0:T(8,128)(2,1)S(1)} %maximum_select_fusion), channel_id=1, source_target_pairs={{0,8},{8,16},{16,24},{24,32},{32,40},{40,48},{48,56},{56,64},{64,7... | collective-permute-start | bytes 110600 | tf_op jit(solution)/shard_map/ppermute | solution.py:207
  80.2 12.4 %all-to-all-start.3 = ((bf16[2,64,32,128]{3,2,1,0:T(8,128)(2,1)}), bf16[2,64,32,128]{3,2,1,0:T(8,128)(2,1)S(1)}, u32[]{:S(2)}, u32[]{:S(2)}) async-start(bf16[2,64,32,128]{3,2,1,0:T(8,128)(2,1)} %broadcast_in_dim.17), calls=%async_computation.3 | async-start | bytes 2097152 | tf_op jit(solution)/shard_map/all_to_all | solution.py:26
  88.0 0.6 copy-start.3
  92.6 22.9 %copy-start.2 = (bf16[2,64,32,128]{3,2,1,0:T(8,128)(2,1)}, bf16[2,64,32,128]{3,2,1,0:T(8,128)(2,1)S(1)}, u32[]{:S(2)}) copy-start(bf16[2,64,32,128]{3,2,1,0:T(8,128)(2,1)S(1)} %all-to-all-done.3) | copy-start | bytes 3145732

commit v3 on v2

--- a/solution.py
+++ b/solution.py
@@ -50,20 +50,26 @@
     inverse = 10000.0 ** (-jnp.arange(half, dtype=jnp.float32) / half)
     positions = (offset + jnp.arange(rows)).astype(jnp.float32)
     angles = positions[:, None] * inverse[None, :]
-    cosine, sine = jnp.cos(angles), jnp.sin(angles)
-    return (
-        jnp.concatenate([cosine] * 4, axis=1),
-        jnp.concatenate([-sine, sine, -sine, sine], axis=1),
-    )
-
-
-def project(tokens, gain, qp, ex, cosine, sine, q_out, kv_out, pool_out, weights):
-    @pl.when(pl.program_id(0) == 0)
+    return jnp.cos(angles), jnp.sin(angles)
+
+
+def project(
+    tokens, gain, own, other, ex, cosine, sine, q_out, kv_out, pool_out, send, weights
+):
+    core = lax.axis_index("c")
+    step = pl.program_id(0)
+    depth = weights.shape[0]
+
+    @pl.when(step == 0)
     def _():
-        depth = weights.shape[0]
-        weights[:, :LANES] = qp[0, :depth]
-        weights[:, LANES : 2 * LANES] = qp[1, :depth]
-        weights[:, 2 * LANES :] = ex[:, : ex.shape[1] // 2].reshape(depth, LANES)
+        weights[:, 2 * LANES :] = ex[...].reshape(depth, LANES)
+
+    for place in range(2):
+
+        @pl.when((step == 0) & (core == place))
+        def _():
+            weights[:, place * LANES : (place + 1) * LANES] = own[:depth]
+            weights[:, (1 - place) * LANES : (2 - place) * LANES] = other[:depth]
 
     values = tokens[...].astype(jnp.float32)
     center = jnp.mean(values, axis=-1, keepdims=True)
@@ -77,18 +83,40 @@
     lane = lax.broadcasted_iota(jnp.int32, (ROWS, LANES), 1)
     first = lane % HEAD < HEAD // 2
 
+    wide_cosine = jnp.concatenate([cosine[...]] * 4, axis=1)
+    wide_sine = jnp.concatenate([-sine[...], sine[...]] * 2, axis=1)
+
     def turned(x):
         other = jnp.where(first, pltpu.roll(x, LANES - HEAD // 2, 1), pltpu.roll(x, HEAD // 2, 1))
-        return x * cosine[...] + other * sine[...]
-
+        return x * wide_cosine + other * wide_sine
+
+    kv = jnp.where(lane < HEAD, turned(kv), kv).astype(jnp.bfloat16)
+    pool = pool.astype(jnp.bfloat16)
     q_out[...] = (turned(query) * HEAD ** (-0.5)).astype(jnp.bfloat16)
-    kv_out[...] = jnp.where(lane < HEAD, turned(kv), kv).astype(jnp.bfloat16)
-    pool_out[...] = pool.astype(jnp.bfloat16)
-
-
-def mix(blocks_total, place, sink, scale, q, kv, pool, halo, out, kv_wide, pool_wide):
-    core, first_block, group = place[0], place[1], place[2]
+    kv_out[...] = kv
+    pool_out[...] = pool
+
+    @pl.when((step == 0) & (core == 1))
+    def _():
+        send[:QB] = kv[:QB]
+        send[QB:] = pool[:EDGE]
+
+    @pl.when((step == pl.num_programs(0) - 1) & (core == 0))
+    def _():
+        send[:QB] = kv[ROWS - QB :]
+        send[QB:] = pool[ROWS - EDGE :]
+
+
+def mix(own, other, q, kv, pool, halo, out, kv_wide, pool_wide):
+    core, group = lax.axis_index("c"), lax.axis_index("x")
     rows = q.shape[0]
+    blocks_total = lax.axis_size(SP) * (rows // QB)
+    first_block = lax.axis_index(SP) * (rows // QB)
+    mine = jnp.sum(own[:3].astype(jnp.float32), axis=0, keepdims=True)
+    theirs = jnp.sum(other[:3].astype(jnp.float32), axis=0, keepdims=True)
+    first = jnp.where(core == 0, mine, theirs)
+    second = jnp.where(core == 0, theirs, mine)
+    scale = jnp.concatenate([first[:, :HEAD], second[:, :HEAD]], axis=1)
     kv_wide[pl.ds(pl.multiple_of((1 - core) * QB, QB), rows), :] = kv[...]
     kv_wide[pl.ds(pl.multiple_of(core * rows, QB), QB), :] = halo[:QB, :]
     edge = halo[QB:, :].astype(jnp.float32)
@@ -100,7 +128,7 @@
     column = lax.broadcasted_iota(jnp.int32, (2 * QB, 3 * QB), 1)
     near = (column >= row) & (column <= row + 2 * WINDOW)
     upper = lax.broadcasted_iota(jnp.int32, (2 * QB, 1), 0) < QB
-    sinks = jnp.where(upper, sink[0], sink[1])
+    sinks = jnp.where(upper, first[:, HEAD : HEAD + 1], second[:, HEAD : HEAD + 1])
     half = lax.shift_left(1, group)
     for i in range(rows // (2 * QB)):
         start = pl.multiple_of(core * QB + 2 * QB * i, QB)
@@ -124,7 +152,6 @@
         weights = (expo / total).astype(jnp.bfloat16)
         mixed = jnp.dot(weights, keys, preferred_element_type=jnp.float32)
         attended = jnp.concatenate([mixed[:QB, HEAD:], mixed[QB:, HEAD:]], axis=1)
-        out[i * QB : (i + 1) * QB, :LANES] = attended.astype(jnp.bfloat16)
 
         near_rows = pool_wide[pl.ds(start, QB + 2 * EDGE), :]
         size = QB + 2 * EDGE
@@ -137,28 +164,36 @@
         position = block * QB + lax.broadcasted_iota(jnp.int32, (QB, 1), 0)
         counted = jnp.minimum(position + half, blocks_total * QB) - jnp.maximum(position - half, 0)
         mean = chosen[EDGE : EDGE + QB] / counted.astype(jnp.float32)
-        pooled = (mean - near_rows[EDGE : EDGE + QB]) * scale[...]
-        out[i * QB : (i + 1) * QB, LANES:] = pooled.astype(jnp.bfloat16)
-
-
-def output_product(joined, columns, out):
-    peers, width = joined.shape[0], columns.shape[2]
-    for side in range(2):
+        pooled = (mean - near_rows[EDGE : EDGE + QB]) * scale
+        both = jnp.concatenate([attended, pooled], axis=1).astype(jnp.bfloat16)
+        for peer in range(out.shape[0]):
+            out[peer, i * QB : (i + 1) * QB] = both
+
+
+def output_product(joined, own, other, out):
+    core = lax.axis_index("c")
+    peers = joined.shape[0]
+
+    def product(columns):
+        columns = columns.reshape(2 * peers, -1, LANES)
         total = None
         for i in range(peers):
-            weights = jnp.concatenate([columns[side, i], columns[side, peers + i]], axis=1)
+            weights = jnp.concatenate([columns[i], columns[peers + i]], axis=1)
             part = lax.dot_general(
                 joined[i], weights, (((1,), (1,)), ((), ())), preferred_element_type=jnp.float32
             )
             total = part if total is None else total + part
-        out[:, side * width : (side + 1) * width] = total.astype(jnp.bfloat16)
+        return total.astype(jnp.bfloat16)
+
+    mine, theirs = product(own[...]), product(other[...])
+    out[...] = jnp.concatenate(
+        [jnp.where(core == 0, mine, theirs), jnp.where(core == 0, theirs, mine)], axis=1
+    )
 
 
 def body(tokens, norm_gain, w_query, w_key, w_value, w_pool_in, sink_logit, pool_scale, w_out):
     rows, depth = tokens.shape
-    core, chip, sp_place = lax.axis_index("c"), lax.axis_index("x"), lax.axis_index(SP)
     sp_count = lax.axis_size(SP)
-    key_head = chip // (lax.axis_size("x") // (w_key.shape[1] // HEAD))
     bf16 = jnp.bfloat16
 
     out_piece = swapped(w_out.T)
@@ -168,72 +203,81 @@
     )
     small = jnp.pad(small, ((0, EDGE - 3), (0, 0)))
     own = jnp.concatenate([jnp.concatenate([w_query, w_pool_in], axis=1), small], axis=0)
-    chip_weights = from_everyone(own, "c")
-    small = jnp.sum(chip_weights[:, depth : depth + 3].astype(jnp.float32), axis=1)
-    scale = small[:, :HEAD].reshape(1, LANES)
-    sink = small[:, HEAD]
-
-    cosine, sine = rope_tables(sp_place * rows, rows)
+    other = lax.ppermute(own, "c", [(0, 1), (1, 0)])
+
+    cosine, sine = rope_tables(lax.axis_index(SP) * rows, rows)
+    key_head = lax.axis_index("x") // (lax.axis_size("x") // (w_key.shape[1] // HEAD))
     key_cols = lax.dynamic_slice_in_dim(w_key, key_head * HEAD, HEAD, 1)
     value_cols = lax.dynamic_slice_in_dim(w_value, key_head * HEAD, HEAD, 1)
     both = jnp.concatenate([jnp.concatenate([key_cols, value_cols], axis=1), out_piece], axis=0)
-    both, cosine, sine, scale, sink = lax.optimization_barrier((both, cosine, sine, scale, sink))
+    both, cosine, sine, own, other = lax.optimization_barrier((both, cosine, sine, own, other))
     exchanged = from_everyone(both, SP)
-
+    peers, pieces = exchanged.shape[0], key_cols.shape[0]
+
+    at = lambda *shape: lambda *place: pl.BlockSpec(shape, lambda i: place)
     whole = lambda *shape: pl.BlockSpec(shape, lambda i: (0,) * len(shape))
     part = lambda *shape: pl.BlockSpec(shape, lambda i: (i,) + (0,) * (len(shape) - 1))
-    query, kv, pool_in = pl.pallas_call(
+    query, kv, pool_in, send = pl.pallas_call(
         project,
         grid=(rows // ROWS,),
         in_specs=[
             part(ROWS, depth),
             whole(1, depth),
-            whole(*chip_weights.shape),
-            whole(*exchanged.shape),
-            part(ROWS, LANES),
-            part(ROWS, LANES),
+            whole(*own.shape),
+            whole(*own.shape),
+            whole(peers, pieces, LANES),
+            part(ROWS, HEAD // 2),
+            part(ROWS, HEAD // 2),
         ],
-        out_specs=[part(ROWS, LANES)] * 3,
-        out_shape=[jax.ShapeDtypeStruct((rows, LANES), bf16)] * 3,
+        out_specs=[part(ROWS, LANES)] * 3 + [whole(QB + EDGE, LANES)],
+        out_shape=[jax.ShapeDtypeStruct((rows, LANES), bf16)] * 3
+        + [jax.ShapeDtypeStruct((QB + EDGE, LANES), bf16)],
         scratch_shapes=[pltpu.VMEM((depth, 3 * LANES), bf16)],
         name="project",
         interpret=INTERPRET,
-    )(tokens, norm_gain[None, :], chip_weights, exchanged, cosine, sine)
-
-    tail = jnp.concatenate([kv[rows - QB :], pool_in[rows - EDGE :]], axis=0)
-    head = jnp.concatenate([kv[:QB], pool_in[:EDGE]], axis=0)
+    )(tokens, norm_gain[None, :], own, other, exchanged, cosine, sine)
+
     pairs = [(2 * s, 2 * s + 2) for s in range(sp_count - 1)]
     pairs += [(2 * s + 3, 2 * s + 1) for s in range(sp_count - 1)]
-    halo = lax.ppermute(jnp.where(core == 0, tail, head), SP + ("c",), pairs)
-
-    out_cols = from_everyone(exchanged[:, key_cols.shape[0] :], "c")
-    out_cols = out_cols.reshape(2, lax.axis_size("z"), -1, LANES)
-
-    place = jnp.stack([core, sp_place * (rows // QB), chip]).astype(jnp.int32)
-    smem = pl.BlockSpec(memory_space=pltpu.SMEM)
-    vmem = pl.BlockSpec(memory_space=pltpu.VMEM)
+    halo = lax.ppermute(send, SP + ("c",), pairs)
+
+    own_cols = exchanged[:, pieces:]
+    other_cols = lax.ppermute(own_cols, "c", [(0, 1), (1, 0)])
+
+    peers_x = lax.axis_size("x")
+    small_rows = at(EDGE, LANES)(depth // EDGE, 0)
     local = pl.pallas_call(
-        functools.partial(mix, sp_count * (rows // QB)),
-        in_specs=[smem, smem] + [vmem] * 5,
-        out_specs=vmem,
-        out_shape=jax.ShapeDtypeStruct((rows // 2, 2 * LANES), bf16),
+        mix,
+        grid=(1,),
+        in_specs=[small_rows, small_rows]
+        + [whole(rows, LANES)] * 3
+        + [whole(QB + EDGE, LANES)],
+        out_specs=whole(peers_x, rows // 2, 2 * LANES),
+        out_shape=jax.ShapeDtypeStruct((peers_x, rows // 2, 2 * LANES), bf16),
         scratch_shapes=[
             pltpu.VMEM((rows + QB, LANES), bf16),
             pltpu.VMEM((rows + 2 * EDGE, LANES), jnp.float32),
         ],
         name="mix",
         interpret=INTERPRET,
-    )(place, sink, scale, query, kv, pool_in, halo)
-
-    joined = from_everyone(local, "x")
+    )(own, other, query, kv, pool_in, halo)
+
+    local, other_cols, own_cols = lax.optimization_barrier((local, other_cols, own_cols))
+    joined = lax.all_to_all(local, "x", 0, 0, tiled=True)
+    width = 2 * own_cols.shape[0] // lax.axis_size("z") * own_cols.shape[1]
     partial_cols = pl.pallas_call(
         output_product,
-        in_specs=[vmem] * 2,
-        out_specs=vmem,
-        out_shape=jax.ShapeDtypeStruct((rows // 2, 2 * out_cols.shape[2]), bf16),
+        grid=(peers_x,),
+        in_specs=[
+            pl.BlockSpec((peers_x, QB, 2 * LANES), lambda i: (0, i, 0)),
+            whole(*own_cols.shape),
+            whole(*own_cols.shape),
+        ],
+        out_specs=part(QB, width),
+        out_shape=jax.ShapeDtypeStruct((rows // 2, width), bf16),
         name="output_product",
         interpret=INTERPRET,
-    )(joined, out_cols)
+    )(joined, own_cols, other_cols)
     return lax.all_to_all(partial_cols, "x", split_axis=0, concat_axis=1, tiled=True)
 
 

time: 132 us -> 126 us (0.955); the launches traced: 131 us -> 124 us
  blocking collectives: 33.6 us -> 72.8 us
  waiting for transfers between devices: 28.3 us -> 3.62 us
  starting transfers between devices: 32.3 us -> 16 us
  local copies, waits for them, and re-layouts: 10.7 us -> 4.37 us
  Pallas kernels: 15.9 us -> 18.3 us
  other arithmetic: 6.36 us -> 4.25 us
    all_to_all x3 -> x0, waiting for transfers between devices: 28.2 us -> none  [from_everyone(): lax.all_to_all(jnp.broadcast_to(x[None], (peers, *x.shape)), axis, 0, 0,...]
    all_to_all x3 -> x0, starting transfers between devices: 25.7 us -> none  [from_everyone(): lax.all_to_all(jnp.broadcast_to(x[None], (peers, *x.shape)), axis, 0, 0,...]
    all_to_all x0 -> x1, blocking collectives: none -> 22 us  [body(): joined = lax.all_to_all(local, 'x', 0, 0, tiled=True)]
    all_to_all x1, blocking collectives: 21.7 us -> 39.1 us  [from_everyone(): lax.all_to_all(jnp.broadcast_to(x[None], (peers, *x.shape)), axis, 0, 0,...]
    ppermute x1 -> x3, starting transfers between devices: 1.29 us -> 10.7 us  [the longest x1 4.72 us: body(): other = lax.ppermute(own, 'c', [(0, 1), (1, 0)])]
    broadcast_in_dim x4 -> x1, local copies, waits for them, and re-layouts: 4.62 us -> 0.25 us  [from_everyone(): jnp.broadcast_to(x[None], (peers, *x.shape))]
    ppermute x1 -> x3, waiting for transfers between devices: 0.01 us -> 3.62 us  [the longest x1 3.61 us: body(): halo = lax.ppermute(send, SP + ('c',), pairs)]
    sin x0 -> x1, other arithmetic: none -> 3.05 us  [rope_tables(): return (jnp.cos(angles), jnp.sin(angles))]
  transfers between devices with their start and end apart: 5 -> 4, of which waited for: 1 -> 1; matrix products, arithmetic and copies ran while one was open for 8% -> 6% of each run, Pallas kernels for 3% -> 11%
where the time goes in v3:
time: 126 us; the launch traced here: 124 us
  blocking collectives  72.8 us (58%)
  Pallas kernels  18.3 us (15%)
  starting transfers between devices  16 us (13%)
  between operations  4.44 us (4%)
  local copies, waits for them, and re-layouts  4.37 us (3%)
  other arithmetic  4.25 us (3%)
  waiting for transfers between devices  3.62 us (3%)
    all_to_all x1, blocking collectives, from_everyone(): lax.all_to_all(jnp.broadcast_to(x[None], (peers, *x.shape)), axis, 0, 0,...  39.1 us
    all_to_all x1, blocking collectives, body(): joined = lax.all_to_all(local, 'x', 0, 0, tiled=True)  22 us
    all_to_all x1, blocking collectives, body(): lax.all_to_all(partial_cols, 'x', split_axis=0, concat_axis=1, tiled=True)  11.8 us
    pallas_call x1, Pallas kernels, body(): pl.pallas_call(project, grid=(rows // ROWS,), in_specs=[part(ROWS, depth)...  8.74 us
    ppermute x1, starting transfers between devices, swapped(): return lax.ppermute(piece, SP + TP, pairs)  5.37 us
    pallas_call x1, Pallas kernels, body(): pl.pallas_call(mix, grid=(1,), in_specs=[small_rows, small_rows] + [whole...  5.07 us
    ppermute x1, starting transfers between devices, body(): other = lax.ppermute(own, 'c', [(0, 1), (1, 0)])  4.72 us
    ppermute x1, starting transfers between devices, body(): other_cols = lax.ppermute(own_cols, 'c', [(0, 1), (1, 0)])  4.64 us
  transfers between devices with their start and end apart: 4, of which 1 were waited for; matrix products, arithmetic and copies ran while one was open for 6% of the time, Pallas kernels for 11%

profile of v3, /device:TPU:1, one launch (start us, length us, event | category | flops | bytes accessed | tf_op | source)
XLA Modules:
  0.0 123.9 jit_solution(17402336778632182487)
XLA Ops:
  0.0 5.4 %collective-permute-start = (bf16[32,128]{1,0:T(8,128)(2,1)}, bf16[32,128]{1,0:T(8,128)(2,1)S(1)}, u32[]{:S(2)}, u32[]{:S(2)}) collective-permute-start(bf16[32,128]{1,0:T(8,128)(2,1)} %bitcast.15), channel_id=1, source_target_pairs={{0,0},{1,64},{2,128},{3,192},{4,256},{5,320},{6,384},{7,448},{8,8}... | collective-permute-start | bytes 24584 | tf_op jit(solution)/shard_map/ppermute | solution.py:38
  9.7 0.7 fusion.7
  10.3 1.2 copy.10
  11.5 1.2 copy.11
  12.8 0.1 pad_maximum_fusion.2
  12.9 0.1 broadcast_in_dim.6
  12.9 0.1 fusion.6
  13.0 0.3 pad_maximum_fusion.own
  13.3 4.7 %collective-permute-start.1 = (bf16[2064,128]{1,0:T(8,128)(2,1)S(1)}, bf16[2064,128]{1,0:T(8,128)(2,1)S(1)}, u32[]{:S(2)}, u32[]{:S(2)}) collective-permute-start(bf16[2064,128]{1,0:T(8,128)(2,1)S(1)} %pad_maximum_fusion.own), channel_id=1, source_target_pairs={{0,1},{1,0},{2,3},{3,2},{4,5},{5,4},{6,7},{7,6},{8,9},{9,8},{10,11... | collective-permute-start | bytes 1585160 | tf_op jit(solution)/shard_map/ppermute | solution.py:206
  18.1 3.0 %multiply_sine_fusion = (f32[1024,32]{1,0:T(8,128)}, f32[1024,32]{1,0:T(8,128)}) fusion(f32[32]{0:T(128)S(1)} %multiply_power_fusion, f32[1024]{0:T(1024)S(1)} %add_convert_fusion), kind=kLoop, calls=%fused_computation | loop fusion | flops 32768 | bytes 266368 | tf_op jit(solution)/shard_map/sin | solution.py:53
  21.2 0.1 constant_dynamic-slice_fusion
  21.2 0.1 pad_maximum_fusion.1
  21.3 0.2 broadcast_in_dim.8
  21.6 39.1 %all_to_all.29.ex = bf16[64,64,128]{2,1,0:T(8,128)(2,1)S(1)} all-to-all(bf16[64,64,128]{2,1,0:T(8,128)(2,1)S(1)} %broadcast_in_dim.8), channel_id=1, replica_groups=mesh['z'=8,'y'=8,'x'=4,'c'=2] {'z','y'}, dimensions={0} | all-to-all | bytes 2097152 | tf_op jit(solution)/shard_map/all_to_all | solution.py:26
  60.8 4.6 %collective-permute-start.3 = (bf16[64,32,128]{2,1,0:T(8,128)(2,1)S(1)}, bf16[64,32,128]{2,1,0:T(8,128)(2,1)S(1)}, u32[]{:S(2)}, u32[]{:S(2)}) collective-permute-start(bf16[64,32,128]{2,1,0:T(8,128)(2,1)S(1)} %slice.4.own), channel_id=1, source_target_pairs={{0,1},{1,0},{2,3},{3,2},{4,5},{5,4},{6,7},{7,6},{8,9},{9,8},{10,11... | collective-permute-start | bytes 1572872 | tf_op jit(solution)/shard_map/ppermute | solution.py:245
  65.4 8.7 %project.1 = (bf16[1024,128]{1,0:T(8,128)(2,1)}, bf16[1024,128]{1,0:T(8,128)(2,1)}, bf16[1024,128]{1,0:T(8,128)(2,1)}, bf16[144,128]{1,0:T(8,128)(2,1)}) custom-call(bf16[1024,2048]{1,0:T(8,128)(2,1)} %tokens.1, f32[1,2048]{1,0:T(1,128)} %bitcast.14, bf16[2064,128]{1,0:T(8,128)(2,1)} %copy-done.1, bf16[2064,128]{1,0:T(8,128)(2,1)} %copy-done.2, ...), custom_call_target="tpu_custom_call" | custom-call | tf_op jit(solution)/shard_map/project/pallas_call | solution.py:220
  74.2 1.3 %collective-permute-start.2 = (bf16[144,128]{1,0:T(8,128)(2,1)}, bf16[144,128]{1,0:T(8,128)(2,1)S(1)}, u32[]{:S(2)}, u32[]{:S(2)}) collective-permute-start(bf16[144,128]{1,0:T(8,128)(2,1)} %get-tuple-element.25), channel_id=1, source_target_pairs={{0,8},{8,16},{16,24},{24,32},{32,40},{40,48},{48,56},{56,64},{64,7... | collective-permute-start | bytes 110600 | tf_op jit(solution)/shard_map/ppermute | solution.py:242
  75.5 3.6 %collective-permute-done.2.halo = bf16[144,128]{1,0:T(8,128)(2,1)S(1)} collective-permute-done((bf16[144,128]{1,0:T(8,128)(2,1)}, bf16[144,128]{1,0:T(8,128)(2,1)S(1)}, u32[]{:S(2)}, u32[]{:S(2)}) %collective-permute-start.2) | collective-permute-done | bytes 36896 | tf_op jit(solution)/shard_map/ppermute | solution.py:242
  79.1 0.6 copy-done.5
  79.7 5.1 %mix.1 = bf16[4,512,256]{2,1,0:T(8,128)(2,1)} custom-call(bf16[2064,128]{1,0:T(8,128)(2,1)} %copy-done.1, bf16[2064,128]{1,0:T(8,128)(2,1)} %copy-done.2, bf16[1024,128]{1,0:T(8,128)(2,1)} %get-tuple-element.22.q, bf16[1024,128]{1,0:T(8,128)(2,1)} %get-tuple-element.23.kv, bf16[1024,128]{1,0:T(8,128)(2,1)} %get-tuple-element.24.pool, bf16[144,128]{1,0:T(8,128)(2,1)} %copy-done.5), custom_call_target="tpu_custom_call" | custom-call | tf_op jit(solution)/shard_map/mix/pallas_call | solution.py:249
  84.8 22.0 %all_to_all.30.joined = bf16[4,512,256]{2,1,0:T(8,128)(2,1)} all-to-all(bf16[4,512,256]{2,1,0:T(8,128)(2,1)} %mix.1), channel_id=1, replica_groups=mesh['z'=8,'y'=8,'x'=4,'c'=2] {'x'}, dimensions={0} | all-to-all | bytes 2097152 | tf_op jit(solution)/shard_map/all_to_all | solution.py:266
  106.7 4.5 %output_product.1 = bf16[512,512]{1,0:T(8,128)(2,1)} custom-call(bf16[4,512,256]{2,1,0:T(8,128)(2,1)} %all_to_all.30.joined, bf16[64,32,128]{2,1,0:T(8,128)(2,1)} %copy-done.3, bf16[64,32,128]{2,1,0:T(8,128)(2,1)} %copy-done.4), custom_call_target="tpu_custom_call" | custom-call | tf_op jit(solution)/shard_map/output_product/pallas_call | solution.py:268
  111.3 11.8 %all_to_all.31 = bf16[4,128,512]{2,1,0:T(8,128)(2,1)S(1)} all-to-all(bf16[4,128,512]{2,1,0:T(8,128)(2,1)} %bitcast.12), channel_id=1, replica_groups=mesh['z'=8,'y'=8,'x'=4,'c'=2] {'x'}, dimensions={0} | all-to-all | bytes 1048576 | tf_op jit(solution)/shard_map/all_to_all | solution.py:281
  123.0 0.8 copy.13
  (21 shorter events, 0.1 us)
Async XLA Ops:
  0.0 21.2 %collective-permute-start = (bf16[32,128]{1,0:T(8,128)(2,1)}, bf16[32,128]{1,0:T(8,128)(2,1)S(1)}, u32[]{:S(2)}, u32[]{:S(2)}) collective-permute-start(bf16[32,128]{1,0:T(8,128)(2,1)} %bitcast.15), channel_id=1, source_target_pairs={{0,0},{1,64},{2,128},{3,192},{4,256},{5,320},{6,384},{7,448},{8,8}... | collective-permute-start | bytes 24584 | tf_op jit(solution)/shard_map/ppermute | solution.py:38
  13.0 8.1 %copy-start.6 = (bf16[32,128]{1,0:T(8,128)(2,1)S(1)}, bf16[32,128]{1,0:T(8,128)(2,1)}, u32[]{:S(2)}) copy-start(bf16[32,128]{1,0:T(8,128)(2,1)} %param.13) | copy-start | bytes 24580
  13.0 8.1 %copy-start.7 = (bf16[32,128]{1,0:T(8,128)(2,1)S(1)}, bf16[32,128]{1,0:T(8,128)(2,1)}, u32[]{:S(2)}) copy-start(bf16[32,128]{1,0:T(8,128)(2,1)} %param.12) | copy-start | bytes 24580
  13.3 8.3 %copy-start.1 = (bf16[2064,128]{1,0:T(8,128)(2,1)}, bf16[2064,128]{1,0:T(8,128)(2,1)S(1)}, u32[]{:S(2)}) copy-start(bf16[2064,128]{1,0:T(8,128)(2,1)S(1)} %pad_maximum_fusion.own) | copy-start | bytes 1585156
  13.3 8.0 %collective-permute-start.1 = (bf16[2064,128]{1,0:T(8,128)(2,1)S(1)}, bf16[2064,128]{1,0:T(8,128)(2,1)S(1)}, u32[]{:S(2)}, u32[]{:S(2)}) collective-permute-start(bf16[2064,128]{1,0:T(8,128)(2,1)S(1)} %pad_maximum_fusion.own), channel_id=1, source_target_pairs={{0,1},{1,0},{2,3},{3,2},{4,5},{5,4},{6,7},{7,6},{8,9},{9,8},{10,11... | collective-permute-start | bytes 1585160 | tf_op jit(solution)/shard_map/ppermute | solution.py:206
  21.3 39.4 %copy-start.2 = (bf16[2064,128]{1,0:T(8,128)(2,1)}, bf16[2064,128]{1,0:T(8,128)(2,1)S(1)}, u32[]{:S(2)}) copy-start(bf16[2064,128]{1,0:T(8,128)(2,1)S(1)} %collective-permute-done.1.other) | copy-start | bytes 1585156
  60.7 4.7 %copy-start = (bf16[64,64,128]{2,1,0:T(8,128)(2,1)}, bf16[64,64,128]{2,1,0:T(8,128)(2,1)S(1)}, u32[]{:S(2)}) copy-start(bf16[64,64,128]{2,1,0:T(8,128)(2,1)S(1)} %all_to_all.29.ex) | copy-start | bytes 3145732
  60.7 13.4 %copy-start.3 = (bf16[64,32,128]{2,1,0:T(8,128)(2,1)}, bf16[64,32,128]{2,1,0:T(8,128)(2,1)S(1)}, u32[]{:S(2)}) copy-start(bf16[64,32,128]{2,1,0:T(8,128)(2,1)S(1)} %slice.4.own) | copy-start | bytes 1572868
  60.8 24.0 %collective-permute-start.3 = (bf16[64,32,128]{2,1,0:T(8,128)(2,1)S(1)}, bf16[64,32,128]{2,1,0:T(8,128)(2,1)S(1)}, u32[]{:S(2)}, u32[]{:S(2)}) collective-permute-start(bf16[64,32,128]{2,1,0:T(8,128)(2,1)S(1)} %slice.4.own), channel_id=1, source_target_pairs={{0,1},{1,0},{2,3},{3,2},{4,5},{5,4},{6,7},{7,6},{8,9},{9,8},{10,11... | collective-permute-start | bytes 1572872 | tf_op jit(solution)/shard_map/ppermute | solution.py:245
  74.2 4.9 %collective-permute-start.2 = (bf16[144,128]{1,0:T(8,128)(2,1)}, bf16[144,128]{1,0:T(8,128)(2,1)S(1)}, u32[]{:S(2)}, u32[]{:S(2)}) collective-permute-start(bf16[144,128]{1,0:T(8,128)(2,1)} %get-tuple-element.25), channel_id=1, source_target_pairs={{0,8},{8,16},{16,24},{24,32},{32,40},{40,48},{48,56},{56,64},{64,7... | collective-permute-start | bytes 110600 | tf_op jit(solution)/shard_map/ppermute | solution.py:242
  79.1 0.6 copy-start.5
  84.8 22.0 %copy-start.4 = (bf16[64,32,128]{2,1,0:T(8,128)(2,1)}, bf16[64,32,128]{2,1,0:T(8,128)(2,1)S(1)}, u32[]{:S(2)}) copy-start(bf16[64,32,128]{2,1,0:T(8,128)(2,1)S(1)} %collective-permute-done.3.other) | copy-start | bytes 1572868

commit v4 on v3

v4 whole, which is shorter than its diff:
```python
import functools

import jax
import jax.numpy as jnp
from jax import lax
from jax.experimental import pallas as pl
from jax.experimental.pallas import tpu as pltpu
from jax.sharding import Mesh
from jax.sharding import PartitionSpec as P

HEAD = 64
WINDOW = 128
QB = 128
LANES = 128
ROWS = 256
EDGE = 16
POOL_SPANS = (2, 4, 8, 16)
NEG_BIG = -1e30
SP = ("z", "y")
TP = ("x", "c")
INTERPRET = False


def from_everyone(x, axis):
    peers = lax.axis_size(axis)
    return lax.all_to_all(jnp.broadcast_to(x[None], (peers, *x.shape)), axis, 0, 0, tiled=True)


def swapped(piece):
    side, depth = lax.axis_size("z"), lax.axis_size("y")
    place = lambda z, y, t: (z * depth + y) * side + t
    pairs = [
        (place(z, y, t), place(t, y, z))
        for z in range(side)
        for y in range(depth)
        for t in range(side)
    ]
    return lax.ppermute(piece, SP + TP, pairs)


def three_parts(x):
    high = lax.reduce_precision(x, 8, 7)
    middle = lax.reduce_precision(x - high, 8, 7)
    low = x - high - middle
    return jnp.concatenate([high, middle, low], axis=0).astype(jnp.bfloat16)


def rope_tables(offset, rows):
    half = HEAD // 2
    inverse = 10000.0 ** (-jnp.arange(half, dtype=jnp.float32) / half)
    positions = (offset + jnp.arange(rows)).astype(jnp.float32)
    angles = positions[None, :] * inverse[:, None]
    return jnp.cos(angles), jnp.sin(angles)


def turned(x, cosine, sine):
    lane = lax.broadcasted_iota(jnp.int32, x.shape, 1)
    wide_cosine = jnp.concatenate([cosine] * 4, axis=0).T
    wide_sine = jnp.concatenate([-sine, sine] * 2, axis=0).T
    half = HEAD // 2
    other = jnp.where(lane % HEAD < half, pltpu.roll(x, LANES - half, 1), pltpu.roll(x, half, 1))
    return x * wide_cosine + other * wide_sine


def project(tokens, gain, own, other, cosine, sine, normed_out, q_out, pool_out, weights):
    core = lax.axis_index("c")
    for place in range(2):

        @pl.when((pl.program_id(0) == 0) & (core == place))
        def _():
            for source, head in ((own, place), (other, 1 - place)):
                weights[head * HEAD : (head + 1) * HEAD] = source[:HEAD]
                weights[LANES + head * HEAD : LANES + (head + 1) * HEAD] = source[HEAD:LANES]

    values = tokens[...].astype(jnp.float32)
    center = jnp.mean(values, axis=-1, keepdims=True)
    values = values - center
    spread = jnp.mean(values * values, axis=-1, keepdims=True)
    normed = (values * lax.rsqrt(spread + 1e-06) * gain[...]).astype(jnp.bfloat16)
    normed_out[...] = normed
    sums = lax.dot_general(
        normed, weights[...], (((1,), (1,)), ((), ())), preferred_element_type=jnp.float32
    )
    query = turned(sums[:, :LANES], cosine[...], sine[...])
    q_out[...] = (query * HEAD ** (-0.5)).astype(jnp.bfloat16)
    pool_out[...] = sums[:, LANES:].astype(jnp.bfloat16)


def project_kv(normed, pool, ex, cosine, sine, kv_out, send):
    core = lax.axis_index("c")
    step = pl.program_id(0)
    rows = normed.shape[0]
    sums = jnp.dot(
        normed[...], ex[...].reshape(-1, LANES), preferred_element_type=jnp.float32
    )
    lane = lax.broadcasted_iota(jnp.int32, sums.shape, 1)
    kv = jnp.where(lane < HEAD, turned(sums, cosine[...], sine[...]), sums).astype(jnp.bfloat16)
    kv_out[...] = kv

    @pl.when((step == 0) & (core == 1))
    def _():
        send[:QB] = kv[:QB]
        send[QB:] = pool[:EDGE]

    @pl.when((step == pl.num_programs(0) - 1) & (core == 0))
    def _():
        send[:QB] = kv[rows - QB :]
        send[QB:] = pool[rows - EDGE :]


def mix(own, other, q, kv, pool, halo, out, kv_wide, pool_wide):
    core, group = lax.axis_index("c"), lax.axis_index("x")
    i = pl.program_id(0)
    rows = q.shape[0]
    blocks_total = lax.axis_size(SP) * (rows // QB)
    first_block = lax.axis_index(SP) * (rows // QB)
    mine = jnp.sum(own[:3, :LANES].astype(jnp.float32), axis=0, keepdims=True)
    theirs = jnp.sum(other[:3, :LANES].astype(jnp.float32), axis=0, keepdims=True)
    first = jnp.where(core == 0, mine, theirs)
    second = jnp.where(core == 0, theirs, mine)
    scale = jnp.concatenate([first[:, :HEAD], second[:, :HEAD]], axis=1)

    @pl.when(i == 0)
    def _():
        kv_wide[pl.ds(pl.multiple_of((1 - core) * QB, QB), rows), :] = kv[...]
        kv_wide[pl.ds(pl.multiple_of(core * rows, QB), QB), :] = halo[:QB, :]
        edge = halo[QB:, :].astype(jnp.float32)
        pool_wide[:EDGE, :] = edge
        pool_wide[EDGE : EDGE + rows, :] = pool[...].astype(jnp.float32)
        pool_wide[EDGE + rows :, :] = edge

    lane = lax.broadcasted_iota(jnp.int32, (QB, LANES), 1)
    row = lax.broadcasted_iota(jnp.int32, (2 * QB, 3 * QB), 0) % QB
    column = lax.broadcasted_iota(jnp.int32, (2 * QB, 3 * QB), 1)
    near = (column >= row) & (column <= row + 2 * WINDOW)
    upper = lax.broadcasted_iota(jnp.int32, (2 * QB, 1), 0) < QB
    sinks = jnp.where(upper, first[:, HEAD : HEAD + 1], second[:, HEAD : HEAD + 1])
    half = lax.shift_left(1, group)
    start = pl.multiple_of(core * QB + 2 * QB * i, QB)
    block = first_block + core + 2 * i
    pair = q[pl.ds(start, QB), :]
    zero = jnp.zeros_like(pair)
    lower_head = jnp.where(lane < HEAD, pair, zero)
    upper_head = jnp.concatenate([pair[:, HEAD:], zero[:, HEAD:]], axis=1)
    queries = jnp.concatenate([lower_head, upper_head], axis=0)
    keys = kv_wide[pl.ds(pl.multiple_of(2 * QB * i, QB), 3 * QB), :]
    scores = lax.dot_general(
        queries, keys, (((1,), (1,)), ((), ())), preferred_element_type=jnp.float32
    )
    least = jnp.where(block == 0, QB, 0)
    limit = jnp.where(block == blocks_total - 1, 2 * QB, 3 * QB)
    valid = near & (column >= least) & (column < limit)
    scores = jnp.where(valid, scores, NEG_BIG)
    top = jnp.maximum(jnp.max(scores, axis=-1, keepdims=True), sinks)
    expo = jnp.where(valid, jnp.exp(scores - top), 0.0)
    total = jnp.sum(expo, axis=-1, keepdims=True) + jnp.exp(sinks - top)
    weights = (expo / total).astype(jnp.bfloat16)
    mixed = jnp.dot(weights, keys, preferred_element_type=jnp.float32)
    attended = jnp.concatenate([mixed[:QB, HEAD:], mixed[QB:, HEAD:]], axis=1)

    near_rows = pool_wide[pl.ds(start, QB + 2 * EDGE), :]
    size = QB + 2 * EDGE
    sums = near_rows + pltpu.roll(near_rows, 1, 0)
    chosen = sums
    for index in range(1, len(POOL_SPANS)):
        step = POOL_SPANS[index] // 4
        sums = pltpu.roll(sums, step, 0) + pltpu.roll(sums, size - step, 0)
        chosen = jnp.where(group == index, sums, chosen)
    position = block * QB + lax.broadcasted_iota(jnp.int32, (QB, 1), 0)
    counted = jnp.minimum(position + half, blocks_total * QB) - jnp.maximum(position - half, 0)
    mean = chosen[EDGE : EDGE + QB] / counted.astype(jnp.float32)
    pooled = (mean - near_rows[EDGE : EDGE + QB]) * scale
    both = jnp.concatenate([attended, pooled], axis=1).astype(jnp.bfloat16)
    for peer in range(out.shape[0]):
        out[peer] = both


def output_product(joined, own, other, out):
    core = lax.axis_index("c")
    peers = joined.shape[0]

    def product(columns):
        columns = columns.reshape(2 * peers, -1, LANES)
        total = None
        for i in range(peers):
            weights = jnp.concatenate([columns[i], columns[peers + i]], axis=1)
            part = lax.dot_general(
                joined[i], weights, (((1,), (1,)), ((), ())), preferred_element_type=jnp.float32
            )
            total = part if total is None else total + part
        return total.astype(jnp.bfloat16)

    mine, theirs = product(own[...]), product(other[...])
    out[...] = jnp.concatenate(
        [jnp.where(core == 0, mine, theirs), jnp.where(core == 0, theirs, mine)], axis=1
    )


def body(tokens, norm_gain, w_query, w_key, w_value, w_pool_in, sink_logit, pool_scale, w_out):
    rows, depth = tokens.shape
    sp_count = lax.axis_size(SP)
    bf16 = jnp.bfloat16

    out_piece = swapped(w_out.T)

    small = jnp.concatenate([pool_scale, jnp.broadcast_to(sink_logit, (HEAD,))])[None, :]
    small = three_parts(lax.optimization_barrier(small))
    small = jnp.pad(small, ((0, EDGE - 3), (0, depth - LANES)))
    own = jnp.concatenate([w_query.T, w_pool_in.T, small], axis=0)
    other = lax.ppermute(own, "c", [(0, 1), (1, 0)])

    cosine, sine = rope_tables(lax.axis_index(SP) * rows, rows)
    key_head = lax.axis_index("x") // (lax.axis_size("x") // (w_key.shape[1] // HEAD))
    key_cols = lax.dynamic_slice_in_dim(w_key, key_head * HEAD, HEAD, 1)
    value_cols = lax.dynamic_slice_in_dim(w_value, key_head * HEAD, HEAD, 1)
    both = jnp.concatenate([jnp.concatenate([key_cols, value_cols], axis=1), out_piece], axis=0)
    exchanged = from_everyone(both, SP)
    peers, pieces = exchanged.shape[0], key_cols.shape[0]

    at = lambda *shape: lambda *place: pl.BlockSpec(shape, lambda i: place)
    whole = lambda *shape: pl.BlockSpec(shape, lambda i: (0,) * len(shape))
    part = lambda *shape: pl.BlockSpec(shape, lambda i: (i,) + (0,) * (len(shape) - 1))
    along = lambda *shape: pl.BlockSpec(shape, lambda i: (0, i))
    shaped = lambda *shape: jax.ShapeDtypeStruct(shape, bf16)
    tables = [along(HEAD // 2, ROWS)] * 2
    normed, query, pool_in = pl.pallas_call(
        project,
        grid=(rows // ROWS,),
        in_specs=[part(ROWS, depth), whole(1, depth)] + [whole(*own.shape)] * 2 + tables,
        out_specs=[part(ROWS, depth), part(ROWS, LANES), part(ROWS, LANES)],
        out_shape=[shaped(rows, depth), shaped(rows, LANES), shaped(rows, LANES)],
        scratch_shapes=[pltpu.VMEM((2 * LANES, depth), bf16)],
        name="project",
        interpret=INTERPRET,
    )(tokens, norm_gain[None, :], own, other, cosine, sine)
    kv, send = pl.pallas_call(
        project_kv,
        grid=(rows // ROWS,),
        in_specs=[part(ROWS, depth), part(ROWS, LANES), whole(peers, pieces, LANES)] + tables,
        out_specs=[part(ROWS, LANES), whole(QB + EDGE, LANES)],
        out_shape=[shaped(rows, LANES), shaped(QB + EDGE, LANES)],
        name="project_kv",
        interpret=INTERPRET,
    )(normed, pool_in, exchanged, cosine, sine)

    pairs = [(2 * s, 2 * s + 2) for s in range(sp_count - 1)]
    pairs += [(2 * s + 3, 2 * s + 1) for s in range(sp_count - 1)]
    exchanged, send = lax.optimization_barrier((exchanged, send))
    halo = lax.ppermute(send, SP + ("c",), pairs)
    other_exchanged = lax.ppermute(exchanged, "c", [(0, 1), (1, 0)])

    peers_x = lax.axis_size("x")
    small_rows = at(EDGE, depth)(LANES // EDGE, 0)
    local = pl.pallas_call(
        mix,
        grid=(peers_x,),
        in_specs=[small_rows, small_rows]
        + [whole(rows, LANES)] * 3
        + [whole(QB + EDGE, LANES)],
        out_specs=pl.BlockSpec((peers_x, QB, 2 * LANES), lambda i: (0, i, 0)),
        out_shape=shaped(peers_x, rows // 2, 2 * LANES),
        scratch_shapes=[
            pltpu.VMEM((rows + QB, LANES), bf16),
            pltpu.VMEM((rows + 2 * EDGE, LANES), jnp.float32),
        ],
        name="mix",
        interpret=INTERPRET,
    )(own, other, query, kv, pool_in, halo)

    local, other_exchanged = lax.optimization_barrier((local, other_exchanged))
    joined = lax.all_to_all(local, "x", 0, 0, tiled=True)
    columns = at(peers, pieces, LANES)(0, 1, 0)
    width = 2 * peers // lax.axis_size("z") * pieces
    partial_cols = pl.pallas_call(
        output_product,
        grid=(1,),
        in_specs=[whole(*joined.shape), columns, columns],
        out_specs=whole(rows // 2, width),
        out_shape=shaped(rows // 2, width),
        name="output_product",
        interpret=INTERPRET,
    )(joined, exchanged, other_exchanged)
    return lax.all_to_all(partial_cols, "x", split_axis=0, concat_axis=1, tiled=True)


def solution(mesh):
    devices = mesh.devices
    mesh = Mesh(devices.reshape(8, devices.size // 64, 4, 2), SP + TP)
    in_specs = (
        P(SP, None),
        P(),
        P(None, TP),
        P(SP, None),
        P(SP, None),
        P(None, TP),
        P(TP),
        P(TP),
        P(TP, SP),
    )
    out_specs = P(SP + TP, None)
    return jax.shard_map(body, mesh=mesh, in_specs=in_specs, out_specs=out_specs, check_vma=False)
```

time: 126 us -> 116 us (0.921)
  blocking collectives: 72.8 us -> 31.1 us
  starting transfers between devices: 16 us -> 38.7 us
  waiting for transfers between devices: 3.62 us -> 16 us
  between operations: 4.44 us -> 0.8 us
  other arithmetic: 4.25 us -> 1.41 us
  Pallas kernels: 18.3 us -> 20.7 us
    all_to_all x1 -> x0, blocking collectives: 39.1 us -> none  [from_everyone(): lax.all_to_all(jnp.broadcast_to(x[None], (peers, *x.shape)), axis, 0, 0,...]
    all_to_all x0 -> x1, starting transfers between devices: none -> 21.2 us  [from_everyone(): lax.all_to_all(jnp.broadcast_to(x[None], (peers, *x.shape)), axis, 0, 0,...]
    all_to_all x0 -> x1, waiting for transfers between devices: none -> 11.3 us  [from_everyone(): lax.all_to_all(jnp.broadcast_to(x[None], (peers, *x.shape)), axis, 0, 0,...]
    pallas_call x2 -> x3, Pallas kernels: 9.58 us -> 13.4 us  [the longest x1 5.23 us: body(): pl.pallas_call(mix, grid=(peers_x,), in_specs=[small_rows, small_rows] +...]
    all_to_all x1, blocking collectives: 22 us -> 19.2 us  [body(): joined = lax.all_to_all(local, 'x', 0, 0, tiled=True)]
    ppermute x1, starting transfers between devices: 4.64 us -> 6.81 us  [body(): other_exchanged = lax.ppermute(exchanged, 'c', [(0, 1), (1, 0)])]
    sin x1, other arithmetic: 3.05 us -> 1.24 us  [rope_tables(): return (jnp.cos(angles), jnp.sin(angles))]
    pallas_call x1, Pallas kernels: 8.74 us -> 7.34 us  [body(): pl.pallas_call(project, grid=(rows // ROWS,), in_specs=[part(ROWS, depth)...]
  transfers between devices with their start and end apart: 4 -> 5, of which waited for: 1 -> 4; matrix products, arithmetic and copies ran while one was open for 6% -> 2% of each run, Pallas kernels for 11% -> 11%
where the time goes in v4:
time: 116 us; the launch traced here: 114 us
  starting transfers between devices  38.7 us (33%)
  blocking collectives  31.1 us (27%)
  Pallas kernels  20.7 us (18%)
  waiting for transfers between devices  16 us (14%)
  local copies, waits for them, and re-layouts  5.3 us (5%)
  other arithmetic  1.41 us (1%)
    all_to_all x1, starting transfers between devices, from_everyone(): lax.all_to_all(jnp.broadcast_to(x[None], (peers, *x.shape)), axis, 0, 0,...  21.2 us
    all_to_all x1, blocking collectives, body(): joined = lax.all_to_all(local, 'x', 0, 0, tiled=True)  19.2 us
    all_to_all x1, blocking collectives, body(): lax.all_to_all(partial_cols, 'x', split_axis=0, concat_axis=1, tiled=True)  11.9 us
    all_to_all x1, waiting for transfers between devices, from_everyone(): lax.all_to_all(jnp.broadcast_to(x[None], (peers, *x.shape)), axis, 0, 0,...  11.3 us
    pallas_call x1, Pallas kernels, body(): pl.pallas_call(project, grid=(rows // ROWS,), in_specs=[part(ROWS, depth)...  7.34 us
    ppermute x1, starting transfers between devices, body(): other_exchanged = lax.ppermute(exchanged, 'c', [(0, 1), (1, 0)])  6.81 us
    ppermute x1, starting transfers between devices, swapped(): return lax.ppermute(piece, SP + TP, pairs)  5.37 us
    pallas_call x1, Pallas kernels, body(): pl.pallas_call(mix, grid=(peers_x,), in_specs=[small_rows, small_rows] +...  5.23 us
  transfers between devices with their start and end apart: 5, of which 4 were waited for; matrix products, arithmetic and copies ran while one was open for 2% of the time, Pallas kernels for 11%

profile of v4, /device:TPU:1, one launch (start us, length us, event | category | flops | bytes accessed | tf_op | source)
XLA Modules:
  0.0 114.1 jit_solution(8301322257097635646)
XLA Ops:
  0.0 5.4 %collective-permute-start.1 = (bf16[32,128]{1,0:T(8,128)(2,1)}, bf16[32,128]{1,0:T(8,128)(2,1)S(1)}, u32[]{:S(2)}, u32[]{:S(2)}) collective-permute-start(bf16[32,128]{1,0:T(8,128)(2,1)} %bitcast.17), channel_id=1, source_target_pairs={{0,0},{1,64},{2,128},{3,192},{4,256},{5,320},{6,384},{7,448},{8,8}... | collective-permute-start | bytes 24584 | tf_op jit(solution)/shard_map/ppermute | solution.py:38
  5.4 0.8 constant_dynamic-slice_fusion
  6.2 0.7 collective-permute-done.1
  6.9 0.1 pad_maximum_fusion.1
  7.0 1.2 %broadcast_in_dim.22 = bf16[64,64,128]{2,1,0:T(8,128)(2,1)} broadcast(bf16[64,128]{1,0:T(8,128)(2,1)S(1)} %pad_maximum_fusion.1), dimensions={1,2} | broadcast | bytes 1064960 | tf_op jit(solution)/shard_map/broadcast_in_dim | solution.py:26
  8.2 21.2 %all-to-all-start = ((bf16[64,64,128]{2,1,0:T(8,128)(2,1)}), bf16[64,64,128]{2,1,0:T(8,128)(2,1)S(1)}, u32[]{:S(2)}, u32[]{:S(2)}) async-start(bf16[64,64,128]{2,1,0:T(8,128)(2,1)} %broadcast_in_dim.22), calls=%async_computation | async-start | bytes 2097152 | tf_op jit(solution)/shard_map/all_to_all | solution.py:26
  30.2 4.0 %collective-permute-start = (bf16[144,2048]{1,0:T(8,128)(2,1)S(1)}, bf16[144,2048]{1,0:T(8,128)(2,1)S(1)}, u32[]{:S(2)}, u32[]{:S(2)}) collective-permute-start(bf16[144,2048]{1,0:T(8,128)(2,1)S(1)} %pad_maximum_fusion.own), channel_id=1, source_target_pairs={{0,1},{1,0},{2,3},{3,2},{4,5},{5,4},{6,7},{7,6},{8,9},{9,8},{10,11... | collective-permute-start | bytes 1769480 | tf_op jit(solution)/shard_map/ppermute | solution.py:210
  34.3 1.2 %multiply_sine_fusion = (f32[32,1024]{1,0:T(8,128)}, f32[32,1024]{1,0:T(8,128)}) fusion(f32[32]{0:T(128)S(1)} %multiply_power_fusion, f32[1024]{0:T(1024)S(1)} %add_convert_fusion), kind=kLoop, calls=%fused_computation.1 | loop fusion | flops 32768 | bytes 266368 | tf_op jit(solution)/shard_map/sin | solution.py:53
  35.5 0.3 collective-permute-done.other
  35.9 0.8 copy-done.2
  36.7 7.3 %project.1 = (bf16[1024,2048]{1,0:T(8,128)(2,1)}, bf16[1024,128]{1,0:T(8,128)(2,1)}, bf16[1024,128]{1,0:T(8,128)(2,1)}) custom-call(bf16[1024,2048]{1,0:T(8,128)(2,1)} %tokens.1, f32[1,2048]{1,0:T(1,128)} %bitcast.16, bf16[144,2048]{1,0:T(8,128)(2,1)} %copy-done.1, bf16[144,2048]{1,0:T(8,128)(2,1)} %copy-done.2, f32[32,1024]{1,0:T(8,128)} %get-tuple-element.24.cosine, ...), custom_call_target="tpu_custom_call" | custom-call | tf_op jit(solution)/shard_map/project/pallas_call | solution.py:226
  44.0 11.3 %all-to-all-done.ex.own = bf16[64,64,128]{2,1,0:T(8,128)(2,1)S(1)} async-done(((bf16[64,64,128]{2,1,0:T(8,128)(2,1)}), bf16[64,64,128]{2,1,0:T(8,128)(2,1)S(1)}, u32[]{:S(2)}, u32[]{:S(2)}) %all-to-all-start) | async-done | bytes 1048608 | tf_op jit(solution)/shard_map/all_to_all | solution.py:26
  55.4 1.0 copy-done
  56.4 5.1 %project_kv.1 = (bf16[1024,128]{1,0:T(8,128)(2,1)}, bf16[144,128]{1,0:T(8,128)(2,1)}) custom-call(bf16[1024,2048]{1,0:T(8,128)(2,1)} %get-tuple-element.15.normed, bf16[1024,128]{1,0:T(8,128)(2,1)} %get-tuple-element.16.pool, bf16[64,64,128]{2,1,0:T(8,128)(2,1)} %copy-done, f32[32,1024]{1,0:T(8,128)} %get-tuple-element.24.cosine, ...), custom_call_target="tpu_custom_call" | custom-call | tf_op jit(solution)/shard_map/project_kv/pallas_call | solution.py:236
  61.4 6.8 %collective-permute-start.3 = (bf16[64,64,128]{2,1,0:T(8,128)(2,1)}, bf16[64,64,128]{2,1,0:T(8,128)(2,1)S(1)}, u32[]{:S(2)}, u32[]{:S(2)}) collective-permute-start(bf16[64,64,128]{2,1,0:T(8,128)(2,1)} %copy-done), channel_id=1, source_target_pairs={{0,1},{1,0},{2,3},{3,2},{4,5},{5,4},{6,7},{7,6},{8,9},{9,8},{10,11... | collective-permute-start | bytes 3145736 | tf_op jit(solution)/shard_map/ppermute | solution.py:250
  68.2 1.3 %collective-permute-start.2 = (bf16[144,128]{1,0:T(8,128)(2,1)}, bf16[144,128]{1,0:T(8,128)(2,1)S(1)}, u32[]{:S(2)}, u32[]{:S(2)}) collective-permute-start(bf16[144,128]{1,0:T(8,128)(2,1)} %get-tuple-element.19), channel_id=1, source_target_pairs={{0,8},{8,16},{16,24},{24,32},{32,40},{40,48},{48,56},{56,64},{64,7... | collective-permute-start | bytes 110600 | tf_op jit(solution)/shard_map/ppermute | solution.py:249
  69.5 3.6 %collective-permute-done.2.halo = bf16[144,128]{1,0:T(8,128)(2,1)S(1)} collective-permute-done((bf16[144,128]{1,0:T(8,128)(2,1)}, bf16[144,128]{1,0:T(8,128)(2,1)S(1)}, u32[]{:S(2)}, u32[]{:S(2)}) %collective-permute-start.2) | collective-permute-done | bytes 36896 | tf_op jit(solution)/shard_map/ppermute | solution.py:249
  73.1 0.6 copy-done.6
  73.8 5.2 %mix.1 = bf16[4,512,256]{2,1,0:T(8,128)(2,1)} custom-call(bf16[144,2048]{1,0:T(8,128)(2,1)} %copy-done.1, bf16[144,2048]{1,0:T(8,128)(2,1)} %copy-done.2, bf16[1024,128]{1,0:T(8,128)(2,1)} %get-tuple-element.14.q, bf16[1024,128]{1,0:T(8,128)(2,1)} %get-tuple-element.17.kv, bf16[1024,128]{1,0:T(8,128)(2,1)} %get-tuple-element.16.pool, bf16[144,128]{1,0:T(8,128)(2,1)} %copy-done.6), custom_call_target="tpu_custom_call" | custom-call | tf_op jit(solution)/shard_map/mix/pallas_call | solution.py:254
  79.0 0.0 collective-permute-done.3.other
  79.0 19.2 %all_to_all.29.joined = bf16[4,512,256]{2,1,0:T(8,128)(2,1)} all-to-all(bf16[4,512,256]{2,1,0:T(8,128)(2,1)} %mix.1), channel_id=1, replica_groups=mesh['z'=8,'y'=8,'x'=4,'c'=2] {'x'}, dimensions={0} | all-to-all | bytes 2097152 | tf_op jit(solution)/shard_map/all_to_all | solution.py:271
  98.2 3.1 %output_product.1 = bf16[512,512]{1,0:T(8,128)(2,1)} custom-call(bf16[4,512,256]{2,1,0:T(8,128)(2,1)} %all_to_all.29.joined, bf16[64,64,128]{2,1,0:T(8,128)(2,1)} %copy-done, bf16[64,64,128]{2,1,0:T(8,128)(2,1)} %copy-done.3), custom_call_target="tpu_custom_call" | custom-call | tf_op jit(solution)/shard_map/output_product/pallas_call | solution.py:274
  101.4 11.9 %all_to_all.30 = bf16[4,128,512]{2,1,0:T(8,128)(2,1)S(1)} all-to-all(bf16[4,128,512]{2,1,0:T(8,128)(2,1)} %bitcast.12), channel_id=1, replica_groups=mesh['z'=8,'y'=8,'x'=4,'c'=2] {'x'}, dimensions={0} | all-to-all | bytes 1048576 | tf_op jit(solution)/shard_map/all_to_all | solution.py:283
  113.2 0.8 copy.11
  (19 shorter events, 0.1 us)
Async XLA Ops:
  0.0 6.9 %collective-permute-start.1 = (bf16[32,128]{1,0:T(8,128)(2,1)}, bf16[32,128]{1,0:T(8,128)(2,1)S(1)}, u32[]{:S(2)}, u32[]{:S(2)}) collective-permute-start(bf16[32,128]{1,0:T(8,128)(2,1)} %bitcast.17), channel_id=1, source_target_pairs={{0,0},{1,64},{2,128},{3,192},{4,256},{5,320},{6,384},{7,448},{8,8}... | collective-permute-start | bytes 24584 | tf_op jit(solution)/shard_map/ppermute | solution.py:38
  8.2 21.9 %copy-start.7 = (f32[64]{0:T(128)S(1)}, f32[64]{0:T(128)}, u32[]{:S(2)}) copy-start(f32[64]{0:T(128)} %param.16) | copy-start | bytes 772
  8.2 21.9 %copy-start.4 = (bf16[2048,64]{0,1:T(8,128)(2,1)S(1)}, bf16[2048,64]{0,1:T(8,128)(2,1)}, u32[]{:S(2)}) copy-start(bf16[2048,64]{0,1:T(8,128)(2,1)} %param.14) | copy-start | bytes 786436
  8.2 22.0 %copy-start.5 = (bf16[2048,64]{0,1:T(8,128)(2,1)S(1)}, bf16[2048,64]{0,1:T(8,128)(2,1)}, u32[]{:S(2)}) copy-start(bf16[2048,64]{0,1:T(8,128)(2,1)} %param.11) | copy-start | bytes 786436
  8.2 47.2 %all-to-all-start = ((bf16[64,64,128]{2,1,0:T(8,128)(2,1)}), bf16[64,64,128]{2,1,0:T(8,128)(2,1)S(1)}, u32[]{:S(2)}, u32[]{:S(2)}) async-start(bf16[64,64,128]{2,1,0:T(8,128)(2,1)} %broadcast_in_dim.22), calls=%async_computation | async-start | bytes 2097152 | tf_op jit(solution)/shard_map/all_to_all | solution.py:26
  30.2 5.6 %copy-start.1 = (bf16[144,2048]{1,0:T(8,128)(2,1)}, bf16[144,2048]{1,0:T(8,128)(2,1)S(1)}, u32[]{:S(2)}) copy-start(bf16[144,2048]{1,0:T(8,128)(2,1)S(1)} %pad_maximum_fusion.own) | copy-start | bytes 1769476
  30.2 5.6 %collective-permute-start = (bf16[144,2048]{1,0:T(8,128)(2,1)S(1)}, bf16[144,2048]{1,0:T(8,128)(2,1)S(1)}, u32[]{:S(2)}, u32[]{:S(2)}) collective-permute-start(bf16[144,2048]{1,0:T(8,128)(2,1)S(1)} %pad_maximum_fusion.own), channel_id=1, source_target_pairs={{0,1},{1,0},{2,3},{3,2},{4,5},{5,4},{6,7},{7,6},{8,9},{9,8},{10,11... | collective-permute-start | bytes 1769480 | tf_op jit(solution)/shard_map/ppermute | solution.py:210
  35.9 0.8 copy-start.2
  55.4 1.0 copy-start
  61.4 17.6 %collective-permute-start.3 = (bf16[64,64,128]{2,1,0:T(8,128)(2,1)}, bf16[64,64,128]{2,1,0:T(8,128)(2,1)S(1)}, u32[]{:S(2)}, u32[]{:S(2)}) collective-permute-start(bf16[64,64,128]{2,1,0:T(8,128)(2,1)} %copy-done), channel_id=1, source_target_pairs={{0,1},{1,0},{2,3},{3,2},{4,5},{5,4},{6,7},{7,6},{8,9},{9,8},{10,11... | collective-permute-start | bytes 3145736 | tf_op jit(solution)/shard_map/ppermute | solution.py:250
  68.2 4.9 %collective-permute-start.2 = (bf16[144,128]{1,0:T(8,128)(2,1)}, bf16[144,128]{1,0:T(8,128)(2,1)S(1)}, u32[]{:S(2)}, u32[]{:S(2)}) collective-permute-start(bf16[144,128]{1,0:T(8,128)(2,1)} %get-tuple-element.19), channel_id=1, source_target_pairs={{0,8},{8,16},{16,24},{24,32},{32,40},{40,48},{48,56},{56,64},{64,7... | collective-permute-start | bytes 110600 | tf_op jit(solution)/shard_map/ppermute | solution.py:249
  73.1 0.6 copy-start.6
  79.0 19.3 %copy-start.3 = (bf16[64,64,128]{2,1,0:T(8,128)(2,1)}, bf16[64,64,128]{2,1,0:T(8,128)(2,1)S(1)}, u32[]{:S(2)}) copy-start(bf16[64,64,128]{2,1,0:T(8,128)(2,1)S(1)} %collective-permute-done.3.other) | copy-start | bytes 3145732

commit v5 on v4

--- a/solution.py
+++ b/solution.py
@@ -1,5 +1,3 @@
-import functools
-
 import jax
 import jax.numpy as jnp
 from jax import lax
@@ -201,6 +199,12 @@
     sp_count = lax.axis_size(SP)
     bf16 = jnp.bfloat16
 
+    key_head = lax.axis_index("x") // (lax.axis_size("x") // (w_key.shape[1] // HEAD))
+    key_cols = lax.dynamic_slice_in_dim(w_key, key_head * HEAD, HEAD, 1)
+    value_cols = lax.dynamic_slice_in_dim(w_value, key_head * HEAD, HEAD, 1)
+    exchanged = from_everyone(jnp.concatenate([key_cols, value_cols], axis=1), SP)
+    peers, pieces = exchanged.shape[:2]
+
     out_piece = swapped(w_out.T)
 
     small = jnp.concatenate([pool_scale, jnp.broadcast_to(sink_logit, (HEAD,))])[None, :]
@@ -210,12 +214,6 @@
     other = lax.ppermute(own, "c", [(0, 1), (1, 0)])
 
     cosine, sine = rope_tables(lax.axis_index(SP) * rows, rows)
-    key_head = lax.axis_index("x") // (lax.axis_size("x") // (w_key.shape[1] // HEAD))
-    key_cols = lax.dynamic_slice_in_dim(w_key, key_head * HEAD, HEAD, 1)
-    value_cols = lax.dynamic_slice_in_dim(w_value, key_head * HEAD, HEAD, 1)
-    both = jnp.concatenate([jnp.concatenate([key_cols, value_cols], axis=1), out_piece], axis=0)
-    exchanged = from_everyone(both, SP)
-    peers, pieces = exchanged.shape[0], key_cols.shape[0]
 
     at = lambda *shape: lambda *place: pl.BlockSpec(shape, lambda i: place)
     whole = lambda *shape: pl.BlockSpec(shape, lambda i: (0,) * len(shape))
@@ -245,9 +243,9 @@
 
     pairs = [(2 * s, 2 * s + 2) for s in range(sp_count - 1)]
     pairs += [(2 * s + 3, 2 * s + 1) for s in range(sp_count - 1)]
-    exchanged, send = lax.optimization_barrier((exchanged, send))
+    out_piece, send = lax.optimization_barrier((out_piece, send))
     halo = lax.ppermute(send, SP + ("c",), pairs)
-    other_exchanged = lax.ppermute(exchanged, "c", [(0, 1), (1, 0)])
+    own_cols = from_everyone(out_piece, SP)
 
     peers_x = lax.axis_size("x")
     small_rows = at(EDGE, depth)(LANES // EDGE, 0)
@@ -267,19 +265,20 @@
         interpret=INTERPRET,
     )(own, other, query, kv, pool_in, halo)
 
-    local, other_exchanged = lax.optimization_barrier((local, other_exchanged))
+    local, own_cols = lax.optimization_barrier((local, own_cols))
+    other_cols = lax.ppermute(own_cols, "c", [(0, 1), (1, 0)])
     joined = lax.all_to_all(local, "x", 0, 0, tiled=True)
-    columns = at(peers, pieces, LANES)(0, 1, 0)
+    pieces = out_piece.shape[0]
     width = 2 * peers // lax.axis_size("z") * pieces
     partial_cols = pl.pallas_call(
         output_product,
         grid=(1,),
-        in_specs=[whole(*joined.shape), columns, columns],
+        in_specs=[whole(*joined.shape)] + [whole(peers, pieces, LANES)] * 2,
         out_specs=whole(rows // 2, width),
         out_shape=shaped(rows // 2, width),
         name="output_product",
         interpret=INTERPRET,
-    )(joined, exchanged, other_exchanged)
+    )(joined, own_cols, other_cols)
     return lax.all_to_all(partial_cols, "x", split_axis=0, concat_axis=1, tiled=True)
 
 

time: 116 us -> 113 us (0.974)
  the two profiles are of different devices: /device:TPU:1 before, /device:TPU:24 now
where the time goes in v5:
time: 113 us; the launch traced here: 112 us
  starting transfers between devices  41.6 us (37%)
  waiting for transfers between devices  27.2 us (24%)
  Pallas kernels  21 us (19%)
  blocking collectives  13.5 us (12%)
  local copies, waits for them, and re-layouts  6.72 us (6%)
  other arithmetic  1.41 us (1%)
    all_to_all x2, starting transfers between devices, from_everyone(): lax.all_to_all(jnp.broadcast_to(x[None], (peers, *x.shape)), axis, 0, 0,...  27.7 us
    all_to_all x1, blocking collectives, body(): lax.all_to_all(partial_cols, 'x', split_axis=0, concat_axis=1, tiled=True)  13.5 us
    all_to_all x1, waiting for transfers between devices, body(): joined = lax.all_to_all(local, 'x', 0, 0, tiled=True)  11.3 us
    ppermute x1, waiting for transfers between devices, body(): halo = lax.ppermute(send, SP + ('c',), pairs)  7.94 us
    pallas_call x1, Pallas kernels, body(): pl.pallas_call(project, grid=(rows // ROWS,), in_specs=[part(ROWS, depth)...  7.35 us
    all_to_all x2, waiting for transfers between devices, from_everyone(): lax.all_to_all(jnp.broadcast_to(x[None], (peers, *x.shape)), axis, 0, 0,...  6.39 us
    pallas_call x1, Pallas kernels, body(): pl.pallas_call(project_kv, grid=(rows // ROWS,), in_specs=[part(ROWS, dep...  5.38 us
    pallas_call x1, Pallas kernels, body(): pl.pallas_call(mix, grid=(peers_x,), in_specs=[small_rows, small_rows] +...  5.25 us
  transfers between devices with their start and end apart: 7, of which 5 were waited for; matrix products, arithmetic and copies ran while one was open for 1% of the time, Pallas kernels for 16%

profile of v5, /device:TPU:24, one launch (start us, length us, event | category | flops | bytes accessed | tf_op | source)
XLA Modules:
  0.0 112.3 jit_solution(13817654787494843207)
XLA Ops:
  0.0 0.8 constant_dynamic-slice_fusion
  1.0 0.9 broadcast_in_dim.13
  1.8 16.5 %all-to-all-start = ((bf16[64,32,128]{2,1,0:T(8,128)(2,1)}), bf16[64,32,128]{2,1,0:T(8,128)(2,1)S(1)}, u32[]{:S(2)}, u32[]{:S(2)}) async-start(bf16[64,32,128]{2,1,0:T(8,128)(2,1)} %broadcast_in_dim.13), calls=%async_computation | async-start | bytes 1048576 | tf_op jit(solution)/shard_map/all_to_all | solution.py:24
  19.1 1.9 %collective-permute-start = (bf16[144,2048]{1,0:T(8,128)(2,1)S(1)}, bf16[144,2048]{1,0:T(8,128)(2,1)S(1)}, u32[]{:S(2)}, u32[]{:S(2)}) collective-permute-start(bf16[144,2048]{1,0:T(8,128)(2,1)S(1)} %pad_maximum_fusion.own), channel_id=1, source_target_pairs={{0,1},{1,0},{2,3},{3,2},{4,5},{5,4},{6,7},{7,6},{8,9},{9,8},{10,11... | collective-permute-start | bytes 1769480 | tf_op jit(solution)/shard_map/ppermute | solution.py:214
  21.7 1.2 %multiply_sine_fusion = (f32[32,1024]{1,0:T(8,128)}, f32[32,1024]{1,0:T(8,128)}) fusion(f32[32]{0:T(128)S(1)} %multiply_power_fusion, f32[1024]{0:T(1024)S(1)} %add_convert_fusion), kind=kLoop, calls=%fused_computation.1 | loop fusion | flops 32768 | bytes 266368 | tf_op jit(solution)/shard_map/sin | solution.py:51
  23.0 0.8 copy-done.2
  23.8 7.3 %project.1 = (bf16[1024,2048]{1,0:T(8,128)(2,1)}, bf16[1024,128]{1,0:T(8,128)(2,1)}, bf16[1024,128]{1,0:T(8,128)(2,1)}) custom-call(bf16[1024,2048]{1,0:T(8,128)(2,1)} %tokens.1, f32[1,2048]{1,0:T(1,128)} %bitcast.16, bf16[144,2048]{1,0:T(8,128)(2,1)} %copy-done, bf16[144,2048]{1,0:T(8,128)(2,1)} %copy-done.2, f32[32,1024]{1,0:T(8,128)} %get-tuple-element.24.cosine, ...), custom_call_target="tpu_custom_call" | custom-call | tf_op jit(solution)/shard_map/project/pallas_call | solution.py:224
  31.2 5.7 %all-to-all-done.ex = bf16[64,32,128]{2,1,0:T(8,128)(2,1)S(1)} async-done(((bf16[64,32,128]{2,1,0:T(8,128)(2,1)}), bf16[64,32,128]{2,1,0:T(8,128)(2,1)S(1)}, u32[]{:S(2)}, u32[]{:S(2)}) %all-to-all-start) | async-done | bytes 524320 | tf_op jit(solution)/shard_map/all_to_all | solution.py:24
  36.9 0.8 copy-done.3
  37.7 5.4 %project_kv.1 = (bf16[1024,128]{1,0:T(8,128)(2,1)}, bf16[144,128]{1,0:T(8,128)(2,1)}) custom-call(bf16[1024,2048]{1,0:T(8,128)(2,1)} %get-tuple-element.15.normed, bf16[1024,128]{1,0:T(8,128)(2,1)} %get-tuple-element.16.pool, bf16[64,32,128]{2,1,0:T(8,128)(2,1)} %copy-done.3, f32[32,1024]{1,0:T(8,128)} %get-tuple-element.24.cosine, ...), custom_call_target="tpu_custom_call" | custom-call | tf_op jit(solution)/shard_map/project_kv/pallas_call | solution.py:234
  43.0 0.9 broadcast_in_dim.14
  43.9 11.2 %all-to-all-start.1 = ((bf16[64,32,128]{2,1,0:T(8,128)(2,1)}), bf16[64,32,128]{2,1,0:T(8,128)(2,1)S(1)}, u32[]{:S(2)}, u32[]{:S(2)}) async-start(bf16[64,32,128]{2,1,0:T(8,128)(2,1)} %broadcast_in_dim.14), calls=%async_computation.1 | async-start | bytes 1048576 | tf_op jit(solution)/shard_map/all_to_all | solution.py:24
  55.1 4.6 %collective-permute-start.2 = (bf16[144,128]{1,0:T(8,128)(2,1)S(1)}, bf16[144,128]{1,0:T(8,128)(2,1)S(1)}, u32[]{:S(2)}, u32[]{:S(2)}) collective-permute-start(bf16[144,128]{1,0:T(8,128)(2,1)S(1)} %copy-done.9), channel_id=1, source_target_pairs={{0,8},{8,16},{16,24},{24,32},{32,40},{40,48},{48,56},{56,64},{64,7... | collective-permute-start | bytes 110600 | tf_op jit(solution)/shard_map/ppermute | solution.py:247
  59.7 7.9 %collective-permute-done.2.halo = bf16[144,128]{1,0:T(8,128)(2,1)S(1)} collective-permute-done((bf16[144,128]{1,0:T(8,128)(2,1)S(1)}, bf16[144,128]{1,0:T(8,128)(2,1)S(1)}, u32[]{:S(2)}, u32[]{:S(2)}) %collective-permute-start.2) | collective-permute-done | bytes 36896 | tf_op jit(solution)/shard_map/ppermute | solution.py:247
  68.3 5.3 %mix.1 = bf16[4,512,256]{2,1,0:T(8,128)(2,1)} custom-call(bf16[144,2048]{1,0:T(8,128)(2,1)} %copy-done, bf16[144,2048]{1,0:T(8,128)(2,1)} %copy-done.2, bf16[1024,128]{1,0:T(8,128)(2,1)} %get-tuple-element.14.q, bf16[1024,128]{1,0:T(8,128)(2,1)} %get-tuple-element.17.kv, bf16[1024,128]{1,0:T(8,128)(2,1)} %get-tuple-element.16.pool, bf16[144,128]{1,0:T(8,128)(2,1)} %copy-done.8), custom_call_target="tpu_custom_call" | custom-call | tf_op jit(solution)/shard_map/mix/pallas_call | solution.py:252
  73.5 0.7 all-to-all-done.1.own
  74.2 3.5 %all-to-all-start.2 = ((bf16[4,512,256]{2,1,0:T(8,128)(2,1)}), bf16[4,512,256]{2,1,0:T(8,128)(2,1)S(1)}, u32[]{:S(2)}, u32[]{:S(2)}) async-start(bf16[4,512,256]{2,1,0:T(8,128)(2,1)} %mix.1), calls=%async_computation.2 | async-start | bytes 2097152 | tf_op jit(solution)/shard_map/all_to_all | solution.py:270
  77.8 3.2 %collective-permute-start.3 = (bf16[64,32,128]{2,1,0:T(8,128)(2,1)S(1)}, bf16[64,32,128]{2,1,0:T(8,128)(2,1)S(1)}, u32[]{:S(2)}, u32[]{:S(2)}) collective-permute-start(bf16[64,32,128]{2,1,0:T(8,128)(2,1)S(1)} %all-to-all-done.1.own), channel_id=1, source_target_pairs={{0,1},{1,0},{2,3},{3,2},{4,5},{5,4},{6,7},{7,6},{8,9},{9,8},{10,11... | collective-permute-start | bytes 1572872 | tf_op jit(solution)/shard_map/ppermute | solution.py:269
  81.0 1.5 %collective-permute-done.3.other = bf16[64,32,128]{2,1,0:T(8,128)(2,1)S(1)} collective-permute-done((bf16[64,32,128]{2,1,0:T(8,128)(2,1)S(1)}, bf16[64,32,128]{2,1,0:T(8,128)(2,1)S(1)}, u32[]{:S(2)}, u32[]{:S(2)}) %collective-permute-start.3) | collective-permute-done | bytes 524320 | tf_op jit(solution)/shard_map/ppermute | solution.py:269
  82.5 11.3 %all-to-all-done.2.joined = bf16[4,512,256]{2,1,0:T(8,128)(2,1)S(1)} async-done(((bf16[4,512,256]{2,1,0:T(8,128)(2,1)}), bf16[4,512,256]{2,1,0:T(8,128)(2,1)S(1)}, u32[]{:S(2)}, u32[]{:S(2)}) %all-to-all-start.2) | async-done | bytes 1048608 | tf_op jit(solution)/shard_map/all_to_all | solution.py:270
  93.9 1.0 copy-done.1
  94.9 3.0 %output_product.1 = bf16[512,512]{1,0:T(8,128)(2,1)} custom-call(bf16[4,512,256]{2,1,0:T(8,128)(2,1)} %copy-done.1, bf16[64,32,128]{2,1,0:T(8,128)(2,1)} %copy-done.4, bf16[64,32,128]{2,1,0:T(8,128)(2,1)} %copy-done.5), custom_call_target="tpu_custom_call" | custom-call | tf_op jit(solution)/shard_map/output_product/pallas_call | solution.py:273
  98.0 13.5 %all_to_all.34 = bf16[4,128,512]{2,1,0:T(8,128)(2,1)S(1)} all-to-all(bf16[4,128,512]{2,1,0:T(8,128)(2,1)} %bitcast.12), channel_id=1, replica_groups=mesh['z'=8,'y'=8,'x'=4,'c'=2] {'x'}, dimensions={0} | all-to-all | bytes 1048576 | tf_op jit(solution)/shard_map/all_to_all | solution.py:282
  111.5 0.8 copy.11
  (31 shorter events, 1.5 us)
Async XLA Ops:
  0.0 19.0 %copy-start.11 = (f32[64]{0:T(128)S(1)}, f32[64]{0:T(128)}, u32[]{:S(2)}) copy-start(f32[64]{0:T(128)} %param.16) | copy-start | bytes 772
  0.0 19.0 %copy-start.7 = (bf16[2048,64]{0,1:T(8,128)(2,1)S(1)}, bf16[2048,64]{0,1:T(8,128)(2,1)}, u32[]{:S(2)}) copy-start(bf16[2048,64]{0,1:T(8,128)(2,1)} %param.11) | copy-start | bytes 786436
  0.0 19.0 %copy-start.6 = (bf16[2048,64]{0,1:T(8,128)(2,1)S(1)}, bf16[2048,64]{0,1:T(8,128)(2,1)}, u32[]{:S(2)}) copy-start(bf16[2048,64]{0,1:T(8,128)(2,1)} %param.14) | copy-start | bytes 786436
  1.8 19.2 %copy-start.10 = (bf16[128,32]{0,1:T(8,128)(2,1)S(1)}, bf16[128,32]{0,1:T(8,128)(2,1)}, u32[]{:S(2)}) copy-start(bf16[128,32]{0,1:T(8,128)(2,1)} %param.17) | copy-start | bytes 24580
  1.8 35.0 %all-to-all-start = ((bf16[64,32,128]{2,1,0:T(8,128)(2,1)}), bf16[64,32,128]{2,1,0:T(8,128)(2,1)S(1)}, u32[]{:S(2)}, u32[]{:S(2)}) async-start(bf16[64,32,128]{2,1,0:T(8,128)(2,1)} %broadcast_in_dim.13), calls=%async_computation | async-start | bytes 1048576 | tf_op jit(solution)/shard_map/all_to_all | solution.py:24
  19.1 3.9 %copy-start = (bf16[144,2048]{1,0:T(8,128)(2,1)}, bf16[144,2048]{1,0:T(8,128)(2,1)S(1)}, u32[]{:S(2)}) copy-start(bf16[144,2048]{1,0:T(8,128)(2,1)S(1)} %pad_maximum_fusion.own) | copy-start | bytes 1769476
  19.1 3.9 %collective-permute-start = (bf16[144,2048]{1,0:T(8,128)(2,1)S(1)}, bf16[144,2048]{1,0:T(8,128)(2,1)S(1)}, u32[]{:S(2)}, u32[]{:S(2)}) collective-permute-start(bf16[144,2048]{1,0:T(8,128)(2,1)S(1)} %pad_maximum_fusion.own), channel_id=1, source_target_pairs={{0,1},{1,0},{2,3},{3,2},{4,5},{5,4},{6,7},{7,6},{8,9},{9,8},{10,11... | collective-permute-start | bytes 1769480 | tf_op jit(solution)/shard_map/ppermute | solution.py:214
  21.0 22.0 %collective-permute-start.1 = (bf16[32,128]{1,0:T(8,128)(2,1)S(1)}, bf16[32,128]{1,0:T(8,128)(2,1)S(1)}, u32[]{:S(2)}, u32[]{:S(2)}) collective-permute-start(bf16[32,128]{1,0:T(8,128)(2,1)S(1)} %bitcast.17), channel_id=1, source_target_pairs={{0,0},{1,64},{2,128},{3,192},{4,256},{5,320},{6,384},{7,448},{8,8}... | collective-permute-start | bytes 24584 | tf_op jit(solution)/shard_map/ppermute | solution.py:36
  23.0 0.8 copy-start.2
  36.9 0.8 copy-start.3
  43.0 12.1 %copy-start.9 = (bf16[144,128]{1,0:T(8,128)(2,1)S(1)}, bf16[144,128]{1,0:T(8,128)(2,1)}, u32[]{:S(2)}) copy-start(bf16[144,128]{1,0:T(8,128)(2,1)} %get-tuple-element.19) | copy-start | bytes 110596
  43.9 30.3 %all-to-all-start.1 = ((bf16[64,32,128]{2,1,0:T(8,128)(2,1)}), bf16[64,32,128]{2,1,0:T(8,128)(2,1)S(1)}, u32[]{:S(2)}, u32[]{:S(2)}) async-start(bf16[64,32,128]{2,1,0:T(8,128)(2,1)} %broadcast_in_dim.14), calls=%async_computation.1 | async-start | bytes 1048576 | tf_op jit(solution)/shard_map/all_to_all | solution.py:24
  55.1 12.5 %collective-permute-start.2 = (bf16[144,128]{1,0:T(8,128)(2,1)S(1)}, bf16[144,128]{1,0:T(8,128)(2,1)S(1)}, u32[]{:S(2)}, u32[]{:S(2)}) collective-permute-start(bf16[144,128]{1,0:T(8,128)(2,1)S(1)} %copy-done.9), channel_id=1, source_target_pairs={{0,8},{8,16},{16,24},{24,32},{32,40},{40,48},{48,56},{56,64},{64,7... | collective-permute-start | bytes 110600 | tf_op jit(solution)/shard_map/ppermute | solution.py:247
  67.6 0.6 copy-start.8
  74.2 19.6 %copy-start.4 = (bf16[64,32,128]{2,1,0:T(8,128)(2,1)}, bf16[64,32,128]{2,1,0:T(8,128)(2,1)S(1)}, u32[]{:S(2)}) copy-start(bf16[64,32,128]{2,1,0:T(8,128)(2,1)S(1)} %all-to-all-done.1.own) | copy-start | bytes 1572868
  74.2 19.6 %all-to-all-start.2 = ((bf16[4,512,256]{2,1,0:T(8,128)(2,1)}), bf16[4,512,256]{2,1,0:T(8,128)(2,1)S(1)}, u32[]{:S(2)}, u32[]{:S(2)}) async-start(bf16[4,512,256]{2,1,0:T(8,128)(2,1)} %mix.1), calls=%async_computation.2 | async-start | bytes 2097152 | tf_op jit(solution)/shard_map/all_to_all | solution.py:270
  77.8 4.8 %collective-permute-start.3 = (bf16[64,32,128]{2,1,0:T(8,128)(2,1)S(1)}, bf16[64,32,128]{2,1,0:T(8,128)(2,1)S(1)}, u32[]{:S(2)}, u32[]{:S(2)}) collective-permute-start(bf16[64,32,128]{2,1,0:T(8,128)(2,1)S(1)} %all-to-all-done.1.own), channel_id=1, source_target_pairs={{0,1},{1,0},{2,3},{3,2},{4,5},{5,4},{6,7},{7,6},{8,9},{9,8},{10,11... | collective-permute-start | bytes 1572872 | tf_op jit(solution)/shard_map/ppermute | solution.py:269
  82.5 11.3 %copy-start.5 = (bf16[64,32,128]{2,1,0:T(8,128)(2,1)}, bf16[64,32,128]{2,1,0:T(8,128)(2,1)S(1)}, u32[]{:S(2)}) copy-start(bf16[64,32,128]{2,1,0:T(8,128)(2,1)S(1)} %collective-permute-done.3.other) | copy-start | bytes 1572868
  93.9 1.0 copy-start.1

commit v6 on v5

--- a/solution.py
+++ b/solution.py
@@ -214,6 +214,11 @@
     other = lax.ppermute(own, "c", [(0, 1), (1, 0)])
 
     cosine, sine = rope_tables(lax.axis_index(SP) * rows, rows)
+
+    exchanged, out_piece, cosine, sine, other = lax.optimization_barrier(
+        (exchanged, out_piece, cosine, sine, other)
+    )
+    own_cols = from_everyone(out_piece, SP)
 
     at = lambda *shape: lambda *place: pl.BlockSpec(shape, lambda i: place)
     whole = lambda *shape: pl.BlockSpec(shape, lambda i: (0,) * len(shape))
@@ -243,9 +248,8 @@
 
     pairs = [(2 * s, 2 * s + 2) for s in range(sp_count - 1)]
     pairs += [(2 * s + 3, 2 * s + 1) for s in range(sp_count - 1)]
-    out_piece, send = lax.optimization_barrier((out_piece, send))
     halo = lax.ppermute(send, SP + ("c",), pairs)
-    own_cols = from_everyone(out_piece, SP)
+    other_cols = lax.ppermute(own_cols, "c", [(0, 1), (1, 0)])
 
     peers_x = lax.axis_size("x")
     small_rows = at(EDGE, depth)(LANES // EDGE, 0)
@@ -265,8 +269,7 @@
         interpret=INTERPRET,
     )(own, other, query, kv, pool_in, halo)
 
-    local, own_cols = lax.optimization_barrier((local, own_cols))
-    other_cols = lax.ppermute(own_cols, "c", [(0, 1), (1, 0)])
+    local, other_cols = lax.optimization_barrier((local, other_cols))
     joined = lax.all_to_all(local, "x", 0, 0, tiled=True)
     pieces = out_piece.shape[0]
     width = 2 * peers // lax.axis_size("z") * pieces

time: 113 us -> 128 us (1.13)
  the two profiles are of different devices: /device:TPU:24 before, /device:TPU:1 now
where the time goes in v6:
time: 128 us; the launch traced here: 127 us
  blocking collectives  58.1 us (45%)
  starting transfers between devices  29.6 us (23%)
  Pallas kernels  21.1 us (16%)
  waiting for transfers between devices  13 us (10%)
  local copies, waits for them, and re-layouts  3.28 us (3%)
  other arithmetic  1.42 us (1%)
    all_to_all x1, blocking collectives, from_everyone(): lax.all_to_all(jnp.broadcast_to(x[None], (peers, *x.shape)), axis, 0, 0,...  27.1 us
    all_to_all x1, blocking collectives, body(): joined = lax.all_to_all(local, 'x', 0, 0, tiled=True)  19.2 us
    all_to_all x1, starting transfers between devices, from_everyone(): lax.all_to_all(jnp.broadcast_to(x[None], (peers, *x.shape)), axis, 0, 0,...  17.3 us
    all_to_all x1, blocking collectives, body(): lax.all_to_all(partial_cols, 'x', split_axis=0, concat_axis=1, tiled=True)  11.8 us
    all_to_all x1, waiting for transfers between devices, from_everyone(): lax.all_to_all(jnp.broadcast_to(x[None], (peers, *x.shape)), axis, 0, 0,...  8.01 us
    pallas_call x1, Pallas kernels, body(): pl.pallas_call(project, grid=(rows // ROWS,), in_specs=[part(ROWS, depth)...  7.39 us
    pallas_call x1, Pallas kernels, body(): pl.pallas_call(project_kv, grid=(rows // ROWS,), in_specs=[part(ROWS, dep...  5.41 us
    pallas_call x1, Pallas kernels, body(): pl.pallas_call(mix, grid=(peers_x,), in_specs=[small_rows, small_rows] +...  5.24 us
  transfers between devices with their start and end apart: 5, of which 3 were waited for; matrix products, arithmetic and copies ran while one was open for 1% of the time, Pallas kernels for 14%

profile of v6, /device:TPU:1, one launch (start us, length us, event | category | flops | bytes accessed | tf_op | source)
XLA Modules:
  0.0 127.3 jit_solution(9438676576332045585)
XLA Ops:
  0.0 0.8 constant_dynamic-slice_fusion
  0.9 0.1 pad_maximum_fusion.1
  1.0 0.9 broadcast_in_dim.12
  1.8 17.3 %all-to-all-start = ((bf16[64,32,128]{2,1,0:T(8,128)(2,1)}), bf16[64,32,128]{2,1,0:T(8,128)(2,1)S(1)}, u32[]{:S(2)}, u32[]{:S(2)}) async-start(bf16[64,32,128]{2,1,0:T(8,128)(2,1)} %broadcast_in_dim.12), calls=%async_computation | async-start | bytes 1048576 | tf_op jit(solution)/shard_map/all_to_all | solution.py:24
  19.9 2.9 %collective-permute-start.1 = (bf16[144,2048]{1,0:T(8,128)(2,1)S(1)}, bf16[144,2048]{1,0:T(8,128)(2,1)S(1)}, u32[]{:S(2)}, u32[]{:S(2)}) collective-permute-start(bf16[144,2048]{1,0:T(8,128)(2,1)S(1)} %pad_maximum_fusion.own), channel_id=1, source_target_pairs={{0,1},{1,0},{2,3},{3,2},{4,5},{5,4},{6,7},{7,6},{8,9},{9,8},{10,11... | collective-permute-start | bytes 1769480 | tf_op jit(solution)/shard_map/ppermute | solution.py:214
  22.8 3.1 %collective-permute-start = (bf16[32,128]{1,0:T(8,128)(2,1)S(1)}, bf16[32,128]{1,0:T(8,128)(2,1)S(1)}, u32[]{:S(2)}, u32[]{:S(2)}) collective-permute-start(bf16[32,128]{1,0:T(8,128)(2,1)S(1)} %bitcast.17), channel_id=1, source_target_pairs={{0,0},{1,64},{2,128},{3,192},{4,256},{5,320},{6,384},{7,448},{8,8}... | collective-permute-start | bytes 24584 | tf_op jit(solution)/shard_map/ppermute | solution.py:36
  25.9 1.3 multiply_sine_fusion
  27.2 1.3 %collective-permute-done = bf16[32,128]{1,0:T(8,128)(2,1)S(1)} collective-permute-done((bf16[32,128]{1,0:T(8,128)(2,1)S(1)}, bf16[32,128]{1,0:T(8,128)(2,1)S(1)}, u32[]{:S(2)}, u32[]{:S(2)}) %collective-permute-start) | collective-permute-done | bytes 8224 | tf_op jit(solution)/shard_map/ppermute | solution.py:36
  28.5 0.0 collective-permute-done.1.other
  28.5 8.0 %all-to-all-done.ex = bf16[64,32,128]{2,1,0:T(8,128)(2,1)S(1)} async-done(((bf16[64,32,128]{2,1,0:T(8,128)(2,1)}), bf16[64,32,128]{2,1,0:T(8,128)(2,1)S(1)}, u32[]{:S(2)}, u32[]{:S(2)}) %all-to-all-start) | async-done | bytes 524320 | tf_op jit(solution)/shard_map/all_to_all | solution.py:24
  36.5 0.1 broadcast_in_dim.14
  36.6 27.1 %all_to_all.34.own = bf16[64,32,128]{2,1,0:T(8,128)(2,1)S(1)} all-to-all(bf16[64,32,128]{2,1,0:T(8,128)(2,1)S(1)} %broadcast_in_dim.14), channel_id=1, replica_groups=mesh['z'=8,'y'=8,'x'=4,'c'=2] {'z','y'}, dimensions={0} | all-to-all | bytes 1048576 | tf_op jit(solution)/shard_map/all_to_all | solution.py:24
  63.6 5.1 %collective-permute-start.3 = (bf16[64,32,128]{2,1,0:T(8,128)(2,1)S(1)}, bf16[64,32,128]{2,1,0:T(8,128)(2,1)S(1)}, u32[]{:S(2)}, u32[]{:S(2)}) collective-permute-start(bf16[64,32,128]{2,1,0:T(8,128)(2,1)S(1)} %all_to_all.34.own), channel_id=1, source_target_pairs={{0,1},{1,0},{2,3},{3,2},{4,5},{5,4},{6,7},{7,6},{8,9},{9,8},{10,11... | collective-permute-start | bytes 1572872 | tf_op jit(solution)/shard_map/ppermute | solution.py:252
  68.7 7.4 %project.1 = (bf16[1024,2048]{1,0:T(8,128)(2,1)}, bf16[1024,128]{1,0:T(8,128)(2,1)}, bf16[1024,128]{1,0:T(8,128)(2,1)}) custom-call(bf16[1024,2048]{1,0:T(8,128)(2,1)} %tokens.1, f32[1,2048]{1,0:T(1,128)} %bitcast.16, bf16[144,2048]{1,0:T(8,128)(2,1)} %copy-done, bf16[144,2048]{1,0:T(8,128)(2,1)} %copy-done.1, f32[32,1024]{1,0:T(8,128)} %get-tuple-element.18.cosine, ...), custom_call_target="tpu_custom_call" | custom-call | tf_op jit(solution)/shard_map/project/pallas_call | solution.py:229
  76.1 5.4 %project_kv.1 = (bf16[1024,128]{1,0:T(8,128)(2,1)}, bf16[144,128]{1,0:T(8,128)(2,1)}) custom-call(bf16[1024,2048]{1,0:T(8,128)(2,1)} %get-tuple-element.21.normed, bf16[1024,128]{1,0:T(8,128)(2,1)} %get-tuple-element.22.pool, bf16[64,32,128]{2,1,0:T(8,128)(2,1)} %copy-done.2, f32[32,1024]{1,0:T(8,128)} %get-tuple-element.18.cosine, ...), custom_call_target="tpu_custom_call" | custom-call | tf_op jit(solution)/shard_map/project_kv/pallas_call | solution.py:239
  81.6 1.3 %collective-permute-start.2 = (bf16[144,128]{1,0:T(8,128)(2,1)}, bf16[144,128]{1,0:T(8,128)(2,1)S(1)}, u32[]{:S(2)}, u32[]{:S(2)}) collective-permute-start(bf16[144,128]{1,0:T(8,128)(2,1)} %get-tuple-element.25), channel_id=1, source_target_pairs={{0,8},{8,16},{16,24},{24,32},{32,40},{40,48},{48,56},{56,64},{64,7... | collective-permute-start | bytes 110600 | tf_op jit(solution)/shard_map/ppermute | solution.py:251
  82.8 3.6 %collective-permute-done.2.halo = bf16[144,128]{1,0:T(8,128)(2,1)S(1)} collective-permute-done((bf16[144,128]{1,0:T(8,128)(2,1)}, bf16[144,128]{1,0:T(8,128)(2,1)S(1)}, u32[]{:S(2)}, u32[]{:S(2)}) %collective-permute-start.2) | collective-permute-done | bytes 36896 | tf_op jit(solution)/shard_map/ppermute | solution.py:251
  86.5 0.6 copy-done.7
  87.1 5.2 %mix.1 = bf16[4,512,256]{2,1,0:T(8,128)(2,1)} custom-call(bf16[144,2048]{1,0:T(8,128)(2,1)} %copy-done, bf16[144,2048]{1,0:T(8,128)(2,1)} %copy-done.1, bf16[1024,128]{1,0:T(8,128)(2,1)} %get-tuple-element.20.q, bf16[1024,128]{1,0:T(8,128)(2,1)} %get-tuple-element.24.kv, bf16[1024,128]{1,0:T(8,128)(2,1)} %get-tuple-element.22.pool, bf16[144,128]{1,0:T(8,128)(2,1)} %copy-done.7), custom_call_target="tpu_custom_call" | custom-call | tf_op jit(solution)/shard_map/mix/pallas_call | solution.py:256
  92.3 0.0 collective-permute-done.3.other
  92.3 19.2 %all_to_all.35.joined = bf16[4,512,256]{2,1,0:T(8,128)(2,1)} all-to-all(bf16[4,512,256]{2,1,0:T(8,128)(2,1)} %mix.1), channel_id=1, replica_groups=mesh['z'=8,'y'=8,'x'=4,'c'=2] {'x'}, dimensions={0} | all-to-all | bytes 2097152 | tf_op jit(solution)/shard_map/all_to_all | solution.py:273
  111.5 3.0 %output_product.1 = bf16[512,512]{1,0:T(8,128)(2,1)} custom-call(bf16[4,512,256]{2,1,0:T(8,128)(2,1)} %all_to_all.35.joined, bf16[64,32,128]{2,1,0:T(8,128)(2,1)} %copy-done.3, bf16[64,32,128]{2,1,0:T(8,128)(2,1)} %copy-done.4), custom_call_target="tpu_custom_call" | custom-call | tf_op jit(solution)/shard_map/output_product/pallas_call | solution.py:276
  114.6 11.8 %all_to_all.36 = bf16[4,128,512]{2,1,0:T(8,128)(2,1)S(1)} all-to-all(bf16[4,128,512]{2,1,0:T(8,128)(2,1)} %bitcast.12), channel_id=1, replica_groups=mesh['z'=8,'y'=8,'x'=4,'c'=2] {'x'}, dimensions={0} | all-to-all | bytes 1048576 | tf_op jit(solution)/shard_map/all_to_all | solution.py:285
  126.4 0.8 copy.11
  (25 shorter events, 0.1 us)
Async XLA Ops:
  0.0 19.7 %copy-start.9 = (f32[64]{0:T(128)S(1)}, f32[64]{0:T(128)}, u32[]{:S(2)}) copy-start(f32[64]{0:T(128)} %param.16) | copy-start | bytes 772
  0.0 19.8 %copy-start.5 = (bf16[2048,64]{0,1:T(8,128)(2,1)S(1)}, bf16[2048,64]{0,1:T(8,128)(2,1)}, u32[]{:S(2)}) copy-start(bf16[2048,64]{0,1:T(8,128)(2,1)} %param.14) | copy-start | bytes 786436
  0.0 19.8 %copy-start.6 = (bf16[2048,64]{0,1:T(8,128)(2,1)S(1)}, bf16[2048,64]{0,1:T(8,128)(2,1)}, u32[]{:S(2)}) copy-start(bf16[2048,64]{0,1:T(8,128)(2,1)} %param.11) | copy-start | bytes 786436
  1.8 20.9 %copy-start.8 = (bf16[128,32]{0,1:T(8,128)(2,1)S(1)}, bf16[128,32]{0,1:T(8,128)(2,1)}, u32[]{:S(2)}) copy-start(bf16[128,32]{0,1:T(8,128)(2,1)} %param.17) | copy-start | bytes 24580
  1.8 34.7 %all-to-all-start = ((bf16[64,32,128]{2,1,0:T(8,128)(2,1)}), bf16[64,32,128]{2,1,0:T(8,128)(2,1)S(1)}, u32[]{:S(2)}, u32[]{:S(2)}) async-start(bf16[64,32,128]{2,1,0:T(8,128)(2,1)} %broadcast_in_dim.12), calls=%async_computation | async-start | bytes 1048576 | tf_op jit(solution)/shard_map/all_to_all | solution.py:24
  19.9 48.9 %copy-start = (bf16[144,2048]{1,0:T(8,128)(2,1)}, bf16[144,2048]{1,0:T(8,128)(2,1)S(1)}, u32[]{:S(2)}) copy-start(bf16[144,2048]{1,0:T(8,128)(2,1)S(1)} %pad_maximum_fusion.own) | copy-start | bytes 1769476
  19.9 8.6 %collective-permute-start.1 = (bf16[144,2048]{1,0:T(8,128)(2,1)S(1)}, bf16[144,2048]{1,0:T(8,128)(2,1)S(1)}, u32[]{:S(2)}, u32[]{:S(2)}) collective-permute-start(bf16[144,2048]{1,0:T(8,128)(2,1)S(1)} %pad_maximum_fusion.own), channel_id=1, source_target_pairs={{0,1},{1,0},{2,3},{3,2},{4,5},{5,4},{6,7},{7,6},{8,9},{9,8},{10,11... | collective-permute-start | bytes 1769480 | tf_op jit(solution)/shard_map/ppermute | solution.py:214
  22.8 5.7 %collective-permute-start = (bf16[32,128]{1,0:T(8,128)(2,1)S(1)}, bf16[32,128]{1,0:T(8,128)(2,1)S(1)}, u32[]{:S(2)}, u32[]{:S(2)}) collective-permute-start(bf16[32,128]{1,0:T(8,128)(2,1)S(1)} %bitcast.17), channel_id=1, source_target_pairs={{0,0},{1,64},{2,128},{3,192},{4,256},{5,320},{6,384},{7,448},{8,8}... | collective-permute-start | bytes 24584 | tf_op jit(solution)/shard_map/ppermute | solution.py:36
  28.5 40.2 %copy-start.1 = (bf16[144,2048]{1,0:T(8,128)(2,1)}, bf16[144,2048]{1,0:T(8,128)(2,1)S(1)}, u32[]{:S(2)}) copy-start(bf16[144,2048]{1,0:T(8,128)(2,1)S(1)} %collective-permute-done.1.other) | copy-start | bytes 1769476
  36.5 39.6 %copy-start.2 = (bf16[64,32,128]{2,1,0:T(8,128)(2,1)}, bf16[64,32,128]{2,1,0:T(8,128)(2,1)S(1)}, u32[]{:S(2)}) copy-start(bf16[64,32,128]{2,1,0:T(8,128)(2,1)S(1)} %all-to-all-done.ex) | copy-start | bytes 1572868
  63.6 12.5 %copy-start.3 = (bf16[64,32,128]{2,1,0:T(8,128)(2,1)}, bf16[64,32,128]{2,1,0:T(8,128)(2,1)S(1)}, u32[]{:S(2)}) copy-start(bf16[64,32,128]{2,1,0:T(8,128)(2,1)S(1)} %all_to_all.34.own) | copy-start | bytes 1572868
  63.6 28.7 %collective-permute-start.3 = (bf16[64,32,128]{2,1,0:T(8,128)(2,1)S(1)}, bf16[64,32,128]{2,1,0:T(8,128)(2,1)S(1)}, u32[]{:S(2)}, u32[]{:S(2)}) collective-permute-start(bf16[64,32,128]{2,1,0:T(8,128)(2,1)S(1)} %all_to_all.34.own), channel_id=1, source_target_pairs={{0,1},{1,0},{2,3},{3,2},{4,5},{5,4},{6,7},{7,6},{8,9},{9,8},{10,11... | collective-permute-start | bytes 1572872 | tf_op jit(solution)/shard_map/ppermute | solution.py:252
  81.6 4.9 %collective-permute-start.2 = (bf16[144,128]{1,0:T(8,128)(2,1)}, bf16[144,128]{1,0:T(8,128)(2,1)S(1)}, u32[]{:S(2)}, u32[]{:S(2)}) collective-permute-start(bf16[144,128]{1,0:T(8,128)(2,1)} %get-tuple-element.25), channel_id=1, source_target_pairs={{0,8},{8,16},{16,24},{24,32},{32,40},{40,48},{48,56},{56,64},{64,7... | collective-permute-start | bytes 110600 | tf_op jit(solution)/shard_map/ppermute | solution.py:251
  86.5 0.6 copy-start.7
  92.3 19.2 %copy-start.4 = (bf16[64,32,128]{2,1,0:T(8,128)(2,1)}, bf16[64,32,128]{2,1,0:T(8,128)(2,1)S(1)}, u32[]{:S(2)}) copy-start(bf16[64,32,128]{2,1,0:T(8,128)(2,1)S(1)} %collective-permute-done.3.other) | copy-start | bytes 1572868

commit v7 on v5

--- a/solution.py
+++ b/solution.py
@@ -11,6 +11,7 @@
 QB = 128
 LANES = 128
 ROWS = 256
+STEP = 2
 EDGE = 16
 POOL_SPANS = (2, 4, 8, 16)
 NEG_BIG = -1e30
@@ -108,7 +109,6 @@
 
 def mix(own, other, q, kv, pool, halo, out, kv_wide, pool_wide):
     core, group = lax.axis_index("c"), lax.axis_index("x")
-    i = pl.program_id(0)
     rows = q.shape[0]
     blocks_total = lax.axis_size(SP) * (rows // QB)
     first_block = lax.axis_index(SP) * (rows // QB)
@@ -118,7 +118,7 @@
     second = jnp.where(core == 0, theirs, mine)
     scale = jnp.concatenate([first[:, :HEAD], second[:, :HEAD]], axis=1)
 
-    @pl.when(i == 0)
+    @pl.when(pl.program_id(0) == 0)
     def _():
         kv_wide[pl.ds(pl.multiple_of((1 - core) * QB, QB), rows), :] = kv[...]
         kv_wide[pl.ds(pl.multiple_of(core * rows, QB), QB), :] = halo[:QB, :]
@@ -134,64 +134,45 @@
     upper = lax.broadcasted_iota(jnp.int32, (2 * QB, 1), 0) < QB
     sinks = jnp.where(upper, first[:, HEAD : HEAD + 1], second[:, HEAD : HEAD + 1])
     half = lax.shift_left(1, group)
-    start = pl.multiple_of(core * QB + 2 * QB * i, QB)
-    block = first_block + core + 2 * i
-    pair = q[pl.ds(start, QB), :]
-    zero = jnp.zeros_like(pair)
-    lower_head = jnp.where(lane < HEAD, pair, zero)
-    upper_head = jnp.concatenate([pair[:, HEAD:], zero[:, HEAD:]], axis=1)
-    queries = jnp.concatenate([lower_head, upper_head], axis=0)
-    keys = kv_wide[pl.ds(pl.multiple_of(2 * QB * i, QB), 3 * QB), :]
-    scores = lax.dot_general(
-        queries, keys, (((1,), (1,)), ((), ())), preferred_element_type=jnp.float32
-    )
-    least = jnp.where(block == 0, QB, 0)
-    limit = jnp.where(block == blocks_total - 1, 2 * QB, 3 * QB)
-    valid = near & (column >= least) & (column < limit)
-    scores = jnp.where(valid, scores, NEG_BIG)
-    top = jnp.maximum(jnp.max(scores, axis=-1, keepdims=True), sinks)
-    expo = jnp.where(valid, jnp.exp(scores - top), 0.0)
-    total = jnp.sum(expo, axis=-1, keepdims=True) + jnp.exp(sinks - top)
-    weights = (expo / total).astype(jnp.bfloat16)
-    mixed = jnp.dot(weights, keys, preferred_element_type=jnp.float32)
-    attended = jnp.concatenate([mixed[:QB, HEAD:], mixed[QB:, HEAD:]], axis=1)
-
-    near_rows = pool_wide[pl.ds(start, QB + 2 * EDGE), :]
-    size = QB + 2 * EDGE
-    sums = near_rows + pltpu.roll(near_rows, 1, 0)
-    chosen = sums
-    for index in range(1, len(POOL_SPANS)):
-        step = POOL_SPANS[index] // 4
-        sums = pltpu.roll(sums, step, 0) + pltpu.roll(sums, size - step, 0)
-        chosen = jnp.where(group == index, sums, chosen)
-    position = block * QB + lax.broadcasted_iota(jnp.int32, (QB, 1), 0)
-    counted = jnp.minimum(position + half, blocks_total * QB) - jnp.maximum(position - half, 0)
-    mean = chosen[EDGE : EDGE + QB] / counted.astype(jnp.float32)
-    pooled = (mean - near_rows[EDGE : EDGE + QB]) * scale
-    both = jnp.concatenate([attended, pooled], axis=1).astype(jnp.bfloat16)
-    for peer in range(out.shape[0]):
-        out[peer] = both
-
-
-def output_product(joined, own, other, out):
-    core = lax.axis_index("c")
-    peers = joined.shape[0]
-
-    def product(columns):
-        columns = columns.reshape(2 * peers, -1, LANES)
-        total = None
-        for i in range(peers):
-            weights = jnp.concatenate([columns[i], columns[peers + i]], axis=1)
-            part = lax.dot_general(
-                joined[i], weights, (((1,), (1,)), ((), ())), preferred_element_type=jnp.float32
-            )
-            total = part if total is None else total + part
-        return total.astype(jnp.bfloat16)
-
-    mine, theirs = product(own[...]), product(other[...])
-    out[...] = jnp.concatenate(
-        [jnp.where(core == 0, mine, theirs), jnp.where(core == 0, theirs, mine)], axis=1
-    )
+    for j in range(STEP):
+        i = pl.program_id(0) * STEP + j
+        start = pl.multiple_of(core * QB + 2 * QB * i, QB)
+        block = first_block + core + 2 * i
+        pair = q[pl.ds(start, QB), :]
+        zero = jnp.zeros_like(pair)
+        lower_head = jnp.where(lane < HEAD, pair, zero)
+        upper_head = jnp.concatenate([pair[:, HEAD:], zero[:, HEAD:]], axis=1)
+        queries = jnp.concatenate([lower_head, upper_head], axis=0)
+        keys = kv_wide[pl.ds(pl.multiple_of(2 * QB * i, QB), 3 * QB), :]
+        scores = lax.dot_general(
+            queries, keys, (((1,), (1,)), ((), ())), preferred_element_type=jnp.float32
+        )
+        least = jnp.where(block == 0, QB, 0)
+        limit = jnp.where(block == blocks_total - 1, 2 * QB, 3 * QB)
+        valid = near & (column >= least) & (column < limit)
+        scores = jnp.where(valid, scores, NEG_BIG)
+        top = jnp.maximum(jnp.max(scores, axis=-1, keepdims=True), sinks)
+        expo = jnp.where(valid, jnp.exp(scores - top), 0.0)
+        total = jnp.sum(expo, axis=-1, keepdims=True) + jnp.exp(sinks - top)
+        weights = (expo / total).astype(jnp.bfloat16)
+        mixed = jnp.dot(weights, keys, preferred_element_type=jnp.float32)
+        attended = jnp.concatenate([mixed[:QB, HEAD:], mixed[QB:, HEAD:]], axis=1)
+
+        near_rows = pool_wide[pl.ds(start, QB + 2 * EDGE), :]
+        size = QB + 2 * EDGE
+        sums = near_rows + pltpu.roll(near_rows, 1, 0)
+        chosen = sums
+        for index in range(1, len(POOL_SPANS)):
+            step = POOL_SPANS[index] // 4
+            sums = pltpu.roll(sums, step, 0) + pltpu.roll(sums, size - step, 0)
+            chosen = jnp.where(group == index, sums, chosen)
+        position = block * QB + lax.broadcasted_iota(jnp.int32, (QB, 1), 0)
+        counted = jnp.minimum(position + half, blocks_total * QB) - jnp.maximum(position - half, 0)
+        mean = chosen[EDGE : EDGE + QB] / counted.astype(jnp.float32)
+        pooled = (mean - near_rows[EDGE : EDGE + QB]) * scale
+        both = jnp.concatenate([attended, pooled], axis=1).astype(jnp.bfloat16)
+        for peer in range(out.shape[0]):
+            out[peer, j * QB : (j + 1) * QB] = both
 
 
 def body(tokens, norm_gain, w_query, w_key, w_value, w_pool_in, sink_logit, pool_scale, w_out):
@@ -231,6 +212,8 @@
         name="project",
         interpret=INTERPRET,
     )(tokens, norm_gain[None, :], own, other, cosine, sine)
+    exchanged, out_piece, normed = lax.optimization_barrier((exchanged, out_piece, normed))
+    own_cols = from_everyone(out_piece, SP)
     kv, send = pl.pallas_call(
         project_kv,
         grid=(rows // ROWS,),
@@ -243,19 +226,16 @@
 
     pairs = [(2 * s, 2 * s + 2) for s in range(sp_count - 1)]
     pairs += [(2 * s + 3, 2 * s + 1) for s in range(sp_count - 1)]
-    out_piece, send = lax.optimization_barrier((out_piece, send))
     halo = lax.ppermute(send, SP + ("c",), pairs)
-    own_cols = from_everyone(out_piece, SP)
-
     peers_x = lax.axis_size("x")
     small_rows = at(EDGE, depth)(LANES // EDGE, 0)
     local = pl.pallas_call(
         mix,
-        grid=(peers_x,),
+        grid=(rows // (2 * QB * STEP),),
         in_specs=[small_rows, small_rows]
         + [whole(rows, LANES)] * 3
         + [whole(QB + EDGE, LANES)],
-        out_specs=pl.BlockSpec((peers_x, QB, 2 * LANES), lambda i: (0, i, 0)),
+        out_specs=pl.BlockSpec((peers_x, STEP * QB, 2 * LANES), lambda i: (0, i, 0)),
         out_shape=shaped(peers_x, rows // 2, 2 * LANES),
         scratch_shapes=[
             pltpu.VMEM((rows + QB, LANES), bf16),
@@ -268,17 +248,19 @@
     local, own_cols = lax.optimization_barrier((local, own_cols))
     other_cols = lax.ppermute(own_cols, "c", [(0, 1), (1, 0)])
     joined = lax.all_to_all(local, "x", 0, 0, tiled=True)
-    pieces = out_piece.shape[0]
-    width = 2 * peers // lax.axis_size("z") * pieces
-    partial_cols = pl.pallas_call(
-        output_product,
-        grid=(1,),
-        in_specs=[whole(*joined.shape)] + [whole(peers, pieces, LANES)] * 2,
-        out_specs=whole(rows // 2, width),
-        out_shape=shaped(rows // 2, width),
-        name="output_product",
-        interpret=INTERPRET,
-    )(joined, own_cols, other_cols)
+
+    def matched(columns):
+        columns = columns.reshape(2, peers_x, -1, LANES)
+        return jnp.concatenate([columns[0], columns[1]], axis=2)
+
+    core = lax.axis_index("c")
+    mine, theirs = matched(own_cols), matched(other_cols)
+    columns = jnp.concatenate(
+        [jnp.where(core == 0, mine, theirs), jnp.where(core == 0, theirs, mine)], axis=1
+    )
+    partial_cols = jnp.einsum(
+        "ptc,pnc->tn", joined, columns, preferred_element_type=jnp.float32
+    ).astype(bf16)
     return lax.all_to_all(partial_cols, "x", split_axis=0, concat_axis=1, tiled=True)
 
 

time: 113 us -> 106 us (0.938)
  the two profiles are of different devices: /device:TPU:24 before, /device:TPU:1 now
where the time goes in v7:
time: 106 us; the launch traced here: 105 us
  starting transfers between devices  45.7 us (43%)
  waiting for transfers between devices  20.6 us (19%)
  Pallas kernels  17.8 us (17%)
  blocking collectives  11 us (10%)
  local copies, waits for them, and re-layouts  5.68 us (5%)
  other arithmetic  2.71 us (3%)
    all_to_all x2, starting transfers between devices, from_everyone(): lax.all_to_all(jnp.broadcast_to(x[None], (peers, *x.shape)), axis, 0, 0,...  31 us
    all_to_all x1, waiting for transfers between devices, body(): joined = lax.all_to_all(local, 'x', 0, 0, tiled=True)  14.8 us
    all_to_all x1, blocking collectives, body(): lax.all_to_all(partial_cols, 'x', split_axis=0, concat_axis=1, tiled=True)  11 us
    pallas_call x1, Pallas kernels, body(): pl.pallas_call(project, grid=(rows // ROWS,), in_specs=[part(ROWS, depth)...  7.36 us
    ppermute x1, waiting for transfers between devices, body(): halo = lax.ppermute(send, SP + ('c',), pairs)  5.86 us
    pallas_call x1, Pallas kernels, body(): pl.pallas_call(project_kv, grid=(rows // ROWS,), in_specs=[part(ROWS, dep...  5.39 us
    pallas_call x1, Pallas kernels, body(): pl.pallas_call(mix, grid=(rows // (2 * QB * STEP),), in_specs=[small_rows...  5.07 us
    ppermute x1, starting transfers between devices, body(): other_cols = lax.ppermute(own_cols, 'c', [(0, 1), (1, 0)])  3.94 us
  transfers between devices with their start and end apart: 7, of which 2 were waited for; matrix products, arithmetic and copies ran while one was open for 3% of the time, Pallas kernels for 17%

profile of v7, /device:TPU:1, one launch (start us, length us, event | category | flops | bytes accessed | tf_op | source)
XLA Modules:
  0.0 105.0 jit_solution(8884800710365550621)
XLA Ops:
  0.0 0.8 constant_dynamic-slice_fusion
  0.9 0.9 broadcast_in_dim.13
  1.8 17.1 %all-to-all-start = ((bf16[64,32,128]{2,1,0:T(8,128)(2,1)}), bf16[64,32,128]{2,1,0:T(8,128)(2,1)S(1)}, u32[]{:S(2)}, u32[]{:S(2)}) async-start(bf16[64,32,128]{2,1,0:T(8,128)(2,1)} %broadcast_in_dim.13), calls=%async_computation | async-start | bytes 1048576 | tf_op jit(solution)/shard_map/all_to_all | solution.py:25
  19.5 0.7 pad_bitcast_fusion
  20.2 1.1 %pad_maximum_fusion.own = bf16[144,2048]{1,0:T(8,128)(2,1)S(1)} fusion(bf16[16,2048]{1,0:T(8,128)(2,1)S(1)} %fusion.12, bf16[64,2048]{1,0:T(8,128)(2,1)} %bitcast.27, bf16[64,2048]{1,0:T(8,128)(2,1)} %bitcast.28), kind=kLoop, calls=%fused_computation.5 | loop fusion | flops 1769472 | bytes 1179648 | tf_op jit(solution)/shard_map/concatenate | solution.py:194
  21.3 2.9 %collective-permute-start = (bf16[144,2048]{1,0:T(8,128)(2,1)S(1)}, bf16[144,2048]{1,0:T(8,128)(2,1)S(1)}, u32[]{:S(2)}, u32[]{:S(2)}) collective-permute-start(bf16[144,2048]{1,0:T(8,128)(2,1)S(1)} %pad_maximum_fusion.own), channel_id=1, source_target_pairs={{0,1},{1,0},{2,3},{3,2},{4,5},{5,4},{6,7},{7,6},{8,9},{9,8},{10,11... | collective-permute-start | bytes 1769480 | tf_op jit(solution)/shard_map/ppermute | solution.py:195
  24.2 3.1 %collective-permute-start.1 = (bf16[32,128]{1,0:T(8,128)(2,1)S(1)}, bf16[32,128]{1,0:T(8,128)(2,1)S(1)}, u32[]{:S(2)}, u32[]{:S(2)}) collective-permute-start(bf16[32,128]{1,0:T(8,128)(2,1)S(1)} %bitcast.30), channel_id=1, source_target_pairs={{0,0},{1,64},{2,128},{3,192},{4,256},{5,320},{6,384},{7,448},{8,8}... | collective-permute-start | bytes 24584 | tf_op jit(solution)/shard_map/ppermute | solution.py:37
  27.3 1.3 %multiply_sine_fusion = (f32[32,1024]{1,0:T(8,128)}, f32[32,1024]{1,0:T(8,128)}) fusion(f32[32]{0:T(128)S(1)} %multiply_power_fusion, f32[1024]{0:T(1024)S(1)} %add_convert_fusion), kind=kLoop, calls=%fused_computation.10 | loop fusion | flops 32768 | bytes 266368 | tf_op jit(solution)/shard_map/sin | solution.py:52
  28.6 0.8 copy-done.1
  29.4 7.4 %project.1 = (bf16[1024,2048]{1,0:T(8,128)(2,1)}, bf16[1024,128]{1,0:T(8,128)(2,1)}, bf16[1024,128]{1,0:T(8,128)(2,1)}) custom-call(bf16[1024,2048]{1,0:T(8,128)(2,1)} %tokens.1, f32[1,2048]{1,0:T(1,128)} %bitcast.29, bf16[144,2048]{1,0:T(8,128)(2,1)} %copy-done, bf16[144,2048]{1,0:T(8,128)(2,1)} %copy-done.1, f32[32,1024]{1,0:T(8,128)} %get-tuple-element.32.cosine, ...), custom_call_target="tpu_custom_call" | custom-call | tf_op jit(solution)/shard_map/project/pallas_call | solution.py:205
  36.8 1.0 broadcast_in_dim.14
  37.8 13.8 %all-to-all-start.1 = ((bf16[64,32,128]{2,1,0:T(8,128)(2,1)}), bf16[64,32,128]{2,1,0:T(8,128)(2,1)S(1)}, u32[]{:S(2)}, u32[]{:S(2)}) async-start(bf16[64,32,128]{2,1,0:T(8,128)(2,1)} %broadcast_in_dim.14), calls=%async_computation.1 | async-start | bytes 1048576 | tf_op jit(solution)/shard_map/all_to_all | solution.py:25
  51.6 5.4 %project_kv.1 = (bf16[1024,128]{1,0:T(8,128)(2,1)}, bf16[144,128]{1,0:T(8,128)(2,1)}) custom-call(bf16[1024,2048]{1,0:T(8,128)(2,1)} %get-tuple-element.17.normed, bf16[1024,128]{1,0:T(8,128)(2,1)} %get-tuple-element.18.pool, bf16[64,32,128]{2,1,0:T(8,128)(2,1)} %copy-done.2, f32[32,1024]{1,0:T(8,128)} %get-tuple-element.32.cosine, ...), custom_call_target="tpu_custom_call" | custom-call | tf_op jit(solution)/shard_map/project_kv/pallas_call | solution.py:217
  57.0 1.3 %collective-permute-start.2 = (bf16[144,128]{1,0:T(8,128)(2,1)}, bf16[144,128]{1,0:T(8,128)(2,1)S(1)}, u32[]{:S(2)}, u32[]{:S(2)}) collective-permute-start(bf16[144,128]{1,0:T(8,128)(2,1)} %get-tuple-element.21), channel_id=1, source_target_pairs={{0,8},{8,16},{16,24},{24,32},{32,40},{40,48},{48,56},{56,64},{64,7... | collective-permute-start | bytes 110600 | tf_op jit(solution)/shard_map/ppermute | solution.py:229
  58.3 5.9 %collective-permute-done.2.halo = bf16[144,128]{1,0:T(8,128)(2,1)S(1)} collective-permute-done((bf16[144,128]{1,0:T(8,128)(2,1)}, bf16[144,128]{1,0:T(8,128)(2,1)S(1)}, u32[]{:S(2)}, u32[]{:S(2)}) %collective-permute-start.2) | collective-permute-done | bytes 36896 | tf_op jit(solution)/shard_map/ppermute | solution.py:229
  64.2 0.6 copy-done.3
  64.8 5.1 %mix.1 = bf16[4,512,256]{2,1,0:T(8,128)(2,1)} custom-call(bf16[144,2048]{1,0:T(8,128)(2,1)} %copy-done, bf16[144,2048]{1,0:T(8,128)(2,1)} %copy-done.1, bf16[1024,128]{1,0:T(8,128)(2,1)} %get-tuple-element.15.q, bf16[1024,128]{1,0:T(8,128)(2,1)} %get-tuple-element.20.kv, bf16[1024,128]{1,0:T(8,128)(2,1)} %get-tuple-element.18.pool, bf16[144,128]{1,0:T(8,128)(2,1)} %copy-done.3), custom_call_target="tpu_custom_call" | custom-call | tf_op jit(solution)/shard_map/mix/pallas_call | solution.py:232
  69.9 3.9 %collective-permute-start.3 = (bf16[64,32,128]{2,1,0:T(8,128)(2,1)S(1)}, bf16[64,32,128]{2,1,0:T(8,128)(2,1)S(1)}, u32[]{:S(2)}, u32[]{:S(2)}) collective-permute-start(bf16[64,32,128]{2,1,0:T(8,128)(2,1)S(1)} %all-to-all-done.1), channel_id=1, source_target_pairs={{0,1},{1,0},{2,3},{3,2},{4,5},{5,4},{6,7},{7,6},{8,9},{9,8},{10,11... | collective-permute-start | bytes 1572872 | tf_op jit(solution)/shard_map/ppermute | solution.py:249
  73.8 3.5 %all-to-all-start.2 = ((bf16[4,512,256]{2,1,0:T(8,128)(2,1)}), bf16[4,512,256]{2,1,0:T(8,128)(2,1)S(1)}, u32[]{:S(2)}, u32[]{:S(2)}) async-start(bf16[4,512,256]{2,1,0:T(8,128)(2,1)} %mix.1), calls=%async_computation.2 | async-start | bytes 2097152 | tf_op jit(solution)/shard_map/all_to_all | solution.py:250
  77.5 0.3 broadcast_select_fusion.1
  77.7 14.8 %all-to-all-done.2 = bf16[4,512,256]{2,1,0:T(8,128)(2,1)S(1)} async-done(((bf16[4,512,256]{2,1,0:T(8,128)(2,1)}), bf16[4,512,256]{2,1,0:T(8,128)(2,1)S(1)}, u32[]{:S(2)}, u32[]{:S(2)}) %all-to-all-start.2) | async-done | bytes 1048608 | tf_op jit(solution)/shard_map/all_to_all | solution.py:250
  92.5 0.7 fusion
  93.2 11.0 %all_to_all.34 = bf16[4,128,512]{2,1,0:T(8,128)(2,1)S(1)} all-to-all(bf16[4,128,512]{2,1,0:T(8,128)(2,1)S(1)} %bitcast.26), channel_id=1, replica_groups=mesh['z'=8,'y'=8,'x'=4,'c'=2] {'x'}, dimensions={0} | all-to-all | bytes 1048576 | tf_op jit(solution)/shard_map/all_to_all | solution.py:264
  104.2 0.8 copy.11
  (20 shorter events, 0.2 us)
Async XLA Ops:
  0.0 24.2 %copy-start.4 = (bf16[128,32]{0,1:T(8,128)(2,1)S(1)}, bf16[128,32]{0,1:T(8,128)(2,1)}, u32[]{:S(2)}) copy-start(bf16[128,32]{0,1:T(8,128)(2,1)} %param.17) | copy-start | bytes 24580
  1.8 35.0 %all-to-all-start = ((bf16[64,32,128]{2,1,0:T(8,128)(2,1)}), bf16[64,32,128]{2,1,0:T(8,128)(2,1)S(1)}, u32[]{:S(2)}, u32[]{:S(2)}) async-start(bf16[64,32,128]{2,1,0:T(8,128)(2,1)} %broadcast_in_dim.13), calls=%async_computation | async-start | bytes 1048576 | tf_op jit(solution)/shard_map/all_to_all | solution.py:25
  21.3 7.3 %copy-start = (bf16[144,2048]{1,0:T(8,128)(2,1)}, bf16[144,2048]{1,0:T(8,128)(2,1)S(1)}, u32[]{:S(2)}) copy-start(bf16[144,2048]{1,0:T(8,128)(2,1)S(1)} %pad_maximum_fusion.own) | copy-start | bytes 1769476
  21.3 7.3 %collective-permute-start = (bf16[144,2048]{1,0:T(8,128)(2,1)S(1)}, bf16[144,2048]{1,0:T(8,128)(2,1)S(1)}, u32[]{:S(2)}, u32[]{:S(2)}) collective-permute-start(bf16[144,2048]{1,0:T(8,128)(2,1)S(1)} %pad_maximum_fusion.own), channel_id=1, source_target_pairs={{0,1},{1,0},{2,3},{3,2},{4,5},{5,4},{6,7},{7,6},{8,9},{9,8},{10,11... | collective-permute-start | bytes 1769480 | tf_op jit(solution)/shard_map/ppermute | solution.py:195
  24.2 12.6 %collective-permute-start.1 = (bf16[32,128]{1,0:T(8,128)(2,1)S(1)}, bf16[32,128]{1,0:T(8,128)(2,1)S(1)}, u32[]{:S(2)}, u32[]{:S(2)}) collective-permute-start(bf16[32,128]{1,0:T(8,128)(2,1)S(1)} %bitcast.30), channel_id=1, source_target_pairs={{0,0},{1,64},{2,128},{3,192},{4,256},{5,320},{6,384},{7,448},{8,8}... | collective-permute-start | bytes 24584 | tf_op jit(solution)/shard_map/ppermute | solution.py:37
  28.6 0.8 copy-start.1
  36.8 14.8 %copy-start.2 = (bf16[64,32,128]{2,1,0:T(8,128)(2,1)}, bf16[64,32,128]{2,1,0:T(8,128)(2,1)S(1)}, u32[]{:S(2)}) copy-start(bf16[64,32,128]{2,1,0:T(8,128)(2,1)S(1)} %all-to-all-done.ex) | copy-start | bytes 1572868
  37.8 32.1 %all-to-all-start.1 = ((bf16[64,32,128]{2,1,0:T(8,128)(2,1)}), bf16[64,32,128]{2,1,0:T(8,128)(2,1)S(1)}, u32[]{:S(2)}, u32[]{:S(2)}) async-start(bf16[64,32,128]{2,1,0:T(8,128)(2,1)} %broadcast_in_dim.14), calls=%async_computation.1 | async-start | bytes 1048576 | tf_op jit(solution)/shard_map/all_to_all | solution.py:25
  57.0 7.1 %collective-permute-start.2 = (bf16[144,128]{1,0:T(8,128)(2,1)}, bf16[144,128]{1,0:T(8,128)(2,1)S(1)}, u32[]{:S(2)}, u32[]{:S(2)}) collective-permute-start(bf16[144,128]{1,0:T(8,128)(2,1)} %get-tuple-element.21), channel_id=1, source_target_pairs={{0,8},{8,16},{16,24},{24,32},{32,40},{40,48},{48,56},{56,64},{64,7... | collective-permute-start | bytes 110600 | tf_op jit(solution)/shard_map/ppermute | solution.py:229
  64.2 0.6 copy-start.3
  69.9 7.5 %collective-permute-start.3 = (bf16[64,32,128]{2,1,0:T(8,128)(2,1)S(1)}, bf16[64,32,128]{2,1,0:T(8,128)(2,1)S(1)}, u32[]{:S(2)}, u32[]{:S(2)}) collective-permute-start(bf16[64,32,128]{2,1,0:T(8,128)(2,1)S(1)} %all-to-all-done.1), channel_id=1, source_target_pairs={{0,1},{1,0},{2,3},{3,2},{4,5},{5,4},{6,7},{7,6},{8,9},{9,8},{10,11... | collective-permute-start | bytes 1572872 | tf_op jit(solution)/shard_map/ppermute | solution.py:249
  73.8 18.7 %all-to-all-start.2 = ((bf16[4,512,256]{2,1,0:T(8,128)(2,1)}), bf16[4,512,256]{2,1,0:T(8,128)(2,1)S(1)}, u32[]{:S(2)}, u32[]{:S(2)}) async-start(bf16[4,512,256]{2,1,0:T(8,128)(2,1)} %mix.1), calls=%async_computation.2 | async-start | bytes 2097152 | tf_op jit(solution)/shard_map/all_to_all | solution.py:250

commit v8 on v7

--- a/solution.py
+++ b/solution.py
@@ -1,5 +1,8 @@
+import functools
+
 import jax
 import jax.numpy as jnp
+import numpy as np
 from jax import lax
 from jax.experimental import pallas as pl
 from jax.experimental.pallas import tpu as pltpu
@@ -11,7 +14,7 @@
 QB = 128
 LANES = 128
 ROWS = 256
-STEP = 2
+STEPS = 4
 EDGE = 16
 POOL_SPANS = (2, 4, 8, 16)
 NEG_BIG = -1e30
@@ -47,12 +50,24 @@
 def rope_tables(offset, rows):
     half = HEAD // 2
     inverse = 10000.0 ** (-jnp.arange(half, dtype=jnp.float32) / half)
-    positions = (offset + jnp.arange(rows)).astype(jnp.float32)
-    angles = positions[None, :] * inverse[:, None]
-    return jnp.cos(angles), jnp.sin(angles)
-
-
-def turned(x, cosine, sine):
+    starts = (offset + QB * jnp.arange(rows // QB)).astype(jnp.float32)
+    coarse = starts[None, :] * inverse[:, None]
+    exact = 10000.0 ** (-np.arange(half) / half)
+    fine = np.arange(QB)[None, :] * exact[:, None]
+    fine = jnp.asarray(np.stack([np.cos(fine), np.sin(fine)]), jnp.float32)
+    return jnp.stack([jnp.cos(coarse), jnp.sin(coarse)]), fine
+
+
+def turned(x, coarse, fine, first_block):
+    places = lax.broadcasted_iota(jnp.int32, coarse.shape[1:], 1)
+    cosines, sines = [], []
+    for block in range(x.shape[0] // QB):
+        here = places == first_block + block
+        cosine = jnp.sum(jnp.where(here, coarse[0], 0.0), axis=1, keepdims=True)
+        sine = jnp.sum(jnp.where(here, coarse[1], 0.0), axis=1, keepdims=True)
+        cosines.append(cosine * fine[0] - sine * fine[1])
+        sines.append(sine * fine[0] + cosine * fine[1])
+    cosine, sine = jnp.concatenate(cosines, axis=1), jnp.concatenate(sines, axis=1)
     lane = lax.broadcasted_iota(jnp.int32, x.shape, 1)
     wide_cosine = jnp.concatenate([cosine] * 4, axis=0).T
     wide_sine = jnp.concatenate([-sine, sine] * 2, axis=0).T
@@ -61,7 +76,7 @@
     return x * wide_cosine + other * wide_sine
 
 
-def project(tokens, gain, own, other, cosine, sine, normed_out, q_out, pool_out, weights):
+def project(tokens, gain, own, other, coarse, fine, normed_out, q_out, pool_out, weights):
     core = lax.axis_index("c")
     for place in range(2):
 
@@ -80,34 +95,37 @@
     sums = lax.dot_general(
         normed, weights[...], (((1,), (1,)), ((), ())), preferred_element_type=jnp.float32
     )
-    query = turned(sums[:, :LANES], cosine[...], sine[...])
+    first_block = pl.program_id(0) * (ROWS // QB)
+    query = turned(sums[:, :LANES], coarse[...], fine[...], first_block)
     q_out[...] = (query * HEAD ** (-0.5)).astype(jnp.bfloat16)
     pool_out[...] = sums[:, LANES:].astype(jnp.bfloat16)
 
 
-def project_kv(normed, pool, ex, cosine, sine, kv_out, send):
-    core = lax.axis_index("c")
-    step = pl.program_id(0)
-    rows = normed.shape[0]
-    sums = jnp.dot(
-        normed[...], ex[...].reshape(-1, LANES), preferred_element_type=jnp.float32
-    )
-    lane = lax.broadcasted_iota(jnp.int32, sums.shape, 1)
-    kv = jnp.where(lane < HEAD, turned(sums, cosine[...], sine[...]), sums).astype(jnp.bfloat16)
-    kv_out[...] = kv
-
-    @pl.when((step == 0) & (core == 1))
+def project_kv(normed, pool, ex, coarse, fine, kv_out, send, total):
+    step, rows = pl.program_id(0), normed.shape[0]
+    part = jnp.dot(normed[...], ex[...].reshape(-1, LANES), preferred_element_type=jnp.float32)
+
+    @pl.when(step == 0)
     def _():
-        send[:QB] = kv[:QB]
-        send[QB:] = pool[:EDGE]
-
-    @pl.when((step == pl.num_programs(0) - 1) & (core == 0))
+        total[...] = part
+
+    @pl.when(step > 0)
     def _():
-        send[:QB] = kv[rows - QB :]
-        send[QB:] = pool[rows - EDGE :]
-
-
-def mix(own, other, q, kv, pool, halo, out, kv_wide, pool_wide):
+        total[...] += part
+
+    @pl.when(step == pl.num_programs(0) - 1)
+    def _():
+        core, sums = lax.axis_index("c"), total[...]
+        lane = lax.broadcasted_iota(jnp.int32, sums.shape, 1)
+        kv = jnp.where(lane < HEAD, turned(sums, coarse[...], fine[...], 0), sums)
+        kv = kv.astype(jnp.bfloat16)
+        kv_out[...] = kv
+        send[:QB] = jnp.where(core == 0, kv[rows - QB :], kv[:QB])
+        send[QB:] = jnp.where(core == 0, pool[rows - EDGE :], pool[:EDGE])
+
+
+def mix(inner, own, other, q, kv, pool, *rest):
+    out, kv_wide, pool_wide, both, sems = rest[-5:]
     core, group = lax.axis_index("c"), lax.axis_index("x")
     rows = q.shape[0]
     blocks_total = lax.axis_size(SP) * (rows // QB)
@@ -117,16 +135,14 @@
     first = jnp.where(core == 0, mine, theirs)
     second = jnp.where(core == 0, theirs, mine)
     scale = jnp.concatenate([first[:, :HEAD], second[:, :HEAD]], axis=1)
-
-    @pl.when(pl.program_id(0) == 0)
-    def _():
-        kv_wide[pl.ds(pl.multiple_of((1 - core) * QB, QB), rows), :] = kv[...]
+    kv_wide[pl.ds(pl.multiple_of((1 - core) * QB, QB), rows), :] = kv[...]
+    pool_wide[EDGE : EDGE + rows, :] = pool[...].astype(jnp.float32)
+    if not inner:
+        halo = rest[0]
         kv_wide[pl.ds(pl.multiple_of(core * rows, QB), QB), :] = halo[:QB, :]
         edge = halo[QB:, :].astype(jnp.float32)
         pool_wide[:EDGE, :] = edge
-        pool_wide[EDGE : EDGE + rows, :] = pool[...].astype(jnp.float32)
         pool_wide[EDGE + rows :, :] = edge
-
     lane = lax.broadcasted_iota(jnp.int32, (QB, LANES), 1)
     row = lax.broadcasted_iota(jnp.int32, (2 * QB, 3 * QB), 0) % QB
     column = lax.broadcasted_iota(jnp.int32, (2 * QB, 3 * QB), 1)
@@ -134,8 +150,9 @@
     upper = lax.broadcasted_iota(jnp.int32, (2 * QB, 1), 0) < QB
     sinks = jnp.where(upper, first[:, HEAD : HEAD + 1], second[:, HEAD : HEAD + 1])
     half = lax.shift_left(1, group)
-    for j in range(STEP):
-        i = pl.program_id(0) * STEP + j
+    copies = []
+    for j in range(both.shape[0]):
+        i = 1 - core + j if inner else core * (rows // (2 * QB) - 1)
         start = pl.multiple_of(core * QB + 2 * QB * i, QB)
         block = first_block + core + 2 * i
         pair = q[pl.ds(start, QB), :]
@@ -170,9 +187,13 @@
         counted = jnp.minimum(position + half, blocks_total * QB) - jnp.maximum(position - half, 0)
         mean = chosen[EDGE : EDGE + QB] / counted.astype(jnp.float32)
         pooled = (mean - near_rows[EDGE : EDGE + QB]) * scale
-        both = jnp.concatenate([attended, pooled], axis=1).astype(jnp.bfloat16)
+        both[j] = jnp.concatenate([attended, pooled], axis=1).astype(jnp.bfloat16)
         for peer in range(out.shape[0]):
-            out[peer, j * QB : (j + 1) * QB] = both
+            target = out.at[peer, pl.ds(pl.multiple_of(i * QB, QB), QB)]
+            copies.append(pltpu.make_async_copy(both.at[j], target, sems.at[j, peer]))
+            copies[-1].start()
+    for copy in copies:
+        copy.wait()
 
 
 def body(tokens, norm_gain, w_query, w_key, w_value, w_pool_in, sink_logit, pool_scale, w_out):
@@ -194,14 +215,14 @@
     own = jnp.concatenate([w_query.T, w_pool_in.T, small], axis=0)
     other = lax.ppermute(own, "c", [(0, 1), (1, 0)])
 
-    cosine, sine = rope_tables(lax.axis_index(SP) * rows, rows)
+    coarse, fine = rope_tables(lax.axis_index(SP) * rows, rows)
 
     at = lambda *shape: lambda *place: pl.BlockSpec(shape, lambda i: place)
     whole = lambda *shape: pl.BlockSpec(shape, lambda i: (0,) * len(shape))
     part = lambda *shape: pl.BlockSpec(shape, lambda i: (i,) + (0,) * (len(shape) - 1))
     along = lambda *shape: pl.BlockSpec(shape, lambda i: (0, i))
     shaped = lambda *shape: jax.ShapeDtypeStruct(shape, bf16)
-    tables = [along(HEAD // 2, ROWS)] * 2
+    tables = [whole(*coarse.shape), whole(*fine.shape)]
     normed, query, pool_in = pl.pallas_call(
         project,
         grid=(rows // ROWS,),
@@ -211,39 +232,51 @@
         scratch_shapes=[pltpu.VMEM((2 * LANES, depth), bf16)],
         name="project",
         interpret=INTERPRET,
-    )(tokens, norm_gain[None, :], own, other, cosine, sine)
+    )(tokens, norm_gain[None, :], own, other, coarse, fine)
     exchanged, out_piece, normed = lax.optimization_barrier((exchanged, out_piece, normed))
     own_cols = from_everyone(out_piece, SP)
     kv, send = pl.pallas_call(
         project_kv,
-        grid=(rows // ROWS,),
-        in_specs=[part(ROWS, depth), part(ROWS, LANES), whole(peers, pieces, LANES)] + tables,
-        out_specs=[part(ROWS, LANES), whole(QB + EDGE, LANES)],
+        grid=(STEPS,),
+        in_specs=[along(rows, depth // STEPS), whole(rows, LANES)]
+        + [part(peers // STEPS, pieces, LANES)]
+        + tables,
+        out_specs=[whole(rows, LANES), whole(QB + EDGE, LANES)],
         out_shape=[shaped(rows, LANES), shaped(QB + EDGE, LANES)],
+        scratch_shapes=[pltpu.VMEM((rows, LANES), jnp.float32)],
         name="project_kv",
         interpret=INTERPRET,
-    )(normed, pool_in, exchanged, cosine, sine)
+    )(normed, pool_in, exchanged, coarse, fine)
 
     pairs = [(2 * s, 2 * s + 2) for s in range(sp_count - 1)]
     pairs += [(2 * s + 3, 2 * s + 1) for s in range(sp_count - 1)]
     halo = lax.ppermute(send, SP + ("c",), pairs)
     peers_x = lax.axis_size("x")
     small_rows = at(EDGE, depth)(LANES // EDGE, 0)
-    local = pl.pallas_call(
-        mix,
-        grid=(rows // (2 * QB * STEP),),
-        in_specs=[small_rows, small_rows]
-        + [whole(rows, LANES)] * 3
-        + [whole(QB + EDGE, LANES)],
-        out_specs=pl.BlockSpec((peers_x, STEP * QB, 2 * LANES), lambda i: (0, i, 0)),
-        out_shape=shaped(peers_x, rows // 2, 2 * LANES),
-        scratch_shapes=[
-            pltpu.VMEM((rows + QB, LANES), bf16),
-            pltpu.VMEM((rows + 2 * EDGE, LANES), jnp.float32),
-        ],
-        name="mix",
-        interpret=INTERPRET,
-    )(own, other, query, kv, pool_in, halo)
+    anywhere = pl.BlockSpec(memory_space=pl.ANY)
+    local_specs = [small_rows, small_rows] + [whole(rows, LANES)] * 3
+
+    def mixed(inner, *more):
+        blocks = rows // (2 * QB) - 1 if inner else 1
+        return pl.pallas_call(
+            functools.partial(mix, inner),
+            grid=(1,),
+            in_specs=local_specs + ([] if inner else [whole(QB + EDGE, LANES), anywhere]),
+            out_specs=anywhere,
+            out_shape=shaped(peers_x, rows // 2, 2 * LANES),
+            input_output_aliases={} if inner else {6: 0},
+            scratch_shapes=[
+                pltpu.VMEM((rows + QB, LANES), bf16),
+                pltpu.VMEM((rows + 2 * EDGE, LANES), jnp.float32),
+                pltpu.VMEM((blocks, QB, 2 * LANES), bf16),
+                pltpu.SemaphoreType.DMA((blocks, peers_x)),
+            ],
+            name="mix_inner" if inner else "mix_outer",
+            interpret=INTERPRET,
+        )(own, other, query, kv, pool_in, *more)
+
+    local = mixed(True)
+    local = mixed(False, halo, local)
 
     local, own_cols = lax.optimization_barrier((local, own_cols))
     other_cols = lax.ppermute(own_cols, "c", [(0, 1), (1, 0)])

time: 106 us -> 105 us (level)
  waiting for transfers between devices: 20.6 us -> 18 us
  Pallas kernels: 17.8 us -> 19.9 us
  other arithmetic: 2.71 us -> 1.57 us
    ppermute x1, waiting for transfers between devices: 5.86 us -> 1.47 us  [body(): halo = lax.ppermute(send, SP + ('c',), pairs)]
    pallas_call x2 -> x3, Pallas kernels: 10.5 us -> 12.6 us  [the longest x2 6.95 us: mixed(): pl.pallas_call(functools.partial(mix, inner), grid=(1,), in_specs=local_s...]
    all_to_all x2, waiting for transfers between devices: 0.01 us -> 1.73 us  [from_everyone(): lax.all_to_all(jnp.broadcast_to(x[None], (peers, *x.shape)), axis, 0, 0,...]
    sin x1 -> x0, other arithmetic: 1.26 us -> none  [rope_tables(): return (jnp.cos(angles), jnp.sin(angles))]
  transfers between devices with their start and end apart: 7 -> 7, of which waited for: 2 -> 3; matrix products, arithmetic and copies ran while one was open for 3% -> 3% of each run, Pallas kernels for 17% -> 19%
where the time goes in v8:
time: 105 us; the launch traced here: 104 us
  starting transfers between devices  46.2 us (44%)
  Pallas kernels  19.9 us (19%)
  waiting for transfers between devices  18 us (17%)
  blocking collectives  11 us (10%)
  local copies, waits for them, and re-layouts  6.37 us (6%)
  other arithmetic  1.57 us (1%)
    all_to_all x2, starting transfers between devices, from_everyone(): lax.all_to_all(jnp.broadcast_to(x[None], (peers, *x.shape)), axis, 0, 0,...  31 us
    all_to_all x1, waiting for transfers between devices, body(): joined = lax.all_to_all(local, 'x', 0, 0, tiled=True)  14.8 us
    all_to_all x1, blocking collectives, body(): lax.all_to_all(partial_cols, 'x', split_axis=0, concat_axis=1, tiled=True)  11 us
    pallas_call x1, Pallas kernels, body(): pl.pallas_call(project, grid=(rows // ROWS,), in_specs=[part(ROWS, depth)...  7.31 us
    pallas_call x2, Pallas kernels, mixed(): pl.pallas_call(functools.partial(mix, inner), grid=(1,), in_specs=local_s...  6.95 us
    pallas_call x1, Pallas kernels, body(): pl.pallas_call(project_kv, grid=(STEPS,), in_specs=[along(rows, depth //...  5.61 us
    ppermute x1, starting transfers between devices, body(): other_cols = lax.ppermute(own_cols, 'c', [(0, 1), (1, 0)])  4.42 us
    all_to_all x1, starting transfers between devices, body(): joined = lax.all_to_all(local, 'x', 0, 0, tiled=True)  3.53 us
  transfers between devices with their start and end apart: 7, of which 3 were waited for; matrix products, arithmetic and copies ran while one was open for 3% of the time, Pallas kernels for 19%

profile of v8, /device:TPU:1, one launch (start us, length us, event | category | flops | bytes accessed | tf_op | source)
XLA Modules:
  0.0 104.5 jit_solution(9842414204280016068)
XLA Ops:
  0.0 0.8 constant_dynamic-slice_fusion
  0.9 0.9 broadcast_in_dim.13
  1.8 17.1 %all-to-all-start = ((bf16[64,32,128]{2,1,0:T(8,128)(2,1)}), bf16[64,32,128]{2,1,0:T(8,128)(2,1)S(1)}, u32[]{:S(2)}, u32[]{:S(2)}) async-start(bf16[64,32,128]{2,1,0:T(8,128)(2,1)} %broadcast_in_dim.13), calls=%async_computation | async-start | bytes 1048576 | tf_op jit(solution)/shard_map/all_to_all | solution.py:28
  19.5 0.7 pad_bitcast_fusion
  20.2 1.1 %pad_maximum_fusion.own = bf16[144,2048]{1,0:T(8,128)(2,1)S(1)} fusion(bf16[16,2048]{1,0:T(8,128)(2,1)S(1)} %fusion.12, bf16[64,2048]{1,0:T(8,128)(2,1)} %bitcast.27, bf16[64,2048]{1,0:T(8,128)(2,1)} %bitcast.28), kind=kLoop, calls=%fused_computation.5 | loop fusion | flops 1769472 | bytes 1179648 | tf_op jit(solution)/shard_map/concatenate | solution.py:215
  21.3 2.9 %collective-permute-start = (bf16[144,2048]{1,0:T(8,128)(2,1)S(1)}, bf16[144,2048]{1,0:T(8,128)(2,1)S(1)}, u32[]{:S(2)}, u32[]{:S(2)}) collective-permute-start(bf16[144,2048]{1,0:T(8,128)(2,1)S(1)} %pad_maximum_fusion.own), channel_id=1, source_target_pairs={{0,1},{1,0},{2,3},{3,2},{4,5},{5,4},{6,7},{7,6},{8,9},{9,8},{10,11... | collective-permute-start | bytes 1769480 | tf_op jit(solution)/shard_map/ppermute | solution.py:216
  24.2 3.1 %collective-permute-start.1 = (bf16[32,128]{1,0:T(8,128)(2,1)S(1)}, bf16[32,128]{1,0:T(8,128)(2,1)S(1)}, u32[]{:S(2)}, u32[]{:S(2)}) collective-permute-start(bf16[32,128]{1,0:T(8,128)(2,1)S(1)} %bitcast.30), channel_id=1, source_target_pairs={{0,0},{1,64},{2,128},{3,192},{4,256},{5,320},{6,384},{7,448},{8,8}... | collective-permute-start | bytes 24584 | tf_op jit(solution)/shard_map/ppermute | solution.py:40
  27.4 0.7 copy.13.coarse
  28.1 0.8 copy-done.1
  29.0 7.3 %project.1 = (bf16[1024,2048]{1,0:T(8,128)(2,1)}, bf16[1024,128]{1,0:T(8,128)(2,1)}, bf16[1024,128]{1,0:T(8,128)(2,1)}) custom-call(bf16[1024,2048]{1,0:T(8,128)(2,1)} %tokens.1, f32[1,2048]{1,0:T(1,128)} %bitcast.29, bf16[144,2048]{1,0:T(8,128)(2,1)} %copy-done, bf16[144,2048]{1,0:T(8,128)(2,1)} %copy-done.1, f32[2,32,8]{2,1,0:T(8,128)} %copy.13.coarse, ...), custom_call_target="tpu_custom_call" | custom-call | tf_op jit(solution)/shard_map/project/pallas_call | solution.py:226
  36.3 1.0 broadcast_in_dim.14
  37.3 13.8 %all-to-all-start.1 = ((bf16[64,32,128]{2,1,0:T(8,128)(2,1)}), bf16[64,32,128]{2,1,0:T(8,128)(2,1)S(1)}, u32[]{:S(2)}, u32[]{:S(2)}) async-start(bf16[64,32,128]{2,1,0:T(8,128)(2,1)} %broadcast_in_dim.14), calls=%async_computation.1 | async-start | bytes 1048576 | tf_op jit(solution)/shard_map/all_to_all | solution.py:28
  51.1 5.6 %project_kv.1 = (bf16[1024,128]{1,0:T(8,128)(2,1)}, bf16[144,128]{1,0:T(8,128)(2,1)}) custom-call(bf16[1024,2048]{1,0:T(8,128)(2,1)} %get-tuple-element.17.normed, bf16[1024,128]{1,0:T(8,128)(2,1)} %get-tuple-element.18.pool, bf16[64,32,128]{2,1,0:T(8,128)(2,1)} %copy-done.2, f32[2,32,8]{2,1,0:T(8,128)} %copy.13.coarse, f32[2,32,128]{2,1,0:T(8,128)} %constant.49.clone.fine), custom_call_target="tpu_custom_call" | custom-call | tf_op jit(solution)/shard_map/project_kv/pallas_call | solution.py:238
  56.8 1.3 %collective-permute-start.2 = (bf16[144,128]{1,0:T(8,128)(2,1)}, bf16[144,128]{1,0:T(8,128)(2,1)S(1)}, u32[]{:S(2)}, u32[]{:S(2)}) collective-permute-start(bf16[144,128]{1,0:T(8,128)(2,1)} %get-tuple-element.21), channel_id=1, source_target_pairs={{0,8},{8,16},{16,24},{24,32},{32,40},{40,48},{48,56},{56,64},{64,7... | collective-permute-start | bytes 110600 | tf_op jit(solution)/shard_map/ppermute | solution.py:253
  58.0 4.2 %mix_inner.1.rest_1_ = bf16[4,512,256]{2,1,0:T(8,128)(2,1)} custom-call(bf16[144,2048]{1,0:T(8,128)(2,1)} %copy-done, bf16[144,2048]{1,0:T(8,128)(2,1)} %copy-done.1, bf16[1024,128]{1,0:T(8,128)(2,1)} %get-tuple-element.15.q, bf16[1024,128]{1,0:T(8,128)(2,1)} %get-tuple-element.20.kv, bf16[1024,128]{1,0:T(8,128)(2,1)} %get-tuple-element.18.pool), custom_call_target="tpu_custom_call" | custom-call | tf_op jit(solution)/shard_map/mix_inner/pallas_call | solution.py:261
  62.3 1.5 %collective-permute-done.2.rest_0_ = bf16[144,128]{1,0:T(8,128)(2,1)S(1)} collective-permute-done((bf16[144,128]{1,0:T(8,128)(2,1)}, bf16[144,128]{1,0:T(8,128)(2,1)S(1)}, u32[]{:S(2)}, u32[]{:S(2)}) %collective-permute-start.2) | collective-permute-done | bytes 36896 | tf_op jit(solution)/shard_map/ppermute | solution.py:253
  64.4 2.7 %mix_outer.1 = bf16[4,512,256]{2,1,0:T(8,128)(2,1)} custom-call(bf16[144,2048]{1,0:T(8,128)(2,1)} %copy-done, bf16[144,2048]{1,0:T(8,128)(2,1)} %copy-done.1, bf16[1024,128]{1,0:T(8,128)(2,1)} %get-tuple-element.15.q, bf16[1024,128]{1,0:T(8,128)(2,1)} %get-tuple-element.20.kv, ...), custom_call_target="tpu_custom_call", output_to_operand_aliasing={{}: (6, {})} | custom-call | tf_op jit(solution)/shard_map/mix_outer/pallas_call | solution.py:261
  67.1 1.7 %all-to-all-done.1 = bf16[64,32,128]{2,1,0:T(8,128)(2,1)S(1)} async-done(((bf16[64,32,128]{2,1,0:T(8,128)(2,1)}), bf16[64,32,128]{2,1,0:T(8,128)(2,1)S(1)}, u32[]{:S(2)}, u32[]{:S(2)}) %all-to-all-start.1) | async-done | bytes 524320 | tf_op jit(solution)/shard_map/all_to_all | solution.py:28
  68.8 4.4 %collective-permute-start.3 = (bf16[64,32,128]{2,1,0:T(8,128)(2,1)S(1)}, bf16[64,32,128]{2,1,0:T(8,128)(2,1)S(1)}, u32[]{:S(2)}, u32[]{:S(2)}) collective-permute-start(bf16[64,32,128]{2,1,0:T(8,128)(2,1)S(1)} %all-to-all-done.1), channel_id=1, source_target_pairs={{0,1},{1,0},{2,3},{3,2},{4,5},{5,4},{6,7},{7,6},{8,9},{9,8},{10,11... | collective-permute-start | bytes 1572872 | tf_op jit(solution)/shard_map/ppermute | solution.py:282
  73.3 3.5 %all-to-all-start.2 = ((bf16[4,512,256]{2,1,0:T(8,128)(2,1)}), bf16[4,512,256]{2,1,0:T(8,128)(2,1)S(1)}, u32[]{:S(2)}, u32[]{:S(2)}) async-start(bf16[4,512,256]{2,1,0:T(8,128)(2,1)} %mix_outer.1), calls=%async_computation.2 | async-start | bytes 2097152 | tf_op jit(solution)/shard_map/all_to_all | solution.py:283
  77.2 14.8 %all-to-all-done.2 = bf16[4,512,256]{2,1,0:T(8,128)(2,1)S(1)} async-done(((bf16[4,512,256]{2,1,0:T(8,128)(2,1)}), bf16[4,512,256]{2,1,0:T(8,128)(2,1)S(1)}, u32[]{:S(2)}, u32[]{:S(2)}) %all-to-all-start.2) | async-done | bytes 1048608 | tf_op jit(solution)/shard_map/all_to_all | solution.py:283
  91.9 0.7 fusion
  92.7 11.0 %all_to_all.34 = bf16[4,128,512]{2,1,0:T(8,128)(2,1)S(1)} all-to-all(bf16[4,128,512]{2,1,0:T(8,128)(2,1)S(1)} %bitcast.26), channel_id=1, replica_groups=mesh['z'=8,'y'=8,'x'=4,'c'=2] {'x'}, dimensions={0} | all-to-all | bytes 1048576 | tf_op jit(solution)/shard_map/all_to_all | solution.py:297
  103.6 0.8 copy.16
  (23 shorter events, 1.2 us)
Async XLA Ops:
  0.0 24.2 %copy-start.4 = (bf16[128,32]{0,1:T(8,128)(2,1)S(1)}, bf16[128,32]{0,1:T(8,128)(2,1)}, u32[]{:S(2)}) copy-start(bf16[128,32]{0,1:T(8,128)(2,1)} %param.18) | copy-start | bytes 24580
  1.8 34.6 %all-to-all-start = ((bf16[64,32,128]{2,1,0:T(8,128)(2,1)}), bf16[64,32,128]{2,1,0:T(8,128)(2,1)S(1)}, u32[]{:S(2)}, u32[]{:S(2)}) async-start(bf16[64,32,128]{2,1,0:T(8,128)(2,1)} %broadcast_in_dim.13), calls=%async_computation | async-start | bytes 1048576 | tf_op jit(solution)/shard_map/all_to_all | solution.py:28
  21.3 6.9 %copy-start = (bf16[144,2048]{1,0:T(8,128)(2,1)}, bf16[144,2048]{1,0:T(8,128)(2,1)S(1)}, u32[]{:S(2)}) copy-start(bf16[144,2048]{1,0:T(8,128)(2,1)S(1)} %pad_maximum_fusion.own) | copy-start | bytes 1769476
  21.3 6.8 %collective-permute-start = (bf16[144,2048]{1,0:T(8,128)(2,1)S(1)}, bf16[144,2048]{1,0:T(8,128)(2,1)S(1)}, u32[]{:S(2)}, u32[]{:S(2)}) collective-permute-start(bf16[144,2048]{1,0:T(8,128)(2,1)S(1)} %pad_maximum_fusion.own), channel_id=1, source_target_pairs={{0,1},{1,0},{2,3},{3,2},{4,5},{5,4},{6,7},{7,6},{8,9},{9,8},{10,11... | collective-permute-start | bytes 1769480 | tf_op jit(solution)/shard_map/ppermute | solution.py:216
  24.2 12.1 %collective-permute-start.1 = (bf16[32,128]{1,0:T(8,128)(2,1)S(1)}, bf16[32,128]{1,0:T(8,128)(2,1)S(1)}, u32[]{:S(2)}, u32[]{:S(2)}) collective-permute-start(bf16[32,128]{1,0:T(8,128)(2,1)S(1)} %bitcast.30), channel_id=1, source_target_pairs={{0,0},{1,64},{2,128},{3,192},{4,256},{5,320},{6,384},{7,448},{8,8}... | collective-permute-start | bytes 24584 | tf_op jit(solution)/shard_map/ppermute | solution.py:40
  28.1 0.8 copy-start.1
  36.3 14.8 %copy-start.2 = (bf16[64,32,128]{2,1,0:T(8,128)(2,1)}, bf16[64,32,128]{2,1,0:T(8,128)(2,1)S(1)}, u32[]{:S(2)}) copy-start(bf16[64,32,128]{2,1,0:T(8,128)(2,1)S(1)} %all-to-all-done.ex) | copy-start | bytes 1572868
  37.3 31.5 %all-to-all-start.1 = ((bf16[64,32,128]{2,1,0:T(8,128)(2,1)}), bf16[64,32,128]{2,1,0:T(8,128)(2,1)S(1)}, u32[]{:S(2)}, u32[]{:S(2)}) async-start(bf16[64,32,128]{2,1,0:T(8,128)(2,1)} %broadcast_in_dim.14), calls=%async_computation.1 | async-start | bytes 1048576 | tf_op jit(solution)/shard_map/all_to_all | solution.py:28
  56.8 7.0 %collective-permute-start.2 = (bf16[144,128]{1,0:T(8,128)(2,1)}, bf16[144,128]{1,0:T(8,128)(2,1)S(1)}, u32[]{:S(2)}, u32[]{:S(2)}) collective-permute-start(bf16[144,128]{1,0:T(8,128)(2,1)} %get-tuple-element.21), channel_id=1, source_target_pairs={{0,8},{8,16},{16,24},{24,32},{32,40},{40,48},{48,56},{56,64},{64,7... | collective-permute-start | bytes 110600 | tf_op jit(solution)/shard_map/ppermute | solution.py:253
  63.7 0.6 copy-start.3
  68.8 8.0 %collective-permute-start.3 = (bf16[64,32,128]{2,1,0:T(8,128)(2,1)S(1)}, bf16[64,32,128]{2,1,0:T(8,128)(2,1)S(1)}, u32[]{:S(2)}, u32[]{:S(2)}) collective-permute-start(bf16[64,32,128]{2,1,0:T(8,128)(2,1)S(1)} %all-to-all-done.1), channel_id=1, source_target_pairs={{0,1},{1,0},{2,3},{3,2},{4,5},{5,4},{6,7},{7,6},{8,9},{9,8},{10,11... | collective-permute-start | bytes 1572872 | tf_op jit(solution)/shard_map/ppermute | solution.py:282
  73.3 18.7 %all-to-all-start.2 = ((bf16[4,512,256]{2,1,0:T(8,128)(2,1)}), bf16[4,512,256]{2,1,0:T(8,128)(2,1)S(1)}, u32[]{:S(2)}, u32[]{:S(2)}) async-start(bf16[4,512,256]{2,1,0:T(8,128)(2,1)} %mix_outer.1), calls=%async_computation.2 | async-start | bytes 2097152 | tf_op jit(solution)/shard_map/all_to_all | solution.py:283

commit v9 on v8

--- a/solution.py
+++ b/solution.py
@@ -14,7 +14,7 @@
 QB = 128
 LANES = 128
 ROWS = 256
-STEPS = 4
+KV_ROWS = 512
 EDGE = 16
 POOL_SPANS = (2, 4, 8, 16)
 NEG_BIG = -1e30
@@ -49,34 +49,31 @@
 
 def rope_tables(offset, rows):
     half = HEAD // 2
-    inverse = 10000.0 ** (-jnp.arange(half, dtype=jnp.float32) / half)
+    places = jnp.arange(LANES)
+    inverse = 10000.0 ** (-(places % half).astype(jnp.float32) / half)
     starts = (offset + QB * jnp.arange(rows // QB)).astype(jnp.float32)
-    coarse = starts[None, :] * inverse[:, None]
-    exact = 10000.0 ** (-np.arange(half) / half)
-    fine = np.arange(QB)[None, :] * exact[:, None]
-    fine = jnp.asarray(np.stack([np.cos(fine), np.sin(fine)]), jnp.float32)
-    return jnp.stack([jnp.cos(coarse), jnp.sin(coarse)]), fine
-
-
-def turned(x, coarse, fine, first_block):
-    places = lax.broadcasted_iota(jnp.int32, coarse.shape[1:], 1)
+    coarse = starts[:, None] * inverse[None, :]
+    sign = np.where(np.arange(LANES) % HEAD < half, -1.0, 1.0)
+    exact = np.tile(10000.0 ** (-np.arange(half) / half), 4)
+    fine = np.arange(QB)[:, None] * exact[None, :]
+    fine = jnp.asarray(np.stack([np.cos(fine), np.sin(fine) * sign]), jnp.float32)
+    sine = jnp.sin(coarse)
+    return jnp.cos(coarse), jnp.where(places % HEAD < half, -sine, sine), fine
+
+
+def turned(x, cosine, sine, fine, first_block):
     cosines, sines = [], []
     for block in range(x.shape[0] // QB):
-        here = places == first_block + block
-        cosine = jnp.sum(jnp.where(here, coarse[0], 0.0), axis=1, keepdims=True)
-        sine = jnp.sum(jnp.where(here, coarse[1], 0.0), axis=1, keepdims=True)
-        cosines.append(cosine * fine[0] - sine * fine[1])
-        sines.append(sine * fine[0] + cosine * fine[1])
-    cosine, sine = jnp.concatenate(cosines, axis=1), jnp.concatenate(sines, axis=1)
+        c, s = cosine[pl.ds(first_block + block, 1), :], sine[pl.ds(first_block + block, 1), :]
+        cosines.append(c * fine[0] - s * fine[1])
+        sines.append(s * fine[0] + c * fine[1])
     lane = lax.broadcasted_iota(jnp.int32, x.shape, 1)
-    wide_cosine = jnp.concatenate([cosine] * 4, axis=0).T
-    wide_sine = jnp.concatenate([-sine, sine] * 2, axis=0).T
     half = HEAD // 2
     other = jnp.where(lane % HEAD < half, pltpu.roll(x, LANES - half, 1), pltpu.roll(x, half, 1))
-    return x * wide_cosine + other * wide_sine
-
-
-def project(tokens, gain, own, other, coarse, fine, normed_out, q_out, pool_out, weights):
+    return x * jnp.concatenate(cosines, axis=0) + other * jnp.concatenate(sines, axis=0)
+
+
+def project(tokens, gain, own, other, cosine, sine, fine, normed_out, q_out, pool_out, weights):
     core = lax.axis_index("c")
     for place in range(2):
 
@@ -96,32 +93,28 @@
         normed, weights[...], (((1,), (1,)), ((), ())), preferred_element_type=jnp.float32
     )
     first_block = pl.program_id(0) * (ROWS // QB)
-    query = turned(sums[:, :LANES], coarse[...], fine[...], first_block)
+    query = turned(sums[:, :LANES], cosine, sine, fine, first_block)
     q_out[...] = (query * HEAD ** (-0.5)).astype(jnp.bfloat16)
     pool_out[...] = sums[:, LANES:].astype(jnp.bfloat16)
 
 
-def project_kv(normed, pool, ex, coarse, fine, kv_out, send, total):
-    step, rows = pl.program_id(0), normed.shape[0]
-    part = jnp.dot(normed[...], ex[...].reshape(-1, LANES), preferred_element_type=jnp.float32)
-
-    @pl.when(step == 0)
+def project_kv(normed, pool, ex, cosine, sine, fine, kv_out, send):
+    core, step, rows = lax.axis_index("c"), pl.program_id(0), normed.shape[0]
+    sums = jnp.dot(normed[...], ex[...].reshape(-1, LANES), preferred_element_type=jnp.float32)
+    lane = lax.broadcasted_iota(jnp.int32, sums.shape, 1)
+    kv = jnp.where(lane < HEAD, turned(sums, cosine, sine, fine, step * (rows // QB)), sums)
+    kv = kv.astype(jnp.bfloat16)
+    kv_out[...] = kv
+
+    @pl.when((step == 0) & (core == 1))
     def _():
-        total[...] = part
-
-    @pl.when(step > 0)
+        send[:QB] = kv[:QB]
+        send[QB:] = pool[:EDGE]
+
+    @pl.when((step == pl.num_programs(0) - 1) & (core == 0))
     def _():
-        total[...] += part
-
-    @pl.when(step == pl.num_programs(0) - 1)
-    def _():
-        core, sums = lax.axis_index("c"), total[...]
-        lane = lax.broadcasted_iota(jnp.int32, sums.shape, 1)
-        kv = jnp.where(lane < HEAD, turned(sums, coarse[...], fine[...], 0), sums)
-        kv = kv.astype(jnp.bfloat16)
-        kv_out[...] = kv
-        send[:QB] = jnp.where(core == 0, kv[rows - QB :], kv[:QB])
-        send[QB:] = jnp.where(core == 0, pool[rows - EDGE :], pool[:EDGE])
+        send[:QB] = kv[rows - QB :]
+        send[QB:] = pool[rows - EDGE :]
 
 
 def mix(inner, own, other, q, kv, pool, *rest):
@@ -215,14 +208,13 @@
     own = jnp.concatenate([w_query.T, w_pool_in.T, small], axis=0)
     other = lax.ppermute(own, "c", [(0, 1), (1, 0)])
 
-    coarse, fine = rope_tables(lax.axis_index(SP) * rows, rows)
+    cosine, sine, fine = rope_tables(lax.axis_index(SP) * rows, rows)
 
     at = lambda *shape: lambda *place: pl.BlockSpec(shape, lambda i: place)
     whole = lambda *shape: pl.BlockSpec(shape, lambda i: (0,) * len(shape))
     part = lambda *shape: pl.BlockSpec(shape, lambda i: (i,) + (0,) * (len(shape) - 1))
-    along = lambda *shape: pl.BlockSpec(shape, lambda i: (0, i))
     shaped = lambda *shape: jax.ShapeDtypeStruct(shape, bf16)
-    tables = [whole(*coarse.shape), whole(*fine.shape)]
+    tables = [whole(*cosine.shape)] * 2 + [whole(*fine.shape)]
     normed, query, pool_in = pl.pallas_call(
         project,
         grid=(rows // ROWS,),
@@ -232,21 +224,19 @@
         scratch_shapes=[pltpu.VMEM((2 * LANES, depth), bf16)],
         name="project",
         interpret=INTERPRET,
-    )(tokens, norm_gain[None, :], own, other, coarse, fine)
+    )(tokens, norm_gain[None, :], own, other, cosine, sine, fine)
     exchanged, out_piece, normed = lax.optimization_barrier((exchanged, out_piece, normed))
     own_cols = from_everyone(out_piece, SP)
     kv, send = pl.pallas_call(
         project_kv,
-        grid=(STEPS,),
-        in_specs=[along(rows, depth // STEPS), whole(rows, LANES)]
-        + [part(peers // STEPS, pieces, LANES)]
+        grid=(rows // KV_ROWS,),
+        in_specs=[part(KV_ROWS, depth), part(KV_ROWS, LANES), whole(peers, pieces, LANES)]
         + tables,
-        out_specs=[whole(rows, LANES), whole(QB + EDGE, LANES)],
+        out_specs=[part(KV_ROWS, LANES), whole(QB + EDGE, LANES)],
         out_shape=[shaped(rows, LANES), shaped(QB + EDGE, LANES)],
-        scratch_shapes=[pltpu.VMEM((rows, LANES), jnp.float32)],
         name="project_kv",
         interpret=INTERPRET,
-    )(normed, pool_in, exchanged, coarse, fine)
+    )(normed, pool_in, exchanged, cosine, sine, fine)
 
     pairs = [(2 * s, 2 * s + 2) for s in range(sp_count - 1)]
     pairs += [(2 * s + 3, 2 * s + 1) for s in range(sp_count - 1)]

time: 105 us -> 105 us (level)
  waiting for transfers between devices: 18 us -> 19.6 us
  Pallas kernels: 19.9 us -> 18.5 us
    pallas_call x1, Pallas kernels: 5.61 us -> 4.06 us  [body(): pl.pallas_call(project_kv, grid=(rows // KV_ROWS,), in_specs=[part(KV_ROW...]
    ppermute x1, waiting for transfers between devices: 1.47 us -> 2.96 us  [body(): halo = lax.ppermute(send, SP + ('c',), pairs)]
  transfers between devices with their start and end apart: 7 -> 7, of which waited for: 3 -> 3; matrix products, arithmetic and copies ran while one was open for 3% -> 3% of each run, Pallas kernels for 19% -> 18%
where the time goes in v9:
time: 105 us
  starting transfers between devices  46.3 us (44%)
  waiting for transfers between devices  19.6 us (19%)
  Pallas kernels  18.5 us (18%)
  blocking collectives  10.9 us (10%)
  local copies, waits for them, and re-layouts  5.68 us (5%)
  other arithmetic  2.16 us (2%)
    all_to_all x2, starting transfers between devices, from_everyone(): lax.all_to_all(jnp.broadcast_to(x[None], (peers, *x.shape)), axis, 0, 0,...  31 us
    all_to_all x1, waiting for transfers between devices, body(): joined = lax.all_to_all(local, 'x', 0, 0, tiled=True)  14.8 us
    all_to_all x1, blocking collectives, body(): lax.all_to_all(partial_cols, 'x', split_axis=0, concat_axis=1, tiled=True)  10.9 us
    pallas_call x1, Pallas kernels, body(): pl.pallas_call(project, grid=(rows // ROWS,), in_specs=[part(ROWS, depth)...  7.46 us
    pallas_call x2, Pallas kernels, mixed(): pl.pallas_call(functools.partial(mix, inner), grid=(1,), in_specs=local_s...  6.95 us
    ppermute x1, starting transfers between devices, body(): other_cols = lax.ppermute(own_cols, 'c', [(0, 1), (1, 0)])  4.51 us
    pallas_call x1, Pallas kernels, body(): pl.pallas_call(project_kv, grid=(rows // KV_ROWS,), in_specs=[part(KV_ROW...  4.06 us
    all_to_all x1, starting transfers between devices, body(): joined = lax.all_to_all(local, 'x', 0, 0, tiled=True)  3.53 us
  transfers between devices with their start and end apart: 7, of which 3 were waited for; matrix products, arithmetic and copies ran while one was open for 3% of the time, Pallas kernels for 18%

profile of v9, /device:TPU:1, one launch (start us, length us, event | category | flops | bytes accessed | tf_op | source)
XLA Modules:
  0.0 104.7 jit_solution(1074631603896205513)
XLA Ops:
  0.0 0.8 constant_dynamic-slice_fusion
  0.9 0.9 broadcast_in_dim.33
  1.8 17.1 %all-to-all-start = ((bf16[64,32,128]{2,1,0:T(8,128)(2,1)}), bf16[64,32,128]{2,1,0:T(8,128)(2,1)S(1)}, u32[]{:S(2)}, u32[]{:S(2)}) async-start(bf16[64,32,128]{2,1,0:T(8,128)(2,1)} %broadcast_in_dim.33), calls=%async_computation | async-start | bytes 1048576 | tf_op jit(solution)/shard_map/all_to_all | solution.py:28
  19.5 0.7 pad_bitcast_fusion
  20.2 1.1 %pad_maximum_fusion.own = bf16[144,2048]{1,0:T(8,128)(2,1)S(1)} fusion(bf16[16,2048]{1,0:T(8,128)(2,1)S(1)} %fusion.12, bf16[64,2048]{1,0:T(8,128)(2,1)} %bitcast.27, bf16[64,2048]{1,0:T(8,128)(2,1)} %bitcast.28), kind=kLoop, calls=%fused_computation.5 | loop fusion | flops 1769472 | bytes 1179648 | tf_op jit(solution)/shard_map/concatenate | solution.py:208
  21.3 2.9 %collective-permute-start = (bf16[144,2048]{1,0:T(8,128)(2,1)S(1)}, bf16[144,2048]{1,0:T(8,128)(2,1)S(1)}, u32[]{:S(2)}, u32[]{:S(2)}) collective-permute-start(bf16[144,2048]{1,0:T(8,128)(2,1)S(1)} %pad_maximum_fusion.own), channel_id=1, source_target_pairs={{0,1},{1,0},{2,3},{3,2},{4,5},{5,4},{6,7},{7,6},{8,9},{9,8},{10,11... | collective-permute-start | bytes 1769480 | tf_op jit(solution)/shard_map/ppermute | solution.py:209
  24.2 3.1 %collective-permute-start.1 = (bf16[32,128]{1,0:T(8,128)(2,1)S(1)}, bf16[32,128]{1,0:T(8,128)(2,1)S(1)}, u32[]{:S(2)}, u32[]{:S(2)}) collective-permute-start(bf16[32,128]{1,0:T(8,128)(2,1)S(1)} %bitcast.30), channel_id=1, source_target_pairs={{0,0},{1,64},{2,128},{3,192},{4,256},{5,320},{6,384},{7,448},{8,8}... | collective-permute-start | bytes 24584 | tf_op jit(solution)/shard_map/ppermute | solution.py:40
  27.3 0.7 negate_select_fusion
  28.1 0.8 copy-done.1
  28.9 7.5 %project.1 = (bf16[1024,2048]{1,0:T(8,128)(2,1)}, bf16[1024,128]{1,0:T(8,128)(2,1)}, bf16[1024,128]{1,0:T(8,128)(2,1)}) custom-call(bf16[1024,2048]{1,0:T(8,128)(2,1)} %tokens.1, f32[1,2048]{1,0:T(1,128)} %bitcast.29, bf16[144,2048]{1,0:T(8,128)(2,1)} %copy-done, bf16[144,2048]{1,0:T(8,128)(2,1)} %copy-done.1, f32[8,128]{1,0:T(8,128)} %get-tuple-element.32.cosine, ...), custom_call_target="tpu_custom_call" | custom-call | tf_op jit(solution)/shard_map/project/pallas_call | solution.py:218
  36.4 1.0 broadcast_in_dim.34
  37.3 13.9 %all-to-all-start.1 = ((bf16[64,32,128]{2,1,0:T(8,128)(2,1)}), bf16[64,32,128]{2,1,0:T(8,128)(2,1)S(1)}, u32[]{:S(2)}, u32[]{:S(2)}) async-start(bf16[64,32,128]{2,1,0:T(8,128)(2,1)} %broadcast_in_dim.34), calls=%async_computation.1 | async-start | bytes 1048576 | tf_op jit(solution)/shard_map/all_to_all | solution.py:28
  51.2 4.1 %project_kv.1 = (bf16[1024,128]{1,0:T(8,128)(2,1)}, bf16[144,128]{1,0:T(8,128)(2,1)}) custom-call(bf16[1024,2048]{1,0:T(8,128)(2,1)} %get-tuple-element.17.normed, bf16[1024,128]{1,0:T(8,128)(2,1)} %get-tuple-element.18.pool, bf16[64,32,128]{2,1,0:T(8,128)(2,1)} %copy-done.2, f32[8,128]{1,0:T(8,128)} %get-tuple-element.32.cosine, ...), custom_call_target="tpu_custom_call" | custom-call | tf_op jit(solution)/shard_map/project_kv/pallas_call | solution.py:230
  55.3 1.3 %collective-permute-start.2 = (bf16[144,128]{1,0:T(8,128)(2,1)}, bf16[144,128]{1,0:T(8,128)(2,1)S(1)}, u32[]{:S(2)}, u32[]{:S(2)}) collective-permute-start(bf16[144,128]{1,0:T(8,128)(2,1)} %get-tuple-element.21), channel_id=1, source_target_pairs={{0,8},{8,16},{16,24},{24,32},{32,40},{40,48},{48,56},{56,64},{64,7... | collective-permute-start | bytes 110600 | tf_op jit(solution)/shard_map/ppermute | solution.py:243
  56.6 4.2 %mix_inner.1.rest_1_ = bf16[4,512,256]{2,1,0:T(8,128)(2,1)} custom-call(bf16[144,2048]{1,0:T(8,128)(2,1)} %copy-done, bf16[144,2048]{1,0:T(8,128)(2,1)} %copy-done.1, bf16[1024,128]{1,0:T(8,128)(2,1)} %get-tuple-element.15.q, bf16[1024,128]{1,0:T(8,128)(2,1)} %get-tuple-element.20.kv, bf16[1024,128]{1,0:T(8,128)(2,1)} %get-tuple-element.18.pool), custom_call_target="tpu_custom_call" | custom-call | tf_op jit(solution)/shard_map/mix_inner/pallas_call | solution.py:251
  60.8 3.0 %collective-permute-done.2.rest_0_ = bf16[144,128]{1,0:T(8,128)(2,1)S(1)} collective-permute-done((bf16[144,128]{1,0:T(8,128)(2,1)}, bf16[144,128]{1,0:T(8,128)(2,1)S(1)}, u32[]{:S(2)}, u32[]{:S(2)}) %collective-permute-start.2) | collective-permute-done | bytes 36896 | tf_op jit(solution)/shard_map/ppermute | solution.py:243
  64.4 2.7 %mix_outer.1 = bf16[4,512,256]{2,1,0:T(8,128)(2,1)} custom-call(bf16[144,2048]{1,0:T(8,128)(2,1)} %copy-done, bf16[144,2048]{1,0:T(8,128)(2,1)} %copy-done.1, bf16[1024,128]{1,0:T(8,128)(2,1)} %get-tuple-element.15.q, bf16[1024,128]{1,0:T(8,128)(2,1)} %get-tuple-element.20.kv, ...), custom_call_target="tpu_custom_call", output_to_operand_aliasing={{}: (6, {})} | custom-call | tf_op jit(solution)/shard_map/mix_outer/pallas_call | solution.py:251
  67.1 1.8 %all-to-all-done.1 = bf16[64,32,128]{2,1,0:T(8,128)(2,1)S(1)} async-done(((bf16[64,32,128]{2,1,0:T(8,128)(2,1)}), bf16[64,32,128]{2,1,0:T(8,128)(2,1)S(1)}, u32[]{:S(2)}, u32[]{:S(2)}) %all-to-all-start.1) | async-done | bytes 524320 | tf_op jit(solution)/shard_map/all_to_all | solution.py:28
  68.9 4.5 %collective-permute-start.3 = (bf16[64,32,128]{2,1,0:T(8,128)(2,1)S(1)}, bf16[64,32,128]{2,1,0:T(8,128)(2,1)S(1)}, u32[]{:S(2)}, u32[]{:S(2)}) collective-permute-start(bf16[64,32,128]{2,1,0:T(8,128)(2,1)S(1)} %all-to-all-done.1), channel_id=1, source_target_pairs={{0,1},{1,0},{2,3},{3,2},{4,5},{5,4},{6,7},{7,6},{8,9},{9,8},{10,11... | collective-permute-start | bytes 1572872 | tf_op jit(solution)/shard_map/ppermute | solution.py:272
  73.4 3.5 %all-to-all-start.2 = ((bf16[4,512,256]{2,1,0:T(8,128)(2,1)}), bf16[4,512,256]{2,1,0:T(8,128)(2,1)S(1)}, u32[]{:S(2)}, u32[]{:S(2)}) async-start(bf16[4,512,256]{2,1,0:T(8,128)(2,1)} %mix_outer.1), calls=%async_computation.2 | async-start | bytes 2097152 | tf_op jit(solution)/shard_map/all_to_all | solution.py:273
  77.3 14.8 %all-to-all-done.2 = bf16[4,512,256]{2,1,0:T(8,128)(2,1)S(1)} async-done(((bf16[4,512,256]{2,1,0:T(8,128)(2,1)}), bf16[4,512,256]{2,1,0:T(8,128)(2,1)S(1)}, u32[]{:S(2)}, u32[]{:S(2)}) %all-to-all-start.2) | async-done | bytes 1048608 | tf_op jit(solution)/shard_map/all_to_all | solution.py:273
  92.1 0.7 fusion
  92.9 10.9 %all_to_all.34 = bf16[4,128,512]{2,1,0:T(8,128)(2,1)S(1)} all-to-all(bf16[4,128,512]{2,1,0:T(8,128)(2,1)S(1)} %bitcast.26), channel_id=1, replica_groups=mesh['z'=8,'y'=8,'x'=4,'c'=2] {'x'}, dimensions={0} | all-to-all | bytes 1048576 | tf_op jit(solution)/shard_map/all_to_all | solution.py:287
  103.8 0.8 copy.13
  (22 shorter events, 1.1 us)
Async XLA Ops:
  0.0 24.2 %copy-start.4 = (bf16[128,32]{0,1:T(8,128)(2,1)S(1)}, bf16[128,32]{0,1:T(8,128)(2,1)}, u32[]{:S(2)}) copy-start(bf16[128,32]{0,1:T(8,128)(2,1)} %param.18) | copy-start | bytes 24580
  1.8 34.6 %all-to-all-start = ((bf16[64,32,128]{2,1,0:T(8,128)(2,1)}), bf16[64,32,128]{2,1,0:T(8,128)(2,1)S(1)}, u32[]{:S(2)}, u32[]{:S(2)}) async-start(bf16[64,32,128]{2,1,0:T(8,128)(2,1)} %broadcast_in_dim.33), calls=%async_computation | async-start | bytes 1048576 | tf_op jit(solution)/shard_map/all_to_all | solution.py:28
  21.3 6.8 %copy-start = (bf16[144,2048]{1,0:T(8,128)(2,1)}, bf16[144,2048]{1,0:T(8,128)(2,1)S(1)}, u32[]{:S(2)}) copy-start(bf16[144,2048]{1,0:T(8,128)(2,1)S(1)} %pad_maximum_fusion.own) | copy-start | bytes 1769476
  21.3 6.7 %collective-permute-start = (bf16[144,2048]{1,0:T(8,128)(2,1)S(1)}, bf16[144,2048]{1,0:T(8,128)(2,1)S(1)}, u32[]{:S(2)}, u32[]{:S(2)}) collective-permute-start(bf16[144,2048]{1,0:T(8,128)(2,1)S(1)} %pad_maximum_fusion.own), channel_id=1, source_target_pairs={{0,1},{1,0},{2,3},{3,2},{4,5},{5,4},{6,7},{7,6},{8,9},{9,8},{10,11... | collective-permute-start | bytes 1769480 | tf_op jit(solution)/shard_map/ppermute | solution.py:209
  24.2 12.2 %collective-permute-start.1 = (bf16[32,128]{1,0:T(8,128)(2,1)S(1)}, bf16[32,128]{1,0:T(8,128)(2,1)S(1)}, u32[]{:S(2)}, u32[]{:S(2)}) collective-permute-start(bf16[32,128]{1,0:T(8,128)(2,1)S(1)} %bitcast.30), channel_id=1, source_target_pairs={{0,0},{1,64},{2,128},{3,192},{4,256},{5,320},{6,384},{7,448},{8,8}... | collective-permute-start | bytes 24584 | tf_op jit(solution)/shard_map/ppermute | solution.py:40
  28.0 0.8 copy-start.1
  36.4 14.8 %copy-start.2 = (bf16[64,32,128]{2,1,0:T(8,128)(2,1)}, bf16[64,32,128]{2,1,0:T(8,128)(2,1)S(1)}, u32[]{:S(2)}) copy-start(bf16[64,32,128]{2,1,0:T(8,128)(2,1)S(1)} %all-to-all-done.ex) | copy-start | bytes 1572868
  37.3 31.6 %all-to-all-start.1 = ((bf16[64,32,128]{2,1,0:T(8,128)(2,1)}), bf16[64,32,128]{2,1,0:T(8,128)(2,1)S(1)}, u32[]{:S(2)}, u32[]{:S(2)}) async-start(bf16[64,32,128]{2,1,0:T(8,128)(2,1)} %broadcast_in_dim.34), calls=%async_computation.1 | async-start | bytes 1048576 | tf_op jit(solution)/shard_map/all_to_all | solution.py:28
  55.3 8.5 %collective-permute-start.2 = (bf16[144,128]{1,0:T(8,128)(2,1)}, bf16[144,128]{1,0:T(8,128)(2,1)S(1)}, u32[]{:S(2)}, u32[]{:S(2)}) collective-permute-start(bf16[144,128]{1,0:T(8,128)(2,1)} %get-tuple-element.21), channel_id=1, source_target_pairs={{0,8},{8,16},{16,24},{24,32},{32,40},{40,48},{48,56},{56,64},{64,7... | collective-permute-start | bytes 110600 | tf_op jit(solution)/shard_map/ppermute | solution.py:243
  63.7 0.6 copy-start.3
  68.9 8.1 %collective-permute-start.3 = (bf16[64,32,128]{2,1,0:T(8,128)(2,1)S(1)}, bf16[64,32,128]{2,1,0:T(8,128)(2,1)S(1)}, u32[]{:S(2)}, u32[]{:S(2)}) collective-permute-start(bf16[64,32,128]{2,1,0:T(8,128)(2,1)S(1)} %all-to-all-done.1), channel_id=1, source_target_pairs={{0,1},{1,0},{2,3},{3,2},{4,5},{5,4},{6,7},{7,6},{8,9},{9,8},{10,11... | collective-permute-start | bytes 1572872 | tf_op jit(solution)/shard_map/ppermute | solution.py:272
  73.4 18.7 %all-to-all-start.2 = ((bf16[4,512,256]{2,1,0:T(8,128)(2,1)}), bf16[4,512,256]{2,1,0:T(8,128)(2,1)S(1)}, u32[]{:S(2)}, u32[]{:S(2)}) async-start(bf16[4,512,256]{2,1,0:T(8,128)(2,1)} %mix_outer.1), calls=%async_computation.2 | async-start | bytes 2097152 | tf_op jit(solution)/shard_map/all_to_all | solution.py:273

commit v10 on v9

--- a/solution.py
+++ b/solution.py
@@ -14,7 +14,6 @@
 QB = 128
 LANES = 128
 ROWS = 256
-KV_ROWS = 512
 EDGE = 16
 POOL_SPANS = (2, 4, 8, 16)
 NEG_BIG = -1e30
@@ -73,7 +72,7 @@
     return x * jnp.concatenate(cosines, axis=0) + other * jnp.concatenate(sines, axis=0)
 
 
-def project(tokens, gain, own, other, cosine, sine, fine, normed_out, q_out, pool_out, weights):
+def project(tokens, gain, own, other, cosine, sine, fine, kept, sent, q_out, pool_out, weights):
     core = lax.axis_index("c")
     for place in range(2):
 
@@ -88,7 +87,16 @@
     values = values - center
     spread = jnp.mean(values * values, axis=-1, keepdims=True)
     normed = (values * lax.rsqrt(spread + 1e-06) * gain[...]).astype(jnp.bfloat16)
-    normed_out[...] = normed
+    step, half = pl.program_id(0), pl.num_programs(0) // 2
+
+    @pl.when(step < half)
+    def _():
+        kept[pl.ds(pl.multiple_of(step * ROWS, ROWS), ROWS), :] = normed
+
+    @pl.when(step >= half)
+    def _():
+        sent[...] = normed
+
     sums = lax.dot_general(
         normed, weights[...], (((1,), (1,)), ((), ())), preferred_element_type=jnp.float32
     )
@@ -98,23 +106,25 @@
     pool_out[...] = sums[:, LANES:].astype(jnp.bfloat16)
 
 
-def project_kv(normed, pool, ex, cosine, sine, fine, kv_out, send):
-    core, step, rows = lax.axis_index("c"), pl.program_id(0), normed.shape[0]
-    sums = jnp.dot(normed[...], ex[...].reshape(-1, LANES), preferred_element_type=jnp.float32)
-    lane = lax.broadcasted_iota(jnp.int32, sums.shape, 1)
-    kv = jnp.where(lane < HEAD, turned(sums, cosine, sine, fine, step * (rows // QB)), sums)
-    kv = kv.astype(jnp.bfloat16)
-    kv_out[...] = kv
-
-    @pl.when((step == 0) & (core == 1))
-    def _():
-        send[:QB] = kv[:QB]
-        send[QB:] = pool[:EDGE]
-
-    @pl.when((step == pl.num_programs(0) - 1) & (core == 0))
-    def _():
-        send[:QB] = kv[rows - QB :]
-        send[QB:] = pool[rows - EDGE :]
+def project_kv(kept, sent, pool, ex, cosine, sine, fine, kv_out, send, landed, sem):
+    core, rows = lax.axis_index("c"), kept.shape[0]
+    copy = pltpu.make_async_copy(sent, landed, sem)
+    copy.start()
+    weights = ex[...].reshape(-1, LANES)
+
+    def product(normed, first_block):
+        sums = jnp.dot(normed, weights, preferred_element_type=jnp.float32)
+        lane = lax.broadcasted_iota(jnp.int32, sums.shape, 1)
+        kv = jnp.where(lane < HEAD, turned(sums, cosine, sine, fine, first_block), sums)
+        return kv.astype(jnp.bfloat16)
+
+    lower = product(kept[...], 0)
+    kv_out[:rows] = lower
+    copy.wait()
+    upper = product(landed[...], rows // QB)
+    kv_out[rows:] = upper
+    send[:QB] = jnp.where(core == 0, upper[rows - QB :], lower[:QB])
+    send[QB:] = jnp.where(core == 0, pool[2 * rows - EDGE :], pool[:EDGE])
 
 
 def mix(inner, own, other, q, kv, pool, *rest):
@@ -215,28 +225,40 @@
     part = lambda *shape: pl.BlockSpec(shape, lambda i: (i,) + (0,) * (len(shape) - 1))
     shaped = lambda *shape: jax.ShapeDtypeStruct(shape, bf16)
     tables = [whole(*cosine.shape)] * 2 + [whole(*fine.shape)]
-    normed, query, pool_in = pl.pallas_call(
+    on_chip = shaped(rows // 2, depth) if INTERPRET else pltpu.VMEM((rows // 2, depth), bf16)
+    kept, sent, query, pool_in = pl.pallas_call(
         project,
         grid=(rows // ROWS,),
         in_specs=[part(ROWS, depth), whole(1, depth)] + [whole(*own.shape)] * 2 + tables,
-        out_specs=[part(ROWS, depth), part(ROWS, LANES), part(ROWS, LANES)],
-        out_shape=[shaped(rows, depth), shaped(rows, LANES), shaped(rows, LANES)],
+        out_specs=[
+            pl.BlockSpec(memory_space=pltpu.VMEM),
+            pl.BlockSpec((ROWS, depth), lambda i: (jnp.maximum(i - rows // ROWS // 2, 0), 0)),
+            part(ROWS, LANES),
+            part(ROWS, LANES),
+        ],
+        out_shape=[on_chip, shaped(rows // 2, depth), shaped(rows, LANES), shaped(rows, LANES)],
         scratch_shapes=[pltpu.VMEM((2 * LANES, depth), bf16)],
         name="project",
         interpret=INTERPRET,
     )(tokens, norm_gain[None, :], own, other, cosine, sine, fine)
-    exchanged, out_piece, normed = lax.optimization_barrier((exchanged, out_piece, normed))
+    exchanged, out_piece, sent = lax.optimization_barrier((exchanged, out_piece, sent))
     own_cols = from_everyone(out_piece, SP)
     kv, send = pl.pallas_call(
         project_kv,
-        grid=(rows // KV_ROWS,),
-        in_specs=[part(KV_ROWS, depth), part(KV_ROWS, LANES), whole(peers, pieces, LANES)]
+        grid=(1,),
+        in_specs=[
+            pl.BlockSpec(memory_space=pltpu.VMEM),
+            pl.BlockSpec(memory_space=pl.ANY),
+            whole(rows, LANES),
+            whole(peers, pieces, LANES),
+        ]
         + tables,
-        out_specs=[part(KV_ROWS, LANES), whole(QB + EDGE, LANES)],
+        out_specs=[whole(rows, LANES), whole(QB + EDGE, LANES)],
         out_shape=[shaped(rows, LANES), shaped(QB + EDGE, LANES)],
+        scratch_shapes=[pltpu.VMEM((rows // 2, depth), bf16), pltpu.SemaphoreType.DMA],
         name="project_kv",
         interpret=INTERPRET,
-    )(normed, pool_in, exchanged, cosine, sine, fine)
+    )(kept, sent, pool_in, exchanged, cosine, sine, fine)
 
     pairs = [(2 * s, 2 * s + 2) for s in range(sp_count - 1)]
     pairs += [(2 * s + 3, 2 * s + 1) for s in range(sp_count - 1)]

time: 105 us -> 107 us (1.019)
  Pallas kernels: 18.5 us -> 20.4 us
  waiting for transfers between devices: 19.6 us -> 18.2 us
  local copies, waits for them, and re-layouts: 5.68 us -> 6.86 us
    pallas_call x1, Pallas kernels: 4.06 us -> 5.42 us  [body(): pl.pallas_call(project_kv, grid=(1,), in_specs=[pl.BlockSpec(memory_space...]
    ppermute x1, waiting for transfers between devices: 2.96 us -> 1.61 us  [body(): halo = lax.ppermute(send, SP + ('c',), pairs)]
    unnamed x10, local copies, waits for them, and re-layouts: 1.47 us -> 2.75 us
  transfers between devices with their start and end apart: 7 -> 7, of which waited for: 3 -> 3; matrix products, arithmetic and copies ran while one was open for 3% -> 3% of each run, Pallas kernels for 18% -> 19%
where the time goes in v10:
time: 107 us
  starting transfers between devices  46.4 us (43%)
  Pallas kernels  20.4 us (19%)
  waiting for transfers between devices  18.2 us (17%)
  blocking collectives  11 us (10%)
  local copies, waits for them, and re-layouts  6.86 us (6%)
  other arithmetic  2.16 us (2%)
    all_to_all x2, starting transfers between devices, from_everyone(): lax.all_to_all(jnp.broadcast_to(x[None], (peers, *x.shape)), axis, 0, 0,...  31.2 us
    all_to_all x1, waiting for transfers between devices, body(): joined = lax.all_to_all(local, 'x', 0, 0, tiled=True)  14.8 us
    all_to_all x1, blocking collectives, body(): lax.all_to_all(partial_cols, 'x', split_axis=0, concat_axis=1, tiled=True)  11 us
    pallas_call x1, Pallas kernels, body(): pl.pallas_call(project, grid=(rows // ROWS,), in_specs=[part(ROWS, depth)...  8.04 us
    pallas_call x2, Pallas kernels, mixed(): pl.pallas_call(functools.partial(mix, inner), grid=(1,), in_specs=local_s...  6.95 us
    pallas_call x1, Pallas kernels, body(): pl.pallas_call(project_kv, grid=(1,), in_specs=[pl.BlockSpec(memory_space...  5.42 us
    ppermute x1, starting transfers between devices, body(): other_cols = lax.ppermute(own_cols, 'c', [(0, 1), (1, 0)])  4.42 us
    all_to_all x1, starting transfers between devices, body(): joined = lax.all_to_all(local, 'x', 0, 0, tiled=True)  3.53 us
  transfers between devices with their start and end apart: 7, of which 3 were waited for; matrix products, arithmetic and copies ran while one was open for 3% of the time, Pallas kernels for 19%

profile of v10, /device:TPU:1, one launch (start us, length us, event | category | flops | bytes accessed | tf_op | source)
XLA Modules:
  0.0 106.5 jit_solution(11379804184938910033)
XLA Ops:
  0.0 0.8 constant_dynamic-slice_fusion
  0.9 0.9 broadcast_in_dim.33
  1.8 17.4 %all-to-all-start = ((bf16[64,32,128]{2,1,0:T(8,128)(2,1)}), bf16[64,32,128]{2,1,0:T(8,128)(2,1)}, u32[]{:S(2)}, u32[]{:S(2)}) async-start(bf16[64,32,128]{2,1,0:T(8,128)(2,1)} %broadcast_in_dim.33), calls=%async_computation | async-start | bytes 1048576 | tf_op jit(solution)/shard_map/all_to_all | solution.py:27
  20.5 1.1 %pad_maximum_fusion.own = bf16[144,2048]{1,0:T(8,128)(2,1)S(1)} fusion(bf16[16,2048]{1,0:T(8,128)(2,1)S(1)} %fusion.12, bf16[64,2048]{1,0:T(8,128)(2,1)} %bitcast.27, bf16[64,2048]{1,0:T(8,128)(2,1)} %bitcast.28), kind=kLoop, calls=%fused_computation.5 | loop fusion | flops 1769472 | bytes 1179648 | tf_op jit(solution)/shard_map/concatenate | solution.py:218
  21.6 2.9 %collective-permute-start = (bf16[144,2048]{1,0:T(8,128)(2,1)S(1)}, bf16[144,2048]{1,0:T(8,128)(2,1)S(1)}, u32[]{:S(2)}, u32[]{:S(2)}) collective-permute-start(bf16[144,2048]{1,0:T(8,128)(2,1)S(1)} %pad_maximum_fusion.own), channel_id=1, source_target_pairs={{0,1},{1,0},{2,3},{3,2},{4,5},{5,4},{6,7},{7,6},{8,9},{9,8},{10,11... | collective-permute-start | bytes 1769480 | tf_op jit(solution)/shard_map/ppermute | solution.py:219
  24.4 3.0 %collective-permute-start.1 = (bf16[32,128]{1,0:T(8,128)(2,1)S(1)}, bf16[32,128]{1,0:T(8,128)(2,1)S(1)}, u32[]{:S(2)}, u32[]{:S(2)}) collective-permute-start(bf16[32,128]{1,0:T(8,128)(2,1)S(1)} %bitcast.30), channel_id=1, source_target_pairs={{0,0},{1,64},{2,128},{3,192},{4,256},{5,320},{6,384},{7,448},{8,8}... | collective-permute-start | bytes 24584 | tf_op jit(solution)/shard_map/ppermute | solution.py:39
  27.5 0.7 negate_select_fusion
  28.2 0.8 copy-done.2
  29.1 8.0 %project.1 = (bf16[512,2048]{1,0:T(8,128)(2,1)S(1)}, bf16[512,2048]{1,0:T(8,128)(2,1)}, bf16[1024,128]{1,0:T(8,128)(2,1)}, bf16[1024,128]{1,0:T(8,128)(2,1)}) custom-call(bf16[1024,2048]{1,0:T(8,128)(2,1)} %tokens.1, f32[1,2048]{1,0:T(1,128)} %bitcast.29, bf16[144,2048]{1,0:T(8,128)(2,1)} %copy-done.1, bf16[144,2048]{1,0:T(8,128)(2,1)} %copy-done.2, ...), custom_call_target="tpu_custom_call" | custom-call | tf_op jit(solution)/shard_map/project/pallas_call | solution.py:229
  37.1 1.3 %copy-done = bf16[512,2048]{1,0:T(8,128)(2,1)} copy-done((bf16[512,2048]{1,0:T(8,128)(2,1)}, bf16[512,2048]{1,0:T(8,128)(2,1)S(1)}, u32[]{:S(2)}) %copy-start) | copy-done | bytes 2097176
  38.4 0.9 broadcast_in_dim.34
  39.3 13.8 %all-to-all-start.1 = ((bf16[64,32,128]{2,1,0:T(8,128)(2,1)}), bf16[64,32,128]{2,1,0:T(8,128)(2,1)S(1)}, u32[]{:S(2)}, u32[]{:S(2)}) async-start(bf16[64,32,128]{2,1,0:T(8,128)(2,1)} %broadcast_in_dim.34), calls=%async_computation.1 | async-start | bytes 1048576 | tf_op jit(solution)/shard_map/all_to_all | solution.py:27
  53.1 5.4 %project_kv.1 = (bf16[1024,128]{1,0:T(8,128)(2,1)}, bf16[144,128]{1,0:T(8,128)(2,1)}) custom-call(bf16[512,2048]{1,0:T(8,128)(2,1)} %copy-done, bf16[512,2048]{1,0:T(8,128)(2,1)} %get-tuple-element.19.sent, bf16[1024,128]{1,0:T(8,128)(2,1)} %get-tuple-element.20.pool, bf16[64,32,128]{2,1,0:T(8,128)(2,1)} %all-to-all-done.ex, ...), custom_call_target="tpu_custom_call" | custom-call | tf_op jit(solution)/shard_map/project_kv/pallas_call | solution.py:246
  58.6 1.3 %collective-permute-start.2 = (bf16[144,128]{1,0:T(8,128)(2,1)}, bf16[144,128]{1,0:T(8,128)(2,1)S(1)}, u32[]{:S(2)}, u32[]{:S(2)}) collective-permute-start(bf16[144,128]{1,0:T(8,128)(2,1)} %get-tuple-element.23), channel_id=1, source_target_pairs={{0,8},{8,16},{16,24},{24,32},{32,40},{40,48},{48,56},{56,64},{64,7... | collective-permute-start | bytes 110600 | tf_op jit(solution)/shard_map/ppermute | solution.py:265
  59.9 4.2 %mix_inner.1.rest_1_ = bf16[4,512,256]{2,1,0:T(8,128)(2,1)} custom-call(bf16[144,2048]{1,0:T(8,128)(2,1)} %copy-done.1, bf16[144,2048]{1,0:T(8,128)(2,1)} %copy-done.2, bf16[1024,128]{1,0:T(8,128)(2,1)} %get-tuple-element.16.q, bf16[1024,128]{1,0:T(8,128)(2,1)} %get-tuple-element.22.kv, bf16[1024,128]{1,0:T(8,128)(2,1)} %get-tuple-element.20.pool), custom_call_target="tpu_custom_call" | custom-call | tf_op jit(solution)/shard_map/mix_inner/pallas_call | solution.py:273
  64.1 1.6 %collective-permute-done.2.rest_0_ = bf16[144,128]{1,0:T(8,128)(2,1)S(1)} collective-permute-done((bf16[144,128]{1,0:T(8,128)(2,1)}, bf16[144,128]{1,0:T(8,128)(2,1)S(1)}, u32[]{:S(2)}, u32[]{:S(2)}) %collective-permute-start.2) | collective-permute-done | bytes 36896 | tf_op jit(solution)/shard_map/ppermute | solution.py:265
  66.3 2.7 %mix_outer.1 = bf16[4,512,256]{2,1,0:T(8,128)(2,1)} custom-call(bf16[144,2048]{1,0:T(8,128)(2,1)} %copy-done.1, bf16[144,2048]{1,0:T(8,128)(2,1)} %copy-done.2, bf16[1024,128]{1,0:T(8,128)(2,1)} %get-tuple-element.16.q, bf16[1024,128]{1,0:T(8,128)(2,1)} %get-tuple-element.22.kv, ...), custom_call_target="tpu_custom_call", output_to_operand_aliasing={{}: (6, {})} | custom-call | tf_op jit(solution)/shard_map/mix_outer/pallas_call | solution.py:273
  69.0 1.8 %all-to-all-done.1 = bf16[64,32,128]{2,1,0:T(8,128)(2,1)S(1)} async-done(((bf16[64,32,128]{2,1,0:T(8,128)(2,1)}), bf16[64,32,128]{2,1,0:T(8,128)(2,1)S(1)}, u32[]{:S(2)}, u32[]{:S(2)}) %all-to-all-start.1) | async-done | bytes 524320 | tf_op jit(solution)/shard_map/all_to_all | solution.py:27
  70.9 4.4 %collective-permute-start.3 = (bf16[64,32,128]{2,1,0:T(8,128)(2,1)S(1)}, bf16[64,32,128]{2,1,0:T(8,128)(2,1)S(1)}, u32[]{:S(2)}, u32[]{:S(2)}) collective-permute-start(bf16[64,32,128]{2,1,0:T(8,128)(2,1)S(1)} %all-to-all-done.1), channel_id=1, source_target_pairs={{0,1},{1,0},{2,3},{3,2},{4,5},{5,4},{6,7},{7,6},{8,9},{9,8},{10,11... | collective-permute-start | bytes 1572872 | tf_op jit(solution)/shard_map/ppermute | solution.py:294
  75.3 3.5 %all-to-all-start.2 = ((bf16[4,512,256]{2,1,0:T(8,128)(2,1)}), bf16[4,512,256]{2,1,0:T(8,128)(2,1)S(1)}, u32[]{:S(2)}, u32[]{:S(2)}) async-start(bf16[4,512,256]{2,1,0:T(8,128)(2,1)} %mix_outer.1), calls=%async_computation.2 | async-start | bytes 2097152 | tf_op jit(solution)/shard_map/all_to_all | solution.py:295
  79.2 14.8 %all-to-all-done.2 = bf16[4,512,256]{2,1,0:T(8,128)(2,1)S(1)} async-done(((bf16[4,512,256]{2,1,0:T(8,128)(2,1)}), bf16[4,512,256]{2,1,0:T(8,128)(2,1)S(1)}, u32[]{:S(2)}, u32[]{:S(2)}) %all-to-all-start.2) | async-done | bytes 1048608 | tf_op jit(solution)/shard_map/all_to_all | solution.py:295
  94.0 0.7 fusion
  94.7 11.0 %all_to_all.34 = bf16[4,128,512]{2,1,0:T(8,128)(2,1)S(1)} all-to-all(bf16[4,128,512]{2,1,0:T(8,128)(2,1)S(1)} %bitcast.26), channel_id=1, replica_groups=mesh['z'=8,'y'=8,'x'=4,'c'=2] {'x'}, dimensions={0} | all-to-all | bytes 1048576 | tf_op jit(solution)/shard_map/all_to_all | solution.py:309
  105.7 0.8 copy.13
  (22 shorter events, 1.7 us)
Async XLA Ops:
  0.0 24.4 %copy-start.4 = (bf16[128,32]{0,1:T(8,128)(2,1)S(1)}, bf16[128,32]{0,1:T(8,128)(2,1)}, u32[]{:S(2)}) copy-start(bf16[128,32]{0,1:T(8,128)(2,1)} %param.18) | copy-start | bytes 24580
  1.8 36.7 %all-to-all-start = ((bf16[64,32,128]{2,1,0:T(8,128)(2,1)}), bf16[64,32,128]{2,1,0:T(8,128)(2,1)}, u32[]{:S(2)}, u32[]{:S(2)}) async-start(bf16[64,32,128]{2,1,0:T(8,128)(2,1)} %broadcast_in_dim.33), calls=%async_computation | async-start | bytes 1048576 | tf_op jit(solution)/shard_map/all_to_all | solution.py:27
  21.6 6.7 %copy-start.1 = (bf16[144,2048]{1,0:T(8,128)(2,1)}, bf16[144,2048]{1,0:T(8,128)(2,1)S(1)}, u32[]{:S(2)}) copy-start(bf16[144,2048]{1,0:T(8,128)(2,1)S(1)} %pad_maximum_fusion.own) | copy-start | bytes 1769476
  21.6 6.7 %collective-permute-start = (bf16[144,2048]{1,0:T(8,128)(2,1)S(1)}, bf16[144,2048]{1,0:T(8,128)(2,1)S(1)}, u32[]{:S(2)}, u32[]{:S(2)}) collective-permute-start(bf16[144,2048]{1,0:T(8,128)(2,1)S(1)} %pad_maximum_fusion.own), channel_id=1, source_target_pairs={{0,1},{1,0},{2,3},{3,2},{4,5},{5,4},{6,7},{7,6},{8,9},{9,8},{10,11... | collective-permute-start | bytes 1769480 | tf_op jit(solution)/shard_map/ppermute | solution.py:219
  24.4 14.0 %collective-permute-start.1 = (bf16[32,128]{1,0:T(8,128)(2,1)S(1)}, bf16[32,128]{1,0:T(8,128)(2,1)S(1)}, u32[]{:S(2)}, u32[]{:S(2)}) collective-permute-start(bf16[32,128]{1,0:T(8,128)(2,1)S(1)} %bitcast.30), channel_id=1, source_target_pairs={{0,0},{1,64},{2,128},{3,192},{4,256},{5,320},{6,384},{7,448},{8,8}... | collective-permute-start | bytes 24584 | tf_op jit(solution)/shard_map/ppermute | solution.py:39
  28.2 0.8 copy-start.2
  37.1 1.3 %copy-start = (bf16[512,2048]{1,0:T(8,128)(2,1)}, bf16[512,2048]{1,0:T(8,128)(2,1)S(1)}, u32[]{:S(2)}) copy-start(bf16[512,2048]{1,0:T(8,128)(2,1)S(1)} %get-tuple-element.17.kept) | copy-start | bytes 6291460
  39.3 31.6 %all-to-all-start.1 = ((bf16[64,32,128]{2,1,0:T(8,128)(2,1)}), bf16[64,32,128]{2,1,0:T(8,128)(2,1)S(1)}, u32[]{:S(2)}, u32[]{:S(2)}) async-start(bf16[64,32,128]{2,1,0:T(8,128)(2,1)} %broadcast_in_dim.34), calls=%async_computation.1 | async-start | bytes 1048576 | tf_op jit(solution)/shard_map/all_to_all | solution.py:27
  58.6 7.1 %collective-permute-start.2 = (bf16[144,128]{1,0:T(8,128)(2,1)}, bf16[144,128]{1,0:T(8,128)(2,1)S(1)}, u32[]{:S(2)}, u32[]{:S(2)}) collective-permute-start(bf16[144,128]{1,0:T(8,128)(2,1)} %get-tuple-element.23), channel_id=1, source_target_pairs={{0,8},{8,16},{16,24},{24,32},{32,40},{40,48},{48,56},{56,64},{64,7... | collective-permute-start | bytes 110600 | tf_op jit(solution)/shard_map/ppermute | solution.py:265
  65.7 0.6 copy-start.3
  70.9 8.0 %collective-permute-start.3 = (bf16[64,32,128]{2,1,0:T(8,128)(2,1)S(1)}, bf16[64,32,128]{2,1,0:T(8,128)(2,1)S(1)}, u32[]{:S(2)}, u32[]{:S(2)}) collective-permute-start(bf16[64,32,128]{2,1,0:T(8,128)(2,1)S(1)} %all-to-all-done.1), channel_id=1, source_target_pairs={{0,1},{1,0},{2,3},{3,2},{4,5},{5,4},{6,7},{7,6},{8,9},{9,8},{10,11... | collective-permute-start | bytes 1572872 | tf_op jit(solution)/shard_map/ppermute | solution.py:294
  75.3 18.7 %all-to-all-start.2 = ((bf16[4,512,256]{2,1,0:T(8,128)(2,1)}), bf16[4,512,256]{2,1,0:T(8,128)(2,1)S(1)}, u32[]{:S(2)}, u32[]{:S(2)}) async-start(bf16[4,512,256]{2,1,0:T(8,128)(2,1)} %mix_outer.1), calls=%async_computation.2 | async-start | bytes 2097152 | tf_op jit(solution)/shard_map/all_to_all | solution.py:295

commit v11 on v9

--- a/solution.py
+++ b/solution.py
@@ -40,6 +40,10 @@
     return lax.ppermute(piece, SP + TP, pairs)
 
 
+def on_chip(x):
+    return x if INTERPRET else pltpu.with_memory_space_constraint(x, pltpu.VMEM)
+
+
 def three_parts(x):
     high = lax.reduce_precision(x, 8, 7)
     middle = lax.reduce_precision(x - high, 8, 7)
@@ -73,7 +77,7 @@
     return x * jnp.concatenate(cosines, axis=0) + other * jnp.concatenate(sines, axis=0)
 
 
-def project(tokens, gain, own, other, cosine, sine, fine, normed_out, q_out, pool_out, weights):
+def project(tokens, gain, own, other, cosine, sine, fine, normed_out, q_out, pool_out, parts, weights):
     core = lax.axis_index("c")
     for place in range(2):
 
@@ -82,6 +86,7 @@
             for source, head in ((own, place), (other, 1 - place)):
                 weights[head * HEAD : (head + 1) * HEAD] = source[:HEAD]
                 weights[LANES + head * HEAD : LANES + (head + 1) * HEAD] = source[HEAD:LANES]
+                parts[head * EDGE : (head + 1) * EDGE] = source[LANES:, :LANES]
 
     values = tokens[...].astype(jnp.float32)
     center = jnp.mean(values, axis=-1, keepdims=True)
@@ -117,16 +122,14 @@
         send[QB:] = pool[rows - EDGE :]
 
 
-def mix(inner, own, other, q, kv, pool, *rest):
+def mix(inner, parts, q, kv, pool, *rest):
     out, kv_wide, pool_wide, both, sems = rest[-5:]
     core, group = lax.axis_index("c"), lax.axis_index("x")
     rows = q.shape[0]
     blocks_total = lax.axis_size(SP) * (rows // QB)
     first_block = lax.axis_index(SP) * (rows // QB)
-    mine = jnp.sum(own[:3, :LANES].astype(jnp.float32), axis=0, keepdims=True)
-    theirs = jnp.sum(other[:3, :LANES].astype(jnp.float32), axis=0, keepdims=True)
-    first = jnp.where(core == 0, mine, theirs)
-    second = jnp.where(core == 0, theirs, mine)
+    first = jnp.sum(parts[:3].astype(jnp.float32), axis=0, keepdims=True)
+    second = jnp.sum(parts[EDGE : EDGE + 3].astype(jnp.float32), axis=0, keepdims=True)
     scale = jnp.concatenate([first[:, :HEAD], second[:, :HEAD]], axis=1)
     kv_wide[pl.ds(pl.multiple_of((1 - core) * QB, QB), rows), :] = kv[...]
     pool_wide[EDGE : EDGE + rows, :] = pool[...].astype(jnp.float32)
@@ -198,7 +201,6 @@
     key_cols = lax.dynamic_slice_in_dim(w_key, key_head * HEAD, HEAD, 1)
     value_cols = lax.dynamic_slice_in_dim(w_value, key_head * HEAD, HEAD, 1)
     exchanged = from_everyone(jnp.concatenate([key_cols, value_cols], axis=1), SP)
-    peers, pieces = exchanged.shape[:2]
 
     out_piece = swapped(w_out.T)
 
@@ -210,51 +212,52 @@
 
     cosine, sine, fine = rope_tables(lax.axis_index(SP) * rows, rows)
 
-    at = lambda *shape: lambda *place: pl.BlockSpec(shape, lambda i: place)
+    held = pl.BlockSpec(memory_space=pltpu.VMEM)
     whole = lambda *shape: pl.BlockSpec(shape, lambda i: (0,) * len(shape))
     part = lambda *shape: pl.BlockSpec(shape, lambda i: (i,) + (0,) * (len(shape) - 1))
     shaped = lambda *shape: jax.ShapeDtypeStruct(shape, bf16)
     tables = [whole(*cosine.shape)] * 2 + [whole(*fine.shape)]
-    normed, query, pool_in = pl.pallas_call(
+    normed, query, pool_in, parts = pl.pallas_call(
         project,
         grid=(rows // ROWS,),
-        in_specs=[part(ROWS, depth), whole(1, depth)] + [whole(*own.shape)] * 2 + tables,
-        out_specs=[part(ROWS, depth), part(ROWS, LANES), part(ROWS, LANES)],
-        out_shape=[shaped(rows, depth), shaped(rows, LANES), shaped(rows, LANES)],
+        in_specs=[part(ROWS, depth), whole(1, depth)] + [held] * 2 + tables,
+        out_specs=[part(ROWS, depth)] + [part(ROWS, LANES)] * 2 + [whole(2 * EDGE, LANES)],
+        out_shape=[shaped(rows, depth)]
+        + [shaped(rows, LANES)] * 2
+        + [shaped(2 * EDGE, LANES)],
         scratch_shapes=[pltpu.VMEM((2 * LANES, depth), bf16)],
         name="project",
         interpret=INTERPRET,
-    )(tokens, norm_gain[None, :], own, other, cosine, sine, fine)
+    )(tokens, norm_gain[None, :], on_chip(own), on_chip(other), cosine, sine, fine)
     exchanged, out_piece, normed = lax.optimization_barrier((exchanged, out_piece, normed))
     own_cols = from_everyone(out_piece, SP)
     kv, send = pl.pallas_call(
         project_kv,
         grid=(rows // KV_ROWS,),
-        in_specs=[part(KV_ROWS, depth), part(KV_ROWS, LANES), whole(peers, pieces, LANES)]
+        in_specs=[part(KV_ROWS, depth), part(KV_ROWS, LANES), held]
         + tables,
         out_specs=[part(KV_ROWS, LANES), whole(QB + EDGE, LANES)],
         out_shape=[shaped(rows, LANES), shaped(QB + EDGE, LANES)],
         name="project_kv",
         interpret=INTERPRET,
-    )(normed, pool_in, exchanged, cosine, sine, fine)
+    )(normed, pool_in, on_chip(exchanged), cosine, sine, fine)
 
     pairs = [(2 * s, 2 * s + 2) for s in range(sp_count - 1)]
     pairs += [(2 * s + 3, 2 * s + 1) for s in range(sp_count - 1)]
     halo = lax.ppermute(send, SP + ("c",), pairs)
     peers_x = lax.axis_size("x")
-    small_rows = at(EDGE, depth)(LANES // EDGE, 0)
     anywhere = pl.BlockSpec(memory_space=pl.ANY)
-    local_specs = [small_rows, small_rows] + [whole(rows, LANES)] * 3
+    local_specs = [whole(2 * EDGE, LANES)] + [whole(rows, LANES)] * 3
 
     def mixed(inner, *more):
         blocks = rows // (2 * QB) - 1 if inner else 1
         return pl.pallas_call(
             functools.partial(mix, inner),
             grid=(1,),
-            in_specs=local_specs + ([] if inner else [whole(QB + EDGE, LANES), anywhere]),
+            in_specs=local_specs + ([] if inner else [held, anywhere]),
             out_specs=anywhere,
             out_shape=shaped(peers_x, rows // 2, 2 * LANES),
-            input_output_aliases={} if inner else {6: 0},
+            input_output_aliases={} if inner else {5: 0},
             scratch_shapes=[
                 pltpu.VMEM((rows + QB, LANES), bf16),
                 pltpu.VMEM((rows + 2 * EDGE, LANES), jnp.float32),
@@ -263,10 +266,10 @@
             ],
             name="mix_inner" if inner else "mix_outer",
             interpret=INTERPRET,
-        )(own, other, query, kv, pool_in, *more)
+        )(parts, query, kv, pool_in, *more)
 
     local = mixed(True)
-    local = mixed(False, halo, local)
+    local = mixed(False, on_chip(halo), local)
 
     local, own_cols = lax.optimization_barrier((local, own_cols))
     other_cols = lax.ppermute(own_cols, "c", [(0, 1), (1, 0)])

time: 105 us -> 104 us (level)
  waiting for transfers between devices: 19.6 us -> 21.8 us
  local copies, waits for them, and re-layouts: 5.68 us -> 4.11 us
  starting transfers between devices: 46.3 us -> 44.9 us
    all_to_all x2, waiting for transfers between devices: 1.82 us -> 3.85 us  [from_everyone(): lax.all_to_all(jnp.broadcast_to(x[None], (peers, *x.shape)), axis, 0, 0,...]
    unnamed x10 -> x2, local copies, waits for them, and re-layouts: 1.47 us -> 0.01 us
    all_to_all x2, starting transfers between devices: 31 us -> 29.7 us  [from_everyone(): lax.all_to_all(jnp.broadcast_to(x[None], (peers, *x.shape)), axis, 0, 0,...]
  transfers between devices with their start and end apart: 7 -> 7, of which waited for: 3 -> 4; matrix products, arithmetic and copies ran while one was open for 3% -> 3% of each run, Pallas kernels for 18% -> 17%
where the time goes in v11:
time: 104 us; the launch traced here: 103 us
  starting transfers between devices  44.9 us (43%)
  waiting for transfers between devices  21.8 us (21%)
  Pallas kernels  17.7 us (17%)
  blocking collectives  11 us (11%)
  local copies, waits for them, and re-layouts  4.11 us (4%)
  other arithmetic  2.16 us (2%)
    all_to_all x2, starting transfers between devices, from_everyone(): lax.all_to_all(jnp.broadcast_to(x[None], (peers, *x.shape)), axis, 0, 0,...  29.7 us
    all_to_all x1, waiting for transfers between devices, body(): joined = lax.all_to_all(local, 'x', 0, 0, tiled=True)  14.8 us
    all_to_all x1, blocking collectives, body(): lax.all_to_all(partial_cols, 'x', split_axis=0, concat_axis=1, tiled=True)  11 us
    pallas_call x1, Pallas kernels, body(): pl.pallas_call(project, grid=(rows // ROWS,), in_specs=[part(ROWS, depth)...  6.95 us
    pallas_call x2, Pallas kernels, mixed(): pl.pallas_call(functools.partial(mix, inner), grid=(1,), in_specs=local_s...  6.77 us
    ppermute x1, starting transfers between devices, body(): other_cols = lax.ppermute(own_cols, 'c', [(0, 1), (1, 0)])  4.51 us
    pallas_call x1, Pallas kernels, body(): pl.pallas_call(project_kv, grid=(rows // KV_ROWS,), in_specs=[part(KV_ROW...  3.93 us
    all_to_all x2, waiting for transfers between devices, from_everyone(): lax.all_to_all(jnp.broadcast_to(x[None], (peers, *x.shape)), axis, 0, 0,...  3.85 us
  transfers between devices with their start and end apart: 7, of which 4 were waited for; matrix products, arithmetic and copies ran while one was open for 3% of the time, Pallas kernels for 17%

profile of v11, /device:TPU:1, one launch (start us, length us, event | category | flops | bytes accessed | tf_op | source)
XLA Modules:
  0.0 103.2 jit_solution(1686236678815817390)
XLA Ops:
  0.0 0.8 constant_dynamic-slice_fusion
  0.9 0.9 broadcast_in_dim.33
  1.8 17.1 %all-to-all-start = ((bf16[64,32,128]{2,1,0:T(8,128)(2,1)}), bf16[64,32,128]{2,1,0:T(8,128)(2,1)S(1)}, u32[]{:S(2)}, u32[]{:S(2)}) async-start(bf16[64,32,128]{2,1,0:T(8,128)(2,1)} %broadcast_in_dim.33), calls=%async_computation | async-start | bytes 1048576 | tf_op jit(solution)/shard_map/all_to_all | solution.py:28
  19.5 0.7 pad_bitcast_fusion
  20.2 1.1 %pad_maximum_fusion.own = bf16[144,2048]{1,0:T(8,128)(2,1)S(1)} fusion(bf16[16,2048]{1,0:T(8,128)(2,1)S(1)} %fusion.12, bf16[64,2048]{1,0:T(8,128)(2,1)} %bitcast.27, bf16[64,2048]{1,0:T(8,128)(2,1)} %bitcast.28), kind=kLoop, calls=%fused_computation.5 | loop fusion | flops 1769472 | bytes 1179648 | tf_op jit(solution)/shard_map/concatenate | solution.py:210
  21.3 2.9 %collective-permute-start = (bf16[144,2048]{1,0:T(8,128)(2,1)S(1)}, bf16[144,2048]{1,0:T(8,128)(2,1)S(1)}, u32[]{:S(2)}, u32[]{:S(2)}) collective-permute-start(bf16[144,2048]{1,0:T(8,128)(2,1)S(1)} %pad_maximum_fusion.own), channel_id=1, source_target_pairs={{0,1},{1,0},{2,3},{3,2},{4,5},{5,4},{6,7},{7,6},{8,9},{9,8},{10,11... | collective-permute-start | bytes 1769480 | tf_op jit(solution)/shard_map/ppermute | solution.py:211
  24.2 3.1 %collective-permute-start.1 = (bf16[32,128]{1,0:T(8,128)(2,1)S(1)}, bf16[32,128]{1,0:T(8,128)(2,1)S(1)}, u32[]{:S(2)}, u32[]{:S(2)}) collective-permute-start(bf16[32,128]{1,0:T(8,128)(2,1)S(1)} %bitcast.30), channel_id=1, source_target_pairs={{0,0},{1,64},{2,128},{3,192},{4,256},{5,320},{6,384},{7,448},{8,8}... | collective-permute-start | bytes 24584 | tf_op jit(solution)/shard_map/ppermute | solution.py:40
  27.3 0.7 negate_select_fusion
  28.0 6.9 %project.1 = (bf16[1024,2048]{1,0:T(8,128)(2,1)}, bf16[1024,128]{1,0:T(8,128)(2,1)}, bf16[1024,128]{1,0:T(8,128)(2,1)}, bf16[32,128]{1,0:T(8,128)(2,1)}) custom-call(bf16[1024,2048]{1,0:T(8,128)(2,1)} %tokens.1, f32[1,2048]{1,0:T(1,128)} %bitcast.29, bf16[144,2048]{1,0:T(8,128)(2,1)S(1)} %pad_maximum_fusion.own, ...), custom_call_target="tpu_custom_call" | custom-call | tf_op jit(solution)/shard_map/project/pallas_call | solution.py:220
  35.0 1.3 %all-to-all-done.ex = bf16[64,32,128]{2,1,0:T(8,128)(2,1)S(1)} async-done(((bf16[64,32,128]{2,1,0:T(8,128)(2,1)}), bf16[64,32,128]{2,1,0:T(8,128)(2,1)S(1)}, u32[]{:S(2)}, u32[]{:S(2)}) %all-to-all-start) | async-done | bytes 524320 | tf_op jit(solution)/shard_map/all_to_all | solution.py:28
  36.3 0.9 broadcast_in_dim.34
  37.2 12.5 %all-to-all-start.1 = ((bf16[64,32,128]{2,1,0:T(8,128)(2,1)}), bf16[64,32,128]{2,1,0:T(8,128)(2,1)S(1)}, u32[]{:S(2)}, u32[]{:S(2)}) async-start(bf16[64,32,128]{2,1,0:T(8,128)(2,1)} %broadcast_in_dim.34), calls=%async_computation.1 | async-start | bytes 1048576 | tf_op jit(solution)/shard_map/all_to_all | solution.py:28
  49.7 3.9 %project_kv.1 = (bf16[1024,128]{1,0:T(8,128)(2,1)}, bf16[144,128]{1,0:T(8,128)(2,1)}) custom-call(bf16[1024,2048]{1,0:T(8,128)(2,1)} %get-tuple-element.19.normed, bf16[1024,128]{1,0:T(8,128)(2,1)} %get-tuple-element.20.pool, bf16[64,32,128]{2,1,0:T(8,128)(2,1)S(1)} %all-to-all-done.ex, f32[8,128]{1,0:T(8,128)} %get-tuple-element.34.cosine, ...), custom_call_target="tpu_custom_call" | custom-call | tf_op jit(solution)/shard_map/project_kv/pallas_call | solution.py:234
  53.6 1.3 %collective-permute-start.2 = (bf16[144,128]{1,0:T(8,128)(2,1)}, bf16[144,128]{1,0:T(8,128)(2,1)S(1)}, u32[]{:S(2)}, u32[]{:S(2)}) collective-permute-start(bf16[144,128]{1,0:T(8,128)(2,1)} %get-tuple-element.23), channel_id=1, source_target_pairs={{0,8},{8,16},{16,24},{24,32},{32,40},{40,48},{48,56},{56,64},{64,7... | collective-permute-start | bytes 110600 | tf_op jit(solution)/shard_map/ppermute | solution.py:247
  54.9 4.2 %mix_inner.1.rest_1_ = bf16[4,512,256]{2,1,0:T(8,128)(2,1)} custom-call(bf16[32,128]{1,0:T(8,128)(2,1)} %get-tuple-element.16.parts, bf16[1024,128]{1,0:T(8,128)(2,1)} %get-tuple-element.17.q, bf16[1024,128]{1,0:T(8,128)(2,1)} %get-tuple-element.22.kv, bf16[1024,128]{1,0:T(8,128)(2,1)} %get-tuple-element.20.pool), custom_call_target="tpu_custom_call" | custom-call | tf_op jit(solution)/shard_map/mix_inner/pallas_call | solution.py:254
  59.1 3.2 %collective-permute-done.2.rest_0_ = bf16[144,128]{1,0:T(8,128)(2,1)S(1)} collective-permute-done((bf16[144,128]{1,0:T(8,128)(2,1)}, bf16[144,128]{1,0:T(8,128)(2,1)S(1)}, u32[]{:S(2)}, u32[]{:S(2)}) %collective-permute-start.2) | collective-permute-done | bytes 36896 | tf_op jit(solution)/shard_map/ppermute | solution.py:247
  62.3 2.6 %mix_outer.1 = bf16[4,512,256]{2,1,0:T(8,128)(2,1)} custom-call(bf16[32,128]{1,0:T(8,128)(2,1)} %get-tuple-element.16.parts, bf16[1024,128]{1,0:T(8,128)(2,1)} %get-tuple-element.17.q, bf16[1024,128]{1,0:T(8,128)(2,1)} %get-tuple-element.22.kv, bf16[1024,128]{1,0:T(8,128)(2,1)} %get-tuple-element.20.pool, ...), custom_call_target="tpu_custom_call", output_to_operand_aliasing={{}: (5, {})} | custom-call | tf_op jit(solution)/shard_map/mix_outer/pallas_call | solution.py:254
  64.9 2.5 %all-to-all-done.1 = bf16[64,32,128]{2,1,0:T(8,128)(2,1)S(1)} async-done(((bf16[64,32,128]{2,1,0:T(8,128)(2,1)}), bf16[64,32,128]{2,1,0:T(8,128)(2,1)S(1)}, u32[]{:S(2)}, u32[]{:S(2)}) %all-to-all-start.1) | async-done | bytes 524320 | tf_op jit(solution)/shard_map/all_to_all | solution.py:28
  67.4 4.5 %collective-permute-start.3 = (bf16[64,32,128]{2,1,0:T(8,128)(2,1)S(1)}, bf16[64,32,128]{2,1,0:T(8,128)(2,1)S(1)}, u32[]{:S(2)}, u32[]{:S(2)}) collective-permute-start(bf16[64,32,128]{2,1,0:T(8,128)(2,1)S(1)} %all-to-all-done.1), channel_id=1, source_target_pairs={{0,1},{1,0},{2,3},{3,2},{4,5},{5,4},{6,7},{7,6},{8,9},{9,8},{10,11... | collective-permute-start | bytes 1572872 | tf_op jit(solution)/shard_map/ppermute | solution.py:275
  72.0 3.5 %all-to-all-start.2 = ((bf16[4,512,256]{2,1,0:T(8,128)(2,1)}), bf16[4,512,256]{2,1,0:T(8,128)(2,1)S(1)}, u32[]{:S(2)}, u32[]{:S(2)}) async-start(bf16[4,512,256]{2,1,0:T(8,128)(2,1)} %mix_outer.1), calls=%async_computation.2 | async-start | bytes 2097152 | tf_op jit(solution)/shard_map/all_to_all | solution.py:276
  75.9 14.8 %all-to-all-done.2 = bf16[4,512,256]{2,1,0:T(8,128)(2,1)S(1)} async-done(((bf16[4,512,256]{2,1,0:T(8,128)(2,1)}), bf16[4,512,256]{2,1,0:T(8,128)(2,1)S(1)}, u32[]{:S(2)}, u32[]{:S(2)}) %all-to-all-start.2) | async-done | bytes 1048608 | tf_op jit(solution)/shard_map/all_to_all | solution.py:276
  90.6 0.7 fusion
  91.4 11.0 %all_to_all.34 = bf16[4,128,512]{2,1,0:T(8,128)(2,1)S(1)} all-to-all(bf16[4,128,512]{2,1,0:T(8,128)(2,1)S(1)} %bitcast.26), channel_id=1, replica_groups=mesh['z'=8,'y'=8,'x'=4,'c'=2] {'x'}, dimensions={0} | all-to-all | bytes 1048576 | tf_op jit(solution)/shard_map/all_to_all | solution.py:290
  102.3 0.8 copy.13
  (14 shorter events, 0.5 us)
Async XLA Ops:
  0.0 24.2 %copy-start = (bf16[128,32]{0,1:T(8,128)(2,1)S(1)}, bf16[128,32]{0,1:T(8,128)(2,1)}, u32[]{:S(2)}) copy-start(bf16[128,32]{0,1:T(8,128)(2,1)} %param.18) | copy-start | bytes 24580
  1.8 34.6 %all-to-all-start = ((bf16[64,32,128]{2,1,0:T(8,128)(2,1)}), bf16[64,32,128]{2,1,0:T(8,128)(2,1)S(1)}, u32[]{:S(2)}, u32[]{:S(2)}) async-start(bf16[64,32,128]{2,1,0:T(8,128)(2,1)} %broadcast_in_dim.33), calls=%async_computation | async-start | bytes 1048576 | tf_op jit(solution)/shard_map/all_to_all | solution.py:28
  21.3 6.7 %collective-permute-start = (bf16[144,2048]{1,0:T(8,128)(2,1)S(1)}, bf16[144,2048]{1,0:T(8,128)(2,1)S(1)}, u32[]{:S(2)}, u32[]{:S(2)}) collective-permute-start(bf16[144,2048]{1,0:T(8,128)(2,1)S(1)} %pad_maximum_fusion.own), channel_id=1, source_target_pairs={{0,1},{1,0},{2,3},{3,2},{4,5},{5,4},{6,7},{7,6},{8,9},{9,8},{10,11... | collective-permute-start | bytes 1769480 | tf_op jit(solution)/shard_map/ppermute | solution.py:211
  24.2 10.8 %collective-permute-start.1 = (bf16[32,128]{1,0:T(8,128)(2,1)S(1)}, bf16[32,128]{1,0:T(8,128)(2,1)S(1)}, u32[]{:S(2)}, u32[]{:S(2)}) collective-permute-start(bf16[32,128]{1,0:T(8,128)(2,1)S(1)} %bitcast.30), channel_id=1, source_target_pairs={{0,0},{1,64},{2,128},{3,192},{4,256},{5,320},{6,384},{7,448},{8,8}... | collective-permute-start | bytes 24584 | tf_op jit(solution)/shard_map/ppermute | solution.py:40
  37.2 30.3 %all-to-all-start.1 = ((bf16[64,32,128]{2,1,0:T(8,128)(2,1)}), bf16[64,32,128]{2,1,0:T(8,128)(2,1)S(1)}, u32[]{:S(2)}, u32[]{:S(2)}) async-start(bf16[64,32,128]{2,1,0:T(8,128)(2,1)} %broadcast_in_dim.34), calls=%async_computation.1 | async-start | bytes 1048576 | tf_op jit(solution)/shard_map/all_to_all | solution.py:28
  53.6 8.6 %collective-permute-start.2 = (bf16[144,128]{1,0:T(8,128)(2,1)}, bf16[144,128]{1,0:T(8,128)(2,1)S(1)}, u32[]{:S(2)}, u32[]{:S(2)}) collective-permute-start(bf16[144,128]{1,0:T(8,128)(2,1)} %get-tuple-element.23), channel_id=1, source_target_pairs={{0,8},{8,16},{16,24},{24,32},{32,40},{40,48},{48,56},{56,64},{64,7... | collective-permute-start | bytes 110600 | tf_op jit(solution)/shard_map/ppermute | solution.py:247
  67.4 8.1 %collective-permute-start.3 = (bf16[64,32,128]{2,1,0:T(8,128)(2,1)S(1)}, bf16[64,32,128]{2,1,0:T(8,128)(2,1)S(1)}, u32[]{:S(2)}, u32[]{:S(2)}) collective-permute-start(bf16[64,32,128]{2,1,0:T(8,128)(2,1)S(1)} %all-to-all-done.1), channel_id=1, source_target_pairs={{0,1},{1,0},{2,3},{3,2},{4,5},{5,4},{6,7},{7,6},{8,9},{9,8},{10,11... | collective-permute-start | bytes 1572872 | tf_op jit(solution)/shard_map/ppermute | solution.py:275
  72.0 18.7 %all-to-all-start.2 = ((bf16[4,512,256]{2,1,0:T(8,128)(2,1)}), bf16[4,512,256]{2,1,0:T(8,128)(2,1)S(1)}, u32[]{:S(2)}, u32[]{:S(2)}) async-start(bf16[4,512,256]{2,1,0:T(8,128)(2,1)} %mix_outer.1), calls=%async_computation.2 | async-start | bytes 2097152 | tf_op jit(solution)/shard_map/all_to_all | solution.py:276

commit v12 on v11

--- a/solution.py
+++ b/solution.py
@@ -99,8 +99,9 @@
     )
     first_block = pl.program_id(0) * (ROWS // QB)
     query = turned(sums[:, :LANES], cosine, sine, fine, first_block)
-    q_out[...] = (query * HEAD ** (-0.5)).astype(jnp.bfloat16)
-    pool_out[...] = sums[:, LANES:].astype(jnp.bfloat16)
+    here = pl.ds(pl.multiple_of(pl.program_id(0) * ROWS, ROWS), ROWS)
+    q_out[here, :] = (query * HEAD ** (-0.5)).astype(jnp.bfloat16)
+    pool_out[here, :] = sums[:, LANES:].astype(jnp.bfloat16)
 
 
 def project_kv(normed, pool, ex, cosine, sine, fine, kv_out, send):
@@ -109,7 +110,7 @@
     lane = lax.broadcasted_iota(jnp.int32, sums.shape, 1)
     kv = jnp.where(lane < HEAD, turned(sums, cosine, sine, fine, step * (rows // QB)), sums)
     kv = kv.astype(jnp.bfloat16)
-    kv_out[...] = kv
+    kv_out[pl.ds(pl.multiple_of(step * rows, rows), rows), :] = kv
 
     @pl.when((step == 0) & (core == 1))
     def _():
@@ -119,7 +120,7 @@
     @pl.when((step == pl.num_programs(0) - 1) & (core == 0))
     def _():
         send[:QB] = kv[rows - QB :]
-        send[QB:] = pool[rows - EDGE :]
+        send[QB:] = pool[pool.shape[0] - EDGE :]
 
 
 def mix(inner, parts, q, kv, pool, *rest):
@@ -216,15 +217,16 @@
     whole = lambda *shape: pl.BlockSpec(shape, lambda i: (0,) * len(shape))
     part = lambda *shape: pl.BlockSpec(shape, lambda i: (i,) + (0,) * (len(shape) - 1))
     shaped = lambda *shape: jax.ShapeDtypeStruct(shape, bf16)
+    kept = lambda *shape: shaped(*shape) if INTERPRET else pltpu.VMEM(shape, bf16)
     tables = [whole(*cosine.shape)] * 2 + [whole(*fine.shape)]
     normed, query, pool_in, parts = pl.pallas_call(
         project,
         grid=(rows // ROWS,),
         in_specs=[part(ROWS, depth), whole(1, depth)] + [held] * 2 + tables,
-        out_specs=[part(ROWS, depth)] + [part(ROWS, LANES)] * 2 + [whole(2 * EDGE, LANES)],
+        out_specs=[part(ROWS, depth)] + [held] * 3,
         out_shape=[shaped(rows, depth)]
-        + [shaped(rows, LANES)] * 2
-        + [shaped(2 * EDGE, LANES)],
+        + [kept(rows, LANES)] * 2
+        + [kept(2 * EDGE, LANES)],
         scratch_shapes=[pltpu.VMEM((2 * LANES, depth), bf16)],
         name="project",
         interpret=INTERPRET,
@@ -234,20 +236,20 @@
     kv, send = pl.pallas_call(
         project_kv,
         grid=(rows // KV_ROWS,),
-        in_specs=[part(KV_ROWS, depth), part(KV_ROWS, LANES), held]
+        in_specs=[part(KV_ROWS, depth), held, held]
         + tables,
-        out_specs=[part(KV_ROWS, LANES), whole(QB + EDGE, LANES)],
-        out_shape=[shaped(rows, LANES), shaped(QB + EDGE, LANES)],
+        out_specs=[held, held],
+        out_shape=[kept(rows, LANES), kept(QB + EDGE, LANES)],
         name="project_kv",
         interpret=INTERPRET,
-    )(normed, pool_in, on_chip(exchanged), cosine, sine, fine)
+    )(normed, on_chip(pool_in), on_chip(exchanged), cosine, sine, fine)
 
     pairs = [(2 * s, 2 * s + 2) for s in range(sp_count - 1)]
     pairs += [(2 * s + 3, 2 * s + 1) for s in range(sp_count - 1)]
     halo = lax.ppermute(send, SP + ("c",), pairs)
     peers_x = lax.axis_size("x")
     anywhere = pl.BlockSpec(memory_space=pl.ANY)
-    local_specs = [whole(2 * EDGE, LANES)] + [whole(rows, LANES)] * 3
+    local_specs = [held] * 4
 
     def mixed(inner, *more):
         blocks = rows // (2 * QB) - 1 if inner else 1
@@ -266,7 +268,7 @@
             ],
             name="mix_inner" if inner else "mix_outer",
             interpret=INTERPRET,
-        )(parts, query, kv, pool_in, *more)
+        )(on_chip(parts), on_chip(query), on_chip(kv), on_chip(pool_in), *more)
 
     local = mixed(True)
     local = mixed(False, on_chip(halo), local)

time: 104 us -> 104 us (level)
  Pallas kernels: 17.7 us -> 15.1 us
  waiting for transfers between devices: 21.8 us -> 24.3 us
    pallas_call x2, Pallas kernels: 6.77 us -> 4.55 us  [mixed(): pl.pallas_call(functools.partial(mix, inner), grid=(1,), in_specs=local_s...]
    ppermute x1, waiting for transfers between devices: 3.17 us -> 4.89 us  [body(): halo = lax.ppermute(send, SP + ('c',), pairs)]
  transfers between devices with their start and end apart: 7 -> 7, of which waited for: 4 -> 4; matrix products, arithmetic and copies ran while one was open for 3% -> 3% of each run, Pallas kernels for 17% -> 15%
where the time goes in v12:
time: 104 us
  starting transfers between devices  45.4 us (44%)
  waiting for transfers between devices  24.3 us (23%)
  Pallas kernels  15.1 us (15%)
  blocking collectives  11 us (11%)
  local copies, waits for them, and re-layouts  4.11 us (4%)
  other arithmetic  2.16 us (2%)
    all_to_all x2, starting transfers between devices, from_everyone(): lax.all_to_all(jnp.broadcast_to(x[None], (peers, *x.shape)), axis, 0, 0,...  30 us
    all_to_all x1, waiting for transfers between devices, body(): joined = lax.all_to_all(local, 'x', 0, 0, tiled=True)  14.8 us
    all_to_all x1, blocking collectives, body(): lax.all_to_all(partial_cols, 'x', split_axis=0, concat_axis=1, tiled=True)  11 us
    pallas_call x1, Pallas kernels, body(): pl.pallas_call(project, grid=(rows // ROWS,), in_specs=[part(ROWS, depth)...  7.28 us
    ppermute x1, waiting for transfers between devices, body(): halo = lax.ppermute(send, SP + ('c',), pairs)  4.89 us
    all_to_all x2, waiting for transfers between devices, from_everyone(): lax.all_to_all(jnp.broadcast_to(x[None], (peers, *x.shape)), axis, 0, 0,...  4.62 us
    ppermute x1, starting transfers between devices, body(): other_cols = lax.ppermute(own_cols, 'c', [(0, 1), (1, 0)])  4.58 us
    pallas_call x2, Pallas kernels, mixed(): pl.pallas_call(functools.partial(mix, inner), grid=(1,), in_specs=local_s...  4.55 us
  transfers between devices with their start and end apart: 7, of which 4 were waited for; matrix products, arithmetic and copies ran while one was open for 3% of the time, Pallas kernels for 15%

profile of v12, /device:TPU:1, one launch (start us, length us, event | category | flops | bytes accessed | tf_op | source)
XLA Modules:
  0.0 103.5 jit_solution(12912928742362810953)
XLA Ops:
  0.0 0.8 constant_dynamic-slice_fusion
  0.9 0.9 broadcast_in_dim.33
  1.8 17.1 %all-to-all-start = ((bf16[64,32,128]{2,1,0:T(8,128)(2,1)}), bf16[64,32,128]{2,1,0:T(8,128)(2,1)S(1)}, u32[]{:S(2)}, u32[]{:S(2)}) async-start(bf16[64,32,128]{2,1,0:T(8,128)(2,1)} %broadcast_in_dim.33), calls=%async_computation | async-start | bytes 1048576 | tf_op jit(solution)/shard_map/all_to_all | solution.py:28
  19.5 0.7 pad_bitcast_fusion
  20.2 1.1 %pad_maximum_fusion.own = bf16[144,2048]{1,0:T(8,128)(2,1)S(1)} fusion(bf16[16,2048]{1,0:T(8,128)(2,1)S(1)} %fusion.12, bf16[64,2048]{1,0:T(8,128)(2,1)} %bitcast.27, bf16[64,2048]{1,0:T(8,128)(2,1)} %bitcast.28), kind=kLoop, calls=%fused_computation.5 | loop fusion | flops 1769472 | bytes 1179648 | tf_op jit(solution)/shard_map/concatenate | solution.py:211
  21.3 2.9 %collective-permute-start = (bf16[144,2048]{1,0:T(8,128)(2,1)S(1)}, bf16[144,2048]{1,0:T(8,128)(2,1)S(1)}, u32[]{:S(2)}, u32[]{:S(2)}) collective-permute-start(bf16[144,2048]{1,0:T(8,128)(2,1)S(1)} %pad_maximum_fusion.own), channel_id=1, source_target_pairs={{0,1},{1,0},{2,3},{3,2},{4,5},{5,4},{6,7},{7,6},{8,9},{9,8},{10,11... | collective-permute-start | bytes 1769480 | tf_op jit(solution)/shard_map/ppermute | solution.py:212
  24.2 3.1 %collective-permute-start.1 = (bf16[32,128]{1,0:T(8,128)(2,1)S(1)}, bf16[32,128]{1,0:T(8,128)(2,1)S(1)}, u32[]{:S(2)}, u32[]{:S(2)}) collective-permute-start(bf16[32,128]{1,0:T(8,128)(2,1)S(1)} %bitcast.30), channel_id=1, source_target_pairs={{0,0},{1,64},{2,128},{3,192},{4,256},{5,320},{6,384},{7,448},{8,8}... | collective-permute-start | bytes 24584 | tf_op jit(solution)/shard_map/ppermute | solution.py:40
  27.3 0.7 negate_select_fusion
  28.0 7.3 %project.1 = (bf16[1024,2048]{1,0:T(8,128)(2,1)}, bf16[1024,128]{1,0:T(8,128)(2,1)S(1)}, bf16[1024,128]{1,0:T(8,128)(2,1)S(1)}, bf16[32,128]{1,0:T(8,128)(2,1)S(1)}) custom-call(bf16[1024,2048]{1,0:T(8,128)(2,1)} %tokens.1, f32[1,2048]{1,0:T(1,128)} %bitcast.29, bf16[144,2048]{1,0:T(8,128)(2,1)S(1)} %pad_maximum_fusion.own, ...), custom_call_target="tpu_custom_call" | custom-call | tf_op jit(solution)/shard_map/project/pallas_call | solution.py:222
  35.3 1.0 all-to-all-done.ex
  36.3 0.9 broadcast_in_dim.34
  37.2 12.9 %all-to-all-start.1 = ((bf16[64,32,128]{2,1,0:T(8,128)(2,1)}), bf16[64,32,128]{2,1,0:T(8,128)(2,1)S(1)}, u32[]{:S(2)}, u32[]{:S(2)}) async-start(bf16[64,32,128]{2,1,0:T(8,128)(2,1)} %broadcast_in_dim.34), calls=%async_computation.1 | async-start | bytes 1048576 | tf_op jit(solution)/shard_map/all_to_all | solution.py:28
  50.0 3.2 %project_kv.1 = (bf16[1024,128]{1,0:T(8,128)(2,1)S(1)}, bf16[144,128]{1,0:T(8,128)(2,1)S(1)}) custom-call(bf16[1024,2048]{1,0:T(8,128)(2,1)} %get-tuple-element.19.normed, bf16[1024,128]{1,0:T(8,128)(2,1)S(1)} %get-tuple-element.20.pool, bf16[64,32,128]{2,1,0:T(8,128)(2,1)S(1)} %all-to-all-done.ex, f32[8,128]{1,0:T(8,128)} %get-tuple-element.34.cosine, ...), custom_call_target="tpu_custom_call" | custom-call | tf_op jit(solution)/shard_map/project_kv/pallas_call | solution.py:236
  53.3 1.3 %collective-permute-start.2 = (bf16[144,128]{1,0:T(8,128)(2,1)S(1)}, bf16[144,128]{1,0:T(8,128)(2,1)S(1)}, u32[]{:S(2)}, u32[]{:S(2)}) collective-permute-start(bf16[144,128]{1,0:T(8,128)(2,1)S(1)} %get-tuple-element.23), channel_id=1, source_target_pairs={{0,8},{8,16},{16,24},{24,32},{32,40},{40,48},{48,56},{56,64},{64,7... | collective-permute-start | bytes 110600 | tf_op jit(solution)/shard_map/ppermute | solution.py:249
  54.6 3.1 %mix_inner.1.rest_1_ = bf16[4,512,256]{2,1,0:T(8,128)(2,1)} custom-call(bf16[32,128]{1,0:T(8,128)(2,1)S(1)} %get-tuple-element.16.parts, bf16[1024,128]{1,0:T(8,128)(2,1)S(1)} %get-tuple-element.17.q, bf16[1024,128]{1,0:T(8,128)(2,1)S(1)} %get-tuple-element.22.kv, bf16[1024,128]{1,0:T(8,128)(2,1)S(1)} %get-tuple-element.20.pool), custom_call_target="tpu_custom_call" | custom-call | tf_op jit(solution)/shard_map/mix_inner/pallas_call | solution.py:256
  57.7 4.9 %collective-permute-done.2.rest_0_ = bf16[144,128]{1,0:T(8,128)(2,1)S(1)} collective-permute-done((bf16[144,128]{1,0:T(8,128)(2,1)S(1)}, bf16[144,128]{1,0:T(8,128)(2,1)S(1)}, u32[]{:S(2)}, u32[]{:S(2)}) %collective-permute-start.2) | collective-permute-done | bytes 36896 | tf_op jit(solution)/shard_map/ppermute | solution.py:249
  62.6 1.5 %mix_outer.1 = bf16[4,512,256]{2,1,0:T(8,128)(2,1)} custom-call(bf16[32,128]{1,0:T(8,128)(2,1)S(1)} %get-tuple-element.16.parts, bf16[1024,128]{1,0:T(8,128)(2,1)S(1)} %get-tuple-element.17.q, bf16[1024,128]{1,0:T(8,128)(2,1)S(1)} %get-tuple-element.22.kv, bf16[1024,128]{1,0:T(8,128)(2,1)S(1)} %get-tuple-element.20.pool, ...), custom_call_target="tpu_custom_call", output_to_operand_aliasing={{}: (5, {})} | custom-call | tf_op jit(solution)/shard_map/mix_outer/pallas_call | solution.py:256
  64.1 3.6 %all-to-all-done.1 = bf16[64,32,128]{2,1,0:T(8,128)(2,1)S(1)} async-done(((bf16[64,32,128]{2,1,0:T(8,128)(2,1)}), bf16[64,32,128]{2,1,0:T(8,128)(2,1)S(1)}, u32[]{:S(2)}, u32[]{:S(2)}) %all-to-all-start.1) | async-done | bytes 524320 | tf_op jit(solution)/shard_map/all_to_all | solution.py:28
  67.7 4.6 %collective-permute-start.3 = (bf16[64,32,128]{2,1,0:T(8,128)(2,1)S(1)}, bf16[64,32,128]{2,1,0:T(8,128)(2,1)S(1)}, u32[]{:S(2)}, u32[]{:S(2)}) collective-permute-start(bf16[64,32,128]{2,1,0:T(8,128)(2,1)S(1)} %all-to-all-done.1), channel_id=1, source_target_pairs={{0,1},{1,0},{2,3},{3,2},{4,5},{5,4},{6,7},{7,6},{8,9},{9,8},{10,11... | collective-permute-start | bytes 1572872 | tf_op jit(solution)/shard_map/ppermute | solution.py:277
  72.3 3.5 %all-to-all-start.2 = ((bf16[4,512,256]{2,1,0:T(8,128)(2,1)}), bf16[4,512,256]{2,1,0:T(8,128)(2,1)S(1)}, u32[]{:S(2)}, u32[]{:S(2)}) async-start(bf16[4,512,256]{2,1,0:T(8,128)(2,1)} %mix_outer.1), calls=%async_computation.2 | async-start | bytes 2097152 | tf_op jit(solution)/shard_map/all_to_all | solution.py:278
  76.2 14.8 %all-to-all-done.2 = bf16[4,512,256]{2,1,0:T(8,128)(2,1)S(1)} async-done(((bf16[4,512,256]{2,1,0:T(8,128)(2,1)}), bf16[4,512,256]{2,1,0:T(8,128)(2,1)S(1)}, u32[]{:S(2)}, u32[]{:S(2)}) %all-to-all-start.2) | async-done | bytes 1048608 | tf_op jit(solution)/shard_map/all_to_all | solution.py:278
  91.0 0.7 fusion
  91.7 11.0 %all_to_all.34 = bf16[4,128,512]{2,1,0:T(8,128)(2,1)S(1)} all-to-all(bf16[4,128,512]{2,1,0:T(8,128)(2,1)S(1)} %bitcast.26), channel_id=1, replica_groups=mesh['z'=8,'y'=8,'x'=4,'c'=2] {'x'}, dimensions={0} | all-to-all | bytes 1048576 | tf_op jit(solution)/shard_map/all_to_all | solution.py:292
  102.7 0.8 copy.13
  (14 shorter events, 0.5 us)
Async XLA Ops:
  0.0 24.2 %copy-start = (bf16[128,32]{0,1:T(8,128)(2,1)S(1)}, bf16[128,32]{0,1:T(8,128)(2,1)}, u32[]{:S(2)}) copy-start(bf16[128,32]{0,1:T(8,128)(2,1)} %param.18) | copy-start | bytes 24580
  1.8 34.6 %all-to-all-start = ((bf16[64,32,128]{2,1,0:T(8,128)(2,1)}), bf16[64,32,128]{2,1,0:T(8,128)(2,1)S(1)}, u32[]{:S(2)}, u32[]{:S(2)}) async-start(bf16[64,32,128]{2,1,0:T(8,128)(2,1)} %broadcast_in_dim.33), calls=%async_computation | async-start | bytes 1048576 | tf_op jit(solution)/shard_map/all_to_all | solution.py:28
  21.3 6.7 %collective-permute-start = (bf16[144,2048]{1,0:T(8,128)(2,1)S(1)}, bf16[144,2048]{1,0:T(8,128)(2,1)S(1)}, u32[]{:S(2)}, u32[]{:S(2)}) collective-permute-start(bf16[144,2048]{1,0:T(8,128)(2,1)S(1)} %pad_maximum_fusion.own), channel_id=1, source_target_pairs={{0,1},{1,0},{2,3},{3,2},{4,5},{5,4},{6,7},{7,6},{8,9},{9,8},{10,11... | collective-permute-start | bytes 1769480 | tf_op jit(solution)/shard_map/ppermute | solution.py:212
  24.2 11.2 %collective-permute-start.1 = (bf16[32,128]{1,0:T(8,128)(2,1)S(1)}, bf16[32,128]{1,0:T(8,128)(2,1)S(1)}, u32[]{:S(2)}, u32[]{:S(2)}) collective-permute-start(bf16[32,128]{1,0:T(8,128)(2,1)S(1)} %bitcast.30), channel_id=1, source_target_pairs={{0,0},{1,64},{2,128},{3,192},{4,256},{5,320},{6,384},{7,448},{8,8}... | collective-permute-start | bytes 24584 | tf_op jit(solution)/shard_map/ppermute | solution.py:40
  37.2 30.5 %all-to-all-start.1 = ((bf16[64,32,128]{2,1,0:T(8,128)(2,1)}), bf16[64,32,128]{2,1,0:T(8,128)(2,1)S(1)}, u32[]{:S(2)}, u32[]{:S(2)}) async-start(bf16[64,32,128]{2,1,0:T(8,128)(2,1)} %broadcast_in_dim.34), calls=%async_computation.1 | async-start | bytes 1048576 | tf_op jit(solution)/shard_map/all_to_all | solution.py:28
  53.3 9.3 %collective-permute-start.2 = (bf16[144,128]{1,0:T(8,128)(2,1)S(1)}, bf16[144,128]{1,0:T(8,128)(2,1)S(1)}, u32[]{:S(2)}, u32[]{:S(2)}) collective-permute-start(bf16[144,128]{1,0:T(8,128)(2,1)S(1)} %get-tuple-element.23), channel_id=1, source_target_pairs={{0,8},{8,16},{16,24},{24,32},{32,40},{40,48},{48,56},{56,64},{64,7... | collective-permute-start | bytes 110600 | tf_op jit(solution)/shard_map/ppermute | solution.py:249
  67.7 8.2 %collective-permute-start.3 = (bf16[64,32,128]{2,1,0:T(8,128)(2,1)S(1)}, bf16[64,32,128]{2,1,0:T(8,128)(2,1)S(1)}, u32[]{:S(2)}, u32[]{:S(2)}) collective-permute-start(bf16[64,32,128]{2,1,0:T(8,128)(2,1)S(1)} %all-to-all-done.1), channel_id=1, source_target_pairs={{0,1},{1,0},{2,3},{3,2},{4,5},{5,4},{6,7},{7,6},{8,9},{9,8},{10,11... | collective-permute-start | bytes 1572872 | tf_op jit(solution)/shard_map/ppermute | solution.py:277
  72.3 18.7 %all-to-all-start.2 = ((bf16[4,512,256]{2,1,0:T(8,128)(2,1)}), bf16[4,512,256]{2,1,0:T(8,128)(2,1)S(1)}, u32[]{:S(2)}, u32[]{:S(2)}) async-start(bf16[4,512,256]{2,1,0:T(8,128)(2,1)} %mix_outer.1), calls=%async_computation.2 | async-start | bytes 2097152 | tf_op jit(solution)/shard_map/all_to_all | solution.py:278

commit v13 on v12

--- a/solution.py
+++ b/solution.py
@@ -202,6 +202,7 @@
     key_cols = lax.dynamic_slice_in_dim(w_key, key_head * HEAD, HEAD, 1)
     value_cols = lax.dynamic_slice_in_dim(w_value, key_head * HEAD, HEAD, 1)
     exchanged = from_everyone(jnp.concatenate([key_cols, value_cols], axis=1), SP)
+    peers, _ = exchanged.shape[:2]
 
     out_piece = swapped(w_out.T)
 
@@ -231,8 +232,9 @@
         name="project",
         interpret=INTERPRET,
     )(tokens, norm_gain[None, :], on_chip(own), on_chip(other), cosine, sine, fine)
-    exchanged, out_piece, normed = lax.optimization_barrier((exchanged, out_piece, normed))
-    own_cols = from_everyone(out_piece, SP)
+    spread = jnp.broadcast_to(out_piece[None], (peers, *out_piece.shape))
+    exchanged, spread, normed = lax.optimization_barrier((exchanged, spread, normed))
+    own_cols = lax.all_to_all(spread, SP, 0, 0, tiled=True)
     kv, send = pl.pallas_call(
         project_kv,
         grid=(rows // KV_ROWS,),

time: 104 us -> 104 us (level)
    all_to_all x2 -> x1, starting transfers between devices: 30 us -> 17.1 us  [from_everyone(): lax.all_to_all(jnp.broadcast_to(x[None], (peers, *x.shape)), axis, 0, 0,...]
    all_to_all x0 -> x1, starting transfers between devices: none -> 12.9 us  [body(): own_cols = lax.all_to_all(spread, SP, 0, 0, tiled=True)]
    all_to_all x0 -> x1, waiting for transfers between devices: none -> 3.64 us  [body(): own_cols = lax.all_to_all(spread, SP, 0, 0, tiled=True)]
    all_to_all x2 -> x1, waiting for transfers between devices: 4.62 us -> 0.98 us  [from_everyone(): lax.all_to_all(jnp.broadcast_to(x[None], (peers, *x.shape)), axis, 0, 0,...]
where the time goes in v13:
time: 104 us
  starting transfers between devices  45.4 us (44%)
  waiting for transfers between devices  24.3 us (23%)
  Pallas kernels  15.1 us (15%)
  blocking collectives  11 us (11%)
  local copies, waits for them, and re-layouts  4.11 us (4%)
  other arithmetic  2.16 us (2%)
    all_to_all x1, starting transfers between devices, from_everyone(): lax.all_to_all(jnp.broadcast_to(x[None], (peers, *x.shape)), axis, 0, 0,...  17.1 us
    all_to_all x1, waiting for transfers between devices, body(): joined = lax.all_to_all(local, 'x', 0, 0, tiled=True)  14.8 us
    all_to_all x1, starting transfers between devices, body(): own_cols = lax.all_to_all(spread, SP, 0, 0, tiled=True)  12.9 us
    all_to_all x1, blocking collectives, body(): lax.all_to_all(partial_cols, 'x', split_axis=0, concat_axis=1, tiled=True)  11 us
    pallas_call x1, Pallas kernels, body(): pl.pallas_call(project, grid=(rows // ROWS,), in_specs=[part(ROWS, depth)...  7.28 us
    ppermute x1, waiting for transfers between devices, body(): halo = lax.ppermute(send, SP + ('c',), pairs)  4.89 us
    ppermute x1, starting transfers between devices, body(): other_cols = lax.ppermute(own_cols, 'c', [(0, 1), (1, 0)])  4.58 us
    pallas_call x2, Pallas kernels, mixed(): pl.pallas_call(functools.partial(mix, inner), grid=(1,), in_specs=local_s...  4.55 us
  transfers between devices with their start and end apart: 7, of which 4 were waited for; matrix products, arithmetic and copies ran while one was open for 3% of the time, Pallas kernels for 15%

profile of v13, /device:TPU:1, one launch (start us, length us, event | category | flops | bytes accessed | tf_op | source)
XLA Modules:
  0.0 103.5 jit_solution(12912928742362810953)
XLA Ops:
  0.0 0.8 constant_dynamic-slice_fusion
  0.9 0.9 broadcast_in_dim.33
  1.8 17.1 %all-to-all-start = ((bf16[64,32,128]{2,1,0:T(8,128)(2,1)}), bf16[64,32,128]{2,1,0:T(8,128)(2,1)S(1)}, u32[]{:S(2)}, u32[]{:S(2)}) async-start(bf16[64,32,128]{2,1,0:T(8,128)(2,1)} %broadcast_in_dim.33), calls=%async_computation | async-start | bytes 1048576 | tf_op jit(solution)/shard_map/all_to_all | solution.py:28
  19.5 0.7 pad_bitcast_fusion
  20.2 1.1 %pad_maximum_fusion.own = bf16[144,2048]{1,0:T(8,128)(2,1)S(1)} fusion(bf16[16,2048]{1,0:T(8,128)(2,1)S(1)} %fusion.12, bf16[64,2048]{1,0:T(8,128)(2,1)} %bitcast.27, bf16[64,2048]{1,0:T(8,128)(2,1)} %bitcast.28), kind=kLoop, calls=%fused_computation.5 | loop fusion | flops 1769472 | bytes 1179648 | tf_op jit(solution)/shard_map/concatenate | solution.py:212
  21.3 2.9 %collective-permute-start = (bf16[144,2048]{1,0:T(8,128)(2,1)S(1)}, bf16[144,2048]{1,0:T(8,128)(2,1)S(1)}, u32[]{:S(2)}, u32[]{:S(2)}) collective-permute-start(bf16[144,2048]{1,0:T(8,128)(2,1)S(1)} %pad_maximum_fusion.own), channel_id=1, source_target_pairs={{0,1},{1,0},{2,3},{3,2},{4,5},{5,4},{6,7},{7,6},{8,9},{9,8},{10,11... | collective-permute-start | bytes 1769480 | tf_op jit(solution)/shard_map/ppermute | solution.py:213
  24.2 3.1 %collective-permute-start.1 = (bf16[32,128]{1,0:T(8,128)(2,1)S(1)}, bf16[32,128]{1,0:T(8,128)(2,1)S(1)}, u32[]{:S(2)}, u32[]{:S(2)}) collective-permute-start(bf16[32,128]{1,0:T(8,128)(2,1)S(1)} %bitcast.30), channel_id=1, source_target_pairs={{0,0},{1,64},{2,128},{3,192},{4,256},{5,320},{6,384},{7,448},{8,8}... | collective-permute-start | bytes 24584 | tf_op jit(solution)/shard_map/ppermute | solution.py:40
  27.3 0.7 negate_select_fusion
  28.0 7.3 %project.1 = (bf16[1024,2048]{1,0:T(8,128)(2,1)}, bf16[1024,128]{1,0:T(8,128)(2,1)S(1)}, bf16[1024,128]{1,0:T(8,128)(2,1)S(1)}, bf16[32,128]{1,0:T(8,128)(2,1)S(1)}) custom-call(bf16[1024,2048]{1,0:T(8,128)(2,1)} %tokens.1, f32[1,2048]{1,0:T(1,128)} %bitcast.29, bf16[144,2048]{1,0:T(8,128)(2,1)S(1)} %pad_maximum_fusion.own, ...), custom_call_target="tpu_custom_call" | custom-call | tf_op jit(solution)/shard_map/project/pallas_call | solution.py:223
  35.3 1.0 all-to-all-done.ex
  36.3 0.9 broadcast_in_dim.34
  37.2 12.9 %all-to-all-start.1 = ((bf16[64,32,128]{2,1,0:T(8,128)(2,1)}), bf16[64,32,128]{2,1,0:T(8,128)(2,1)S(1)}, u32[]{:S(2)}, u32[]{:S(2)}) async-start(bf16[64,32,128]{2,1,0:T(8,128)(2,1)} %broadcast_in_dim.34), calls=%async_computation.1 | async-start | bytes 1048576 | tf_op jit(solution)/shard_map/all_to_all | solution.py:237
  50.0 3.2 %project_kv.1 = (bf16[1024,128]{1,0:T(8,128)(2,1)S(1)}, bf16[144,128]{1,0:T(8,128)(2,1)S(1)}) custom-call(bf16[1024,2048]{1,0:T(8,128)(2,1)} %get-tuple-element.19.normed, bf16[1024,128]{1,0:T(8,128)(2,1)S(1)} %get-tuple-element.20.pool, bf16[64,32,128]{2,1,0:T(8,128)(2,1)S(1)} %all-to-all-done.ex, f32[8,128]{1,0:T(8,128)} %get-tuple-element.34.cosine, ...), custom_call_target="tpu_custom_call" | custom-call | tf_op jit(solution)/shard_map/project_kv/pallas_call | solution.py:238
  53.3 1.3 %collective-permute-start.2 = (bf16[144,128]{1,0:T(8,128)(2,1)S(1)}, bf16[144,128]{1,0:T(8,128)(2,1)S(1)}, u32[]{:S(2)}, u32[]{:S(2)}) collective-permute-start(bf16[144,128]{1,0:T(8,128)(2,1)S(1)} %get-tuple-element.23), channel_id=1, source_target_pairs={{0,8},{8,16},{16,24},{24,32},{32,40},{40,48},{48,56},{56,64},{64,7... | collective-permute-start | bytes 110600 | tf_op jit(solution)/shard_map/ppermute | solution.py:251
  54.6 3.1 %mix_inner.1.rest_1_ = bf16[4,512,256]{2,1,0:T(8,128)(2,1)} custom-call(bf16[32,128]{1,0:T(8,128)(2,1)S(1)} %get-tuple-element.16.parts, bf16[1024,128]{1,0:T(8,128)(2,1)S(1)} %get-tuple-element.17.q, bf16[1024,128]{1,0:T(8,128)(2,1)S(1)} %get-tuple-element.22.kv, bf16[1024,128]{1,0:T(8,128)(2,1)S(1)} %get-tuple-element.20.pool), custom_call_target="tpu_custom_call" | custom-call | tf_op jit(solution)/shard_map/mix_inner/pallas_call | solution.py:258
  57.7 4.9 %collective-permute-done.2.rest_0_ = bf16[144,128]{1,0:T(8,128)(2,1)S(1)} collective-permute-done((bf16[144,128]{1,0:T(8,128)(2,1)S(1)}, bf16[144,128]{1,0:T(8,128)(2,1)S(1)}, u32[]{:S(2)}, u32[]{:S(2)}) %collective-permute-start.2) | collective-permute-done | bytes 36896 | tf_op jit(solution)/shard_map/ppermute | solution.py:251
  62.6 1.5 %mix_outer.1 = bf16[4,512,256]{2,1,0:T(8,128)(2,1)} custom-call(bf16[32,128]{1,0:T(8,128)(2,1)S(1)} %get-tuple-element.16.parts, bf16[1024,128]{1,0:T(8,128)(2,1)S(1)} %get-tuple-element.17.q, bf16[1024,128]{1,0:T(8,128)(2,1)S(1)} %get-tuple-element.22.kv, bf16[1024,128]{1,0:T(8,128)(2,1)S(1)} %get-tuple-element.20.pool, ...), custom_call_target="tpu_custom_call", output_to_operand_aliasing={{}: (5, {})} | custom-call | tf_op jit(solution)/shard_map/mix_outer/pallas_call | solution.py:258
  64.1 3.6 %all-to-all-done.1 = bf16[64,32,128]{2,1,0:T(8,128)(2,1)S(1)} async-done(((bf16[64,32,128]{2,1,0:T(8,128)(2,1)}), bf16[64,32,128]{2,1,0:T(8,128)(2,1)S(1)}, u32[]{:S(2)}, u32[]{:S(2)}) %all-to-all-start.1) | async-done | bytes 524320 | tf_op jit(solution)/shard_map/all_to_all | solution.py:237
  67.7 4.6 %collective-permute-start.3 = (bf16[64,32,128]{2,1,0:T(8,128)(2,1)S(1)}, bf16[64,32,128]{2,1,0:T(8,128)(2,1)S(1)}, u32[]{:S(2)}, u32[]{:S(2)}) collective-permute-start(bf16[64,32,128]{2,1,0:T(8,128)(2,1)S(1)} %all-to-all-done.1), channel_id=1, source_target_pairs={{0,1},{1,0},{2,3},{3,2},{4,5},{5,4},{6,7},{7,6},{8,9},{9,8},{10,11... | collective-permute-start | bytes 1572872 | tf_op jit(solution)/shard_map/ppermute | solution.py:279
  72.3 3.5 %all-to-all-start.2 = ((bf16[4,512,256]{2,1,0:T(8,128)(2,1)}), bf16[4,512,256]{2,1,0:T(8,128)(2,1)S(1)}, u32[]{:S(2)}, u32[]{:S(2)}) async-start(bf16[4,512,256]{2,1,0:T(8,128)(2,1)} %mix_outer.1), calls=%async_computation.2 | async-start | bytes 2097152 | tf_op jit(solution)/shard_map/all_to_all | solution.py:280
  76.2 14.8 %all-to-all-done.2 = bf16[4,512,256]{2,1,0:T(8,128)(2,1)S(1)} async-done(((bf16[4,512,256]{2,1,0:T(8,128)(2,1)}), bf16[4,512,256]{2,1,0:T(8,128)(2,1)S(1)}, u32[]{:S(2)}, u32[]{:S(2)}) %all-to-all-start.2) | async-done | bytes 1048608 | tf_op jit(solution)/shard_map/all_to_all | solution.py:280
  91.0 0.7 fusion
  91.7 11.0 %all_to_all.34 = bf16[4,128,512]{2,1,0:T(8,128)(2,1)S(1)} all-to-all(bf16[4,128,512]{2,1,0:T(8,128)(2,1)S(1)} %bitcast.26), channel_id=1, replica_groups=mesh['z'=8,'y'=8,'x'=4,'c'=2] {'x'}, dimensions={0} | all-to-all | bytes 1048576 | tf_op jit(solution)/shard_map/all_to_all | solution.py:294
  102.7 0.8 copy.13
  (14 shorter events, 0.5 us)
Async XLA Ops:
  0.0 24.2 %copy-start = (bf16[128,32]{0,1:T(8,128)(2,1)S(1)}, bf16[128,32]{0,1:T(8,128)(2,1)}, u32[]{:S(2)}) copy-start(bf16[128,32]{0,1:T(8,128)(2,1)} %param.18) | copy-start | bytes 24580
  1.8 34.6 %all-to-all-start = ((bf16[64,32,128]{2,1,0:T(8,128)(2,1)}), bf16[64,32,128]{2,1,0:T(8,128)(2,1)S(1)}, u32[]{:S(2)}, u32[]{:S(2)}) async-start(bf16[64,32,128]{2,1,0:T(8,128)(2,1)} %broadcast_in_dim.33), calls=%async_computation | async-start | bytes 1048576 | tf_op jit(solution)/shard_map/all_to_all | solution.py:28
  21.3 6.7 %collective-permute-start = (bf16[144,2048]{1,0:T(8,128)(2,1)S(1)}, bf16[144,2048]{1,0:T(8,128)(2,1)S(1)}, u32[]{:S(2)}, u32[]{:S(2)}) collective-permute-start(bf16[144,2048]{1,0:T(8,128)(2,1)S(1)} %pad_maximum_fusion.own), channel_id=1, source_target_pairs={{0,1},{1,0},{2,3},{3,2},{4,5},{5,4},{6,7},{7,6},{8,9},{9,8},{10,11... | collective-permute-start | bytes 1769480 | tf_op jit(solution)/shard_map/ppermute | solution.py:213
  24.2 11.2 %collective-permute-start.1 = (bf16[32,128]{1,0:T(8,128)(2,1)S(1)}, bf16[32,128]{1,0:T(8,128)(2,1)S(1)}, u32[]{:S(2)}, u32[]{:S(2)}) collective-permute-start(bf16[32,128]{1,0:T(8,128)(2,1)S(1)} %bitcast.30), channel_id=1, source_target_pairs={{0,0},{1,64},{2,128},{3,192},{4,256},{5,320},{6,384},{7,448},{8,8}... | collective-permute-start | bytes 24584 | tf_op jit(solution)/shard_map/ppermute | solution.py:40
  37.2 30.5 %all-to-all-start.1 = ((bf16[64,32,128]{2,1,0:T(8,128)(2,1)}), bf16[64,32,128]{2,1,0:T(8,128)(2,1)S(1)}, u32[]{:S(2)}, u32[]{:S(2)}) async-start(bf16[64,32,128]{2,1,0:T(8,128)(2,1)} %broadcast_in_dim.34), calls=%async_computation.1 | async-start | bytes 1048576 | tf_op jit(solution)/shard_map/all_to_all | solution.py:237
  53.3 9.3 %collective-permute-start.2 = (bf16[144,128]{1,0:T(8,128)(2,1)S(1)}, bf16[144,128]{1,0:T(8,128)(2,1)S(1)}, u32[]{:S(2)}, u32[]{:S(2)}) collective-permute-start(bf16[144,128]{1,0:T(8,128)(2,1)S(1)} %get-tuple-element.23), channel_id=1, source_target_pairs={{0,8},{8,16},{16,24},{24,32},{32,40},{40,48},{48,56},{56,64},{64,7... | collective-permute-start | bytes 110600 | tf_op jit(solution)/shard_map/ppermute | solution.py:251
  67.7 8.2 %collective-permute-start.3 = (bf16[64,32,128]{2,1,0:T(8,128)(2,1)S(1)}, bf16[64,32,128]{2,1,0:T(8,128)(2,1)S(1)}, u32[]{:S(2)}, u32[]{:S(2)}) collective-permute-start(bf16[64,32,128]{2,1,0:T(8,128)(2,1)S(1)} %all-to-all-done.1), channel_id=1, source_target_pairs={{0,1},{1,0},{2,3},{3,2},{4,5},{5,4},{6,7},{7,6},{8,9},{9,8},{10,11... | collective-permute-start | bytes 1572872 | tf_op jit(solution)/shard_map/ppermute | solution.py:279
  72.3 18.7 %all-to-all-start.2 = ((bf16[4,512,256]{2,1,0:T(8,128)(2,1)}), bf16[4,512,256]{2,1,0:T(8,128)(2,1)S(1)}, u32[]{:S(2)}, u32[]{:S(2)}) async-start(bf16[4,512,256]{2,1,0:T(8,128)(2,1)} %mix_outer.1), calls=%async_computation.2 | async-start | bytes 2097152 | tf_op jit(solution)/shard_map/all_to_all | solution.py:280
